TPU v7x, 32 devices: a whole 2x2x4 slice. The times are simulated.
32 devices in a mesh: sp: 16 (over z, y, x), tp: 2 (over core).
Axes of the slice: x: 2, y: 2, z: 4, core: 2. Of those that a mesh axis runs over, the one named last changes fastest.
Arguments:
- tokens: bfloat16 [4096, 2048], P('sp', 'tp'), may hold values from -6 to 6
- norm_gain: float32 [2048], replicated, may hold values from 0.1 to 1.9
- glu_value: bfloat16 [2048, 2048], P('sp', 'tp'), may hold values from -0.125 to 0.125
- glu_gate: bfloat16 [2048, 2048], P('sp', 'tp'), may hold values from -0.125 to 0.125
- conv_taps: float32 [31, 2048], P(None, 'tp'), may hold values from -11 to 11
- ln_gain: float32 [2048], P('tp'), may hold values from 0.1 to 1.9
- ln_bias: float32 [2048], P('tp'), may hold values from -3 to 3
- query_weight: bfloat16 [2048, 2048], P('sp', 'tp'), may hold values from -0.125 to 0.125
- key_weight: bfloat16 [2048, 2048], P('sp', 'tp'), may hold values from -0.125 to 0.125
- value_weight: bfloat16 [2048, 2048], P('sp', 'tp'), may hold values from -0.125 to 0.125
- gate_weight: bfloat16 [2048, 32], replicated, may hold values from -0.125 to 0.125
- gate_bias: float32 [32], replicated, may hold values from -1 to 110
- log_decay_extra: float32 [4096, 16], P('sp'), may hold values from -1.3 to 0
- mem_gain: float32 [2048], P('tp'), may hold values from 0.1 to 1.9
- out_conv: bfloat16 [2048, 2048], P('tp'), may hold values from -0.125 to 0.125
- out_mem: bfloat16 [2048, 2048], P('tp'), may hold values from -0.125 to 0.125
Outputs:
- mixed: bfloat16 [4096, 2048], P(('sp', 'tp'))
All inputs are finite; a program needn't handle non-finite values.
Results may differ from a plain program's by a relative error of at most 0.015.
Values may be sent and summed in bfloat16 or wider, within the bound.
A program may use at most 128 MiB of HBM per device.

v0:
```python
import functools
import math

import jax
import jax.numpy as jnp
from jax import lax
from jax.experimental import pallas as pl
from jax.experimental.pallas import tpu as pltpu
from jax.sharding import Mesh, PartitionSpec as P

MEMORY_HEADS = 8
HEAD = 256
KW = 31

EPS = 1e-06
PRECISE = lax.Precision.HIGHEST


def parts_of(x):
    first = lax.reduce_precision(x, 8, 7)
    rest = x - first
    second = lax.reduce_precision(rest, 8, 7)
    third = rest - second
    return [p.astype(jnp.bfloat16) for p in (first, second, third)]


def whole_of(a, b, c):
    return a.astype(jnp.float32) + b.astype(jnp.float32) + c.astype(jnp.float32)


MESH = pl.DeviceIdType.MESH


def exchange_kernel(outer, inner, tp, count, *refs):
    tokens, extra = refs[:2]
    weights = refs[2 : 2 + count]
    whole, extras, pieces, stage_w, stage_t, stage_e = refs[2 + count : 8 + count]
    local, a2a_s, a2a_r, tok_s, tok_r, ext_s, ext_r, half_s, half_r, ring_s, ring_r = refs[8 + count :]
    o, i, t = lax.axis_index("outer"), lax.axis_index("inner"), lax.axis_index("tp")
    right, left = lax.rem(o + 1, outer), lax.rem(o + outer - 1, outer)
    rows, half = tokens.shape
    depth = weights[0].shape[0]
    width = pieces.shape[2]

    barrier = pltpu.get_barrier_semaphore()
    greeted = [(o, lax.rem(i + k, inner), t) for k in range(1, inner)]
    greeted += [(o, i, lax.rem(t + k, tp)) for k in range(1, tp)]
    greeted += [(right, i, t), (left, i, t)]
    for device in greeted:
        pl.semaphore_signal(barrier, inc=1, device_id=device, device_id_type=MESH)
    pl.semaphore_wait(barrier, len(greeted))

    def columns(index):
        return pl.ds(pl.multiple_of(index * width, width), width)

    def piece(owner, index):
        start = pl.multiple_of((owner * inner + index) * depth, depth)
        return pieces.at[:, pl.ds(start, depth), :]

    def block(index, core):
        return whole.at[
            pl.ds(pl.multiple_of(index * rows, rows), rows),
            pl.ds(pl.multiple_of(core * half, half), half),
        ]

    def remote(src, dst, send, recv, device):
        return pltpu.make_async_remote_copy(
            src_ref=src, dst_ref=dst, send_sem=send, recv_sem=recv,
            device_id=device, device_id_type=MESH,
        )

    sends = []

    def start(copy):
        copy.start()
        sends.append(copy)

    staged = [
        pltpu.make_async_copy(weights[j].at[:, columns(i)], stage_w.at[j], local.at[j])
        for j in range(count)
    ]
    staged.append(pltpu.make_async_copy(tokens, stage_t, local.at[count]))
    staged.append(pltpu.make_async_copy(extra, stage_e, local.at[count + 1]))
    for copy in staged:
        copy.start()

    def a2a(k, j):
        peer = lax.rem(i + k, inner)
        start_row = pl.multiple_of((o * inner + i) * depth, depth)
        return remote(
            weights[j].at[:, columns(peer)], pieces.at[j, pl.ds(start_row, depth), :],
            a2a_s.at[k - 1, j], a2a_r.at[k - 1, j], (o, peer, t),
        )

    def ring(way, distance, k, src=None):
        index = lax.rem(i + inner - k, inner)
        back = outer - (distance - 1) if way == 0 else distance - 1
        owner = lax.rem(o + back, outer)
        target = right if way == 0 else left
        return remote(
            piece(owner, index) if src is None else src, piece(owner, index),
            ring_s.at[way, distance - 1, k], ring_r.at[way, distance - 1, k], (target, i, t),
        )

    far = outer // 2

    def uses(way, distance, k):
        if 2 * distance < outer:
            return True
        return (k < inner // 2) == (way == 0)

    def tok(k):
        peer = lax.rem(i + k, inner)
        return remote(tokens, block(i, t), tok_s.at[k - 1], tok_r.at[k - 1], (o, peer, t))

    def ext(k):
        peer = lax.rem(i + k, inner)
        return remote(extra, extras.at[i], ext_s.at[k - 1], ext_r.at[k - 1], (o, peer, t))

    def hand(k, c, src=None):
        index = lax.rem(i + inner - k, inner)
        other = lax.rem(t + c, tp)
        return remote(
            block(index, t) if src is None else src, block(index, t),
            half_s.at[k, c - 1], half_r.at[k, c - 1], (o, i, other),
        )

    for k in range(1, inner):
        for j in range(count):
            start(a2a(k, j))
        start(ext(k))
    for j in range(count):
        staged[j].wait()
    for way in range(2):
        start(ring(way, 1, 0, stage_w))
    for k in range(1, inner):
        start(tok(k))
    for c in range(1, tp):
        start(hand(0, c, tokens))
    staged[count].wait()
    staged[count + 1].wait()
    start_own = [
        pltpu.make_async_copy(stage_w, piece(o, i), local.at[0]),
        pltpu.make_async_copy(stage_t, block(i, t), local.at[1]),
        pltpu.make_async_copy(stage_e, extras.at[i], local.at[2]),
    ]
    for copy in start_own:
        copy.start()

    def relay(distance, k):
        for way in range(2):
            if uses(way, distance, k):
                ring(way, distance, k).wait_recv()
                if distance < far and uses(way, distance + 1, k):
                    start(ring(way, distance + 1, k))

    for k in range(1, inner):
        for j in range(count):
            a2a(k, j).wait_recv()
        for way in range(2):
            start(ring(way, 1, k))
        relay(1, k - 1)
    relay(1, inner - 1)
    for k in range(1, inner):
        tok(k).wait_recv()
        for c in range(1, tp):
            start(hand(k, c))
    for distance in range(2, far + 1):
        for k in range(inner):
            relay(distance, k)
    for k in range(1, inner):
        ext(k).wait_recv()
    for k in range(inner):
        for c in range(1, tp):
            hand(k, c).wait_recv()
    for copy in start_own:
        copy.wait()
    for copy in sends:
        copy.wait_send()


def exchange(tokens, weights, extra, outer, inner, tp):
    rows, half = tokens.shape
    depth, columns = weights[0].shape
    width = columns // inner
    count = len(weights)
    turned = extra.T
    dma = pltpu.SemaphoreType.DMA
    far = outer // 2
    any_space = pl.BlockSpec(memory_space=pl.ANY)
    whole, extras, pieces = pl.pallas_call(
        functools.partial(exchange_kernel, outer, inner, tp, count),
        out_shape=(
            jax.ShapeDtypeStruct((inner * rows, tp * half), tokens.dtype),
            jax.ShapeDtypeStruct((inner,) + turned.shape, turned.dtype),
            jax.ShapeDtypeStruct((count, outer * inner * depth, width), weights[0].dtype),
        ),
        in_specs=[any_space] * (2 + count),
        out_specs=(any_space,) * 3,
        scratch_shapes=[
            pltpu.VMEM((count, depth, width), weights[0].dtype),
            pltpu.VMEM((rows, half), tokens.dtype),
            pltpu.VMEM(turned.shape, turned.dtype),
            dma((count + 2,)),
            dma((inner - 1, count)), dma((inner - 1, count)),
            dma((inner - 1,)), dma((inner - 1,)),
            dma((inner - 1,)), dma((inner - 1,)),
            dma((inner, tp - 1)), dma((inner, tp - 1)),
            dma((2, far, inner)), dma((2, far, inner)),
        ],
        compiler_params=pltpu.CompilerParams(collective_id=0, has_side_effects=True),
    )(tokens, turned, *weights)
    extras = jnp.transpose(extras, (1, 0, 2)).reshape(turned.shape[0], inner * rows)
    return whole, pieces, extras


def gather_inputs(tokens, weights, extra, inner):
    rows, half = tokens.shape
    gathered = lax.all_gather(tokens, ("inner", "tp"), axis=0)
    tp = gathered.shape[0] // inner
    whole = jnp.transpose(gathered.reshape(inner, tp, rows, half), (0, 2, 1, 3))
    whole = whole.reshape(inner * rows, tp * half)
    depth, columns = weights[0].shape
    width = columns // inner
    packed = jnp.stack([w.reshape(depth, inner, width) for w in weights], axis=2)
    packed = jnp.transpose(packed, (1, 0, 2, 3)).reshape(inner, depth, len(weights) * width)
    if inner > 1:
        packed = lax.all_to_all(packed, "inner", split_axis=0, concat_axis=0, tiled=True)
    pieces = lax.all_gather(packed.reshape(inner * depth, -1), "outer", axis=0, tiled=True)
    pieces = pieces.reshape(-1, len(weights), width).transpose(1, 0, 2)
    extras = lax.all_gather(extra, "inner", axis=0, tiled=True) if inner > 1 else extra
    return whole, pieces, extras.T


def local_state(keys, values, shifted, level, total, scale):
    weight = jnp.exp(shifted - level[:, None]) * scale
    weighted = keys.astype(jnp.float32) * weight[:, :, None]
    mat = jnp.einsum(
        "hsd,hse->hde", weighted.astype(jnp.bfloat16), values, preferred_element_type=jnp.float32
    )
    return mat, jnp.sum(weighted, axis=1), level + total, total


def packed_state(mat, vec, level, decay):
    spread = lambda x: jnp.broadcast_to(x[:, None], vec.shape)
    rows = parts_of(vec) + parts_of(spread(level)) + parts_of(spread(decay))
    pad = [jnp.zeros_like(rows[0])] * 7
    return jnp.concatenate([mat.astype(jnp.bfloat16), jnp.stack(rows + pad, axis=1)], axis=1)


def incoming(states, reverse):
    count = states.shape[0]
    mats = states[:, :, :HEAD]
    rows = states[:, :, HEAD:]
    vecs = whole_of(rows[:, :, 0], rows[:, :, 1], rows[:, :, 2])
    levels = whole_of(rows[:, :, 3, 0], rows[:, :, 4, 0], rows[:, :, 5, 0])
    decays = whole_of(rows[:, :, 6, 0], rows[:, :, 7, 0], rows[:, :, 8, 0])
    place = lax.axis_index("outer")
    order = jnp.arange(count)
    if reverse:
        ahead = (order > place)[:, None]
        between = (order[None, :] < order[:, None]) & (order[None, :] > place)
    else:
        ahead = (order < place)[:, None]
        between = (order[None, :] > order[:, None]) & (order[None, :] < place)
    lost = jnp.sum(jnp.where(between[:, :, None], decays[None], 0.0), axis=1)
    reach = jnp.where(ahead, levels + lost, -1e30)
    level = jnp.max(reach, axis=0)
    share = jnp.where(ahead, jnp.exp(reach - level[None]), 0.0)
    mat = jnp.sum(share[:, :, None, None] * mats.astype(jnp.float32), axis=0)
    vec = jnp.sum(share[:, :, None] * vecs, axis=0)
    return mat, vec, level


def finish(query_wide, num, den, running, decay, state):
    mat, vec, level = state
    top = jnp.maximum(running, level[:, None])
    local_weight = jnp.exp(running - top)
    carry_weight = jnp.exp(level[:, None] - top)
    num = local_weight[:, :, None] * num + carry_weight[:, :, None] * jnp.einsum(
        "htd,hde->hte", query_wide, mat, precision=PRECISE
    )
    den = local_weight * den + carry_weight * jnp.einsum(
        "htd,hd->ht", query_wide, vec, precision=PRECISE
    )
    return num / jnp.maximum(jnp.abs(den), jnp.exp(-top - decay))[:, :, None]


def make_shards(inner, outer, tp):
    def own(array, dim):
        size = array.shape[dim] // inner
        return lax.dynamic_slice_in_dim(array, lax.axis_index("inner") * size, size, dim)

    def shards(
        tokens,
        norm_gain,
        glu_value,
        glu_gate,
        conv_taps,
        ln_gain,
        ln_bias,
        query_weight,
        key_weight,
        value_weight,
        gate_weight,
        gate_bias,
        log_decay_extra,
        mem_gain,
        out_conv,
        out_mem,
    ):
        taps, gain, bias, mgain = own(conv_taps, 1), own(ln_gain, 0), own(ln_bias, 0), own(mem_gain, 0)
        channels = conv_taps.shape[1] * tp
        width = gain.shape[0]
        heads = mgain.shape[0] // HEAD
        first = (lax.axis_index("tp") * inner + lax.axis_index("inner")) * heads
        stacked = (query_weight, key_weight, value_weight, glu_value, glu_gate)
        if inner > 1 and tp > 1 and outer > 2:
            whole, weights, extras = exchange(tokens, stacked, log_decay_extra, outer, inner, tp)
        else:
            whole, weights, extras = gather_inputs(tokens, stacked, log_decay_extra, inner)
        rows = whole.shape[0]
        wide = whole.astype(jnp.float32)
        normed = (
            wide * lax.rsqrt(jnp.mean(wide * wide, axis=-1, keepdims=True) + EPS) * norm_gain
        ).astype(jnp.bfloat16)
        own_gate = lax.dynamic_slice_in_dim(
            gate_weight.reshape(-1, 4, MEMORY_HEADS), first, heads, 2
        )
        own_bias = lax.dynamic_slice_in_dim(gate_bias.reshape(4, MEMORY_HEADS), first, heads, 1)
        gates = lax.dot_general(
            own_gate.reshape(-1, 4 * heads), normed, (((0,), (1,)), ((), ())),
            preferred_element_type=jnp.float32,
        ).reshape(4, heads, rows) + own_bias[:, :, None]
        own_extra = lax.dynamic_slice_in_dim(
            extras.reshape(2, MEMORY_HEADS, rows), first, heads, 1
        )
        lf = jax.nn.log_sigmoid(gates[1::2]) + own_extra
        at = jnp.arange(rows)
        causal = at[:, None] >= at[None, :]
        anti = at[:, None] <= at[None, :]

        def total(x, mask):
            return jnp.sum(jnp.where(mask, x[:, None, :], 0.0), axis=-1)

        def highest(x, mask):
            return jnp.max(jnp.where(mask, x[:, None, :], -jnp.inf), axis=-1)

        decay_f = total(lf[0], causal)
        decay_b = total(lf[1], anti)
        shifted_f = gates[0] - decay_f
        shifted_b = gates[2] - decay_b
        running_f = highest(shifted_f, causal)
        running_b = highest(shifted_b, anti)

        def project(i):
            return jnp.dot(normed, weights[i], preferred_element_type=jnp.float32)

        def heads_first(x):
            return jnp.transpose(x.reshape(rows, heads, HEAD), (1, 0, 2)).astype(jnp.bfloat16)

        keys = heads_first(project(1))
        values = heads_first(project(2))
        scale = HEAD ** (-0.5)
        state_f = local_state(
            keys, values, shifted_f, running_f[:, -1], decay_f[:, -1], scale
        )
        state_b = local_state(keys, values, shifted_b, running_b[:, 0], decay_b[:, 0], scale)
        sent = jnp.stack([packed_state(*state_f), packed_state(*state_b)])
        states = lax.all_gather(sent, "outer", axis=0)

        glu = (project(3) * jax.nn.sigmoid(project(4))).astype(jnp.bfloat16)
        reach = KW // 2
        before = lax.ppermute(glu[rows - reach :], "outer", [(i, i + 1) for i in range(outer - 1)])
        after = lax.ppermute(glu[:reach], "outer", [(i + 1, i) for i in range(outer - 1)])
        queries = heads_first(project(0))

        scores = jnp.einsum("htd,hsd->hts", queries, keys, preferred_element_type=jnp.float32) * scale

        def local_out(shifted, running, mask):
            weight = jnp.where(
                mask, jnp.exp(jnp.minimum(shifted[:, None, :] - running[:, :, None], 0.0)), 0.0
            )
            part = scores * weight
            num = jnp.einsum(
                "hts,hse->hte", part.astype(jnp.bfloat16), values,
                preferred_element_type=jnp.float32,
            )
            return num, jnp.sum(part, axis=-1)

        num_f, den_f = local_out(shifted_f, running_f, causal)
        num_b, den_b = local_out(shifted_b, running_b, anti)

        padded = jnp.concatenate([before, glu, after], axis=0).astype(jnp.float32)
        conv = jnp.zeros(glu.shape, jnp.float32)
        for offset in range(KW):
            conv = conv + taps[offset] * padded[offset : offset + rows]
        sums = jnp.stack([jnp.sum(conv, axis=-1), jnp.sum(conv * conv, axis=-1)])
        sums = lax.psum(sums, ("inner", "tp")) / channels
        chan_mean = sums[0]
        chan_var = sums[1] - chan_mean * chan_mean
        normal = (conv - chan_mean[:, None]) * lax.rsqrt(chan_var + EPS)[:, None] * gain + bias
        act = (normal * jax.nn.sigmoid(normal)).astype(jnp.bfloat16)

        query_wide = queries.astype(jnp.float32)
        forward = finish(query_wide, num_f, den_f, running_f, decay_f, incoming(states[:, 0], False))
        backward = finish(query_wide, num_b, den_b, running_b, decay_b, incoming(states[:, 1], True))
        summed = forward + backward
        head_norm = summed * lax.rsqrt(jnp.mean(summed * summed, axis=-1, keepdims=True) + EPS)
        head_norm = head_norm * mgain.reshape(heads, HEAD)[:, None, :]
        memory = jnp.transpose(head_norm, (1, 0, 2)).reshape(rows, heads * HEAD).astype(jnp.bfloat16)

        def back(x):
            if inner == 1:
                return x
            return lax.all_to_all(x, "inner", split_axis=0, concat_axis=1, tiled=True)

        result = jnp.dot(back(act), out_conv, preferred_element_type=jnp.float32)
        result = result + jnp.dot(back(memory), out_mem, preferred_element_type=jnp.float32)
        return lax.psum_scatter(
            result.astype(jnp.bfloat16), "tp", scatter_dimension=0, tiled=True
        )

    return shards


def solution(mesh):
    sp, tp = mesh.shape["sp"], mesh.shape["tp"]
    inner = math.gcd(sp, max(MEMORY_HEADS // tp, 1))
    outer = sp // inner
    fine = Mesh(mesh.devices.reshape(outer, inner, tp), ("outer", "inner", "tp"))
    rows = ("outer", "inner")
    in_specs = (
        P(rows, "tp"),
        P(),
        P(rows, "tp"),
        P(rows, "tp"),
        P(None, "tp"),
        P("tp"),
        P("tp"),
        P(rows, "tp"),
        P(rows, "tp"),
        P(rows, "tp"),
        P(),
        P(),
        P(rows, None),
        P("tp"),
        P("tp", None),
        P("tp", None),
    )
    return jax.shard_map(
        make_shards(inner, outer, tp), mesh=fine, in_specs=in_specs,
        out_specs=P(("outer", "inner", "tp"), None), check_vma=False,
    )
```

profile of v0, /device:TPU:0, one launch (start us, length us, event | category | flops | bytes accessed | tf_op | source)
XLA Modules:
  0.0 237.7 jit_solution(13314778436845445361)
XLA Ops:
  6.5 92.1 %shard_map.154 = (bf16[1024,2048]{1,0:T(8,128)(2,1)}, f32[4,16,256]{2,1,0:T(8,128)}, bf16[5,2048,256]{2,1,0:T(8,128)(2,1)}) custom-call(bf16[256,1024]{1,0:T(8,128)(2,1)} %refs_0_.1, f32[16,256]{1,0:T(8,128)} %bitcast.162, bf16[128,1024]{1,0:T(8,128)(2,1)} %refs_2_.1, bf16[128,1024]{1,0:T(8,128)(2,1)} %refs_3_.1, bf16[128,1024]{1,0:T(8,128)(2,1)} %refs_4_.1, ...), custom_call_target="tpu_custom_call" | custom-call | tf_op jit(solution)/shard_map/pallas_call | solution.py:191
  98.7 3.2 %fusion = f32[1024]{0:T(1024)S(1)} fusion(bf16[1024,2048]{1,0:T(8,128)(2,1)} %get-tuple-element.8), kind=kLoop, calls=%fused_computation.2 | loop fusion | flops 6290432 | bytes 4198400 | tf_op jit(solution)/shard_map/reduce_sum | solution.py:325
  101.9 0.2 copy-done.2
  102.1 1.0 fusion.2
  103.2 2.7 %copy-done.6 = bf16[5,2048,256]{2,1,0:T(8,128)(2,1)S(1)} copy-done((bf16[5,2048,256]{2,1,0:T(8,128)(2,1)S(1)}, bf16[5,2048,256]{2,1,0:T(8,128)(2,1)}, u32[]{:S(2)}) %copy-start.6) | copy-done | bytes 5242904
  105.8 1.3 fusion.25
  107.1 1.3 fusion.26
  108.4 3.5 %collective-permute-start = (bf16[15,256]{1,0:T(8,128)(2,1)S(1)}, bf16[15,256]{1,0:T(8,128)(2,1)S(1)}, u32[]{:S(2)}, u32[]{:S(2)}) collective-permute-start(bf16[15,256]{1,0:T(8,128)(2,1)S(1)} %get-tuple-element.27), channel_id=1, source_target_pairs={{0,8},{8,16},{16,24},{1,9},{9,17},{17,25},{2,10},{10,18},{18,26},{... | collective-permute-start | bytes 23048 | tf_op jit(solution)/shard_map/ppermute | solution.py:374
  111.9 1.5 collective-permute-start.1
  113.4 1.2 convolution_convert_fusion.1
  114.8 0.2 dynamic-slice_reduce_fusion
  115.0 3.4 %convolution_add_fusion.1 = f32[4,1024]{1,0:T(4,128)S(1)} fusion(bf16[1024,2048]{1,0:T(8,128)(2,1)} %copy-done.1, bf16[2048,4,1]{0,2,1:T(2,128)(2,1)S(1)} %constant_dynamic-slice_fusion.2, f32[4]{0:T(128)S(1)} %dynamic-slice_reduce_fusion), kind=kOutput, calls=%fused_computation.51 | convolution fusion | flops 16781312 | bytes 4227088 | tf_op jit(solution)/shard_map/dot_general | solution.py:331
  118.6 0.2 select_reduce_fusion.1
  118.8 0.2 select_reduce_fusion
  119.1 0.5 slice.474
  119.6 0.6 slice.475
  130.0 0.2 select_reduce_fusion.3
  130.2 0.2 select_reduce_fusion.2
  130.4 0.6 slice.470
  131.0 1.2 exponential_multiply_fusion
  132.2 3.8 %fusion.27 = (f32[256]{0:T(256)S(1)}, f32[256]{0:T(256)S(1)}, bf16[1024,256]{1,0:T(8,128)(2,1)S(1)}) fusion(f32[1024]{0:T(1024)S(1)} %get-tuple-element.82, f32[1024]{0:T(1024)S(1)} %get-tuple-element.81, bf16[1024,2048]{1,0:T(8,128)(2,1)} %copy-done.1, bf16[5,2048,256]{2,1,0:T(8,128)(2,1)} %get-tuple-element.9), kind=kOutput, calls=%fused_computation.43 | convolution fusion | flops 1075314176 | bytes 5777408 | tf_op jit(solution)/shard_map/dot_general | solution.py:357
  136.0 0.5 fusion.32
  136.5 0.5 fusion.31
  137.1 0.6 slice.471
  147.9 0.7 pad_maximum_fusion
  148.6 3.7 %convolution_convert_fusion = bf16[1024,256]{1,0:T(8,128)(2,1)S(1)} fusion(bf16[1024,2048]{1,0:T(8,128)(2,1)} %copy-done.1, bf16[5,2048,256]{2,1,0:T(8,128)(2,1)} %get-tuple-element.9), kind=kOutput, calls=%fused_computation.40 | convolution fusion | flops 1074003968 | bytes 5767168 | tf_op jit(solution)/shard_map/dot_general | solution.py:357
  152.4 4.4 %fusion.6 = (f32[1024]{0:T(1024)S(1)}, f32[1024]{0:T(1024)S(1)}, f32[1024,1024]{0,1:T(8,128)}) fusion(f32[1024]{0:T(1024)S(1)} %select_reduce_fusion, f32[1024]{0:T(1024)S(1)} %sub.293, f32[1024]{0:T(1024)S(1)} %select_reduce_fusion.2, f32[1024]{0:T(1024)S(1)} %sub.283, bf16[1024,256]{1,0:T(8,128)(2,1)S(1)} %convolution_convert_fusion, ...), kind=kOutput, calls=%fused_computation.19 | convolution fusion | flops 550500352 | bytes 5267456 | tf_op jit(solution)/shard_map/htd,hsd->hts/dot_general | solution.py:378
  156.8 1.2 fusion.132
  158.0 1.3 constant_dynamic-slice_fusion
  159.3 0.8 dynamic_slice.23
  160.1 0.8 dynamic_slice.22
  160.9 0.8 dynamic_slice.27
  161.6 0.9 concatenate.9
  162.6 4.5 %fusion.125 = (f32[1024]{0:T(1024)S(1)}, f32[1024]{0:T(1024)S(1)}, f32[1024,256]{1,0:T(8,128)S(1)}) fusion(f32[1054,256]{1,0:T(8,128)S(1)} %convert_element_type.466, f32[256]{0:T(256)S(1)} %bitcast.186, f32[256]{0:T(256)S(1)} %bitcast.188, f32[256]{0:T(256)S(1)} %bitcast.189, f32[256]{0:T(256)S(1)} %bitcast.190, f32[256]{0:T(256)S(1)} %bitcast.191, ...), kind=kLoop, calls=%fused_computation.241 | loop fusion | flops 16775168 | bytes 33594368 | tf_op jit(solution)/shard_map/reduce_sum | solution.py:398
  167.2 13.4 %psum.7 = f32[2,1024]{1,0:T(2,128)S(1)} all-reduce(f32[2,1024]{1,0:T(2,128)S(1)} %pad_maximum_fusion.1), channel_id=1, replica_groups=mesh['outer'=4,'inner'=4,'tp'=2] {'inner','tp'}, use_global_device_ids=true, to_apply=%region_3.4 | all-reduce | flops 2048 | bytes 16384 | tf_op jit(solution)/shard_map/psum | solution.py:399
  180.6 0.4 multiply_convert_fusion.1
  181.1 1.0 copy.47
  182.1 3.7 %all-to-all-start = ((bf16[4,256,256]{1,2,0:T(8,128)(2,1)}), bf16[4,256,256]{1,2,0:T(8,128)(2,1)S(1)}, u32[]{:S(2)}, u32[]{:S(2)}) async-start(bf16[4,256,256]{1,2,0:T(8,128)(2,1)} %copy.47), calls=%async_computation | async-start | bytes 1048576 | tf_op jit(solution)/shard_map/all_to_all | solution.py:416
  185.8 1.3 slice_bitcast_fusion
  187.1 0.1 fusion.128
  187.3 0.6 fusion.123
  187.9 0.6 exponential_select_fusion.1
  188.7 0.5 fusion.137
  189.3 0.8 fusion.113
  190.0 0.2 multiply_reduce_fusion.2
  190.2 0.1 fusion.126
  190.4 0.6 fusion.124
  191.1 0.6 exponential_select_fusion
  191.8 0.5 fusion.138
  192.3 0.6 fusion.80
  193.0 4.4 %fusion.18 = f32[1024,256]{1,0:T(8,128)} fusion(bf16[1024,256]{1,0:T(8,128)(2,1)S(1)} %convolution_convert_fusion.1, f32[1024,1024]{0,1:T(8,128)} %get-tuple-element.78, f32[1024]{0:T(1024)S(1)} %select_reduce_fusion.2, f32[1024]{0:T(1024)S(1)} %sub.283, f32[1024]{0:T(1024)S(1)} %get-tuple-element.70), kind=kOutput, calls=%fused_computation.33 | convolution fusion | flops 544473088 | bytes 5779456 | tf_op jit(solution)/shard_map/hts,hse->hte/dot_general | solution.py:385
  197.4 0.6 fusion.85
  198.1 2.2 fusion.21
  200.4 0.8 fusion.114
  201.2 0.2 multiply_reduce_fusion.1
  201.4 1.8 fusion.16
  203.2 1.2 multiply_reduce_fusion
  204.5 0.2 multiply_convert_fusion
  204.7 1.0 copy.54
  205.7 3.9 %all-to-all-start.1 = ((bf16[4,256,256]{1,2,0:T(8,128)(2,1)}), bf16[4,256,256]{1,2,0:T(8,128)(2,1)S(1)}, u32[]{:S(2)}, u32[]{:S(2)}) async-start(bf16[4,256,256]{1,2,0:T(8,128)(2,1)} %copy.54), calls=%async_computation.1 | async-start | bytes 1048576 | tf_op jit(solution)/shard_map/all_to_all | solution.py:416
  209.6 3.5 %fusion.136 = f32[256,2048]{1,0:T(8,128)S(1)} fusion(bf16[256,1024]{0,1:T(8,128)(2,1)S(1)} %bitcast.156, bf16[1024,2048]{1,0:T(8,128)(2,1)} %param.30), kind=kOutput, calls=%fused_computation.249 | convolution fusion | flops 1073741824 | bytes 6815744 | tf_op jit(solution)/shard_map/dot_general | solution.py:418
  213.1 3.4 %all-to-all-done.1 = bf16[4,256,256]{1,2,0:T(8,128)(2,1)S(1)} async-done(((bf16[4,256,256]{1,2,0:T(8,128)(2,1)}), bf16[4,256,256]{1,2,0:T(8,128)(2,1)S(1)}, u32[]{:S(2)}, u32[]{:S(2)}) %all-to-all-start.1) | async-done | bytes 524320 | tf_op jit(solution)/shard_map/all_to_all | solution.py:416
  216.5 4.5 %fusion.3 = bf16[256,2048]{1,0:T(8,128)(2,1)} fusion(f32[256,2048]{1,0:T(8,128)S(1)} %fusion.136, bf16[256,1024]{0,1:T(8,128)(2,1)S(1)} %bitcast.157, bf16[1024,2048]{1,0:T(8,128)(2,1)} %param.31), kind=kOutput, calls=%fused_computation.16 | convolution fusion | flops 1074790400 | bytes 7864320 | tf_op jit(solution)/shard_map/dot_general | solution.py:419
  221.0 9.8 %reduce-scatter.2.cloned.1.call-done = bf16[128,2048]{1,0:T(8,128)(2,1)} async-done(((bf16[256,2048]{1,0:T(8,128)(2,1)}), bf16[128,2048]{1,0:T(8,128)(2,1)}) %reduce-scatter.2.cloned.1.call-update) | async-done | bytes 524304 | tf_op jit(solution)/shard_map/reduce_scatter | solution.py:420
  (69 shorter events, 1.4 us)
Async XLA Ops:
  6.5 108.2 %copy-start = (bf16[2048,32]{0,1:T(8,128)(2,1)S(1)}, bf16[2048,32]{0,1:T(8,128)(2,1)}, u32[]{:S(2)}) copy-start(bf16[2048,32]{0,1:T(8,128)(2,1)} %param.26) | copy-start | bytes 393220
  6.5 95.4 %copy-start.4 = (f32[2048]{0:T(1024)S(1)}, f32[2048]{0:T(1024)}, u32[]{:S(2)}) copy-start(f32[2048]{0:T(1024)} %param.17) | copy-start | bytes 24580
  6.5 179.2 %all-gather.3.cloned.1.call-start = ((), (), s32[]{:S(2)}) async-start(), calls=%async_computation.4 | async-start | bytes 1392640 | tf_op jit(solution)/shard_map/all_gather | solution.py:370
  98.7 3.5 %copy-start.2 = (bf16[1024,2048]{1,0:T(8,128)(2,1)S(1)}, bf16[1024,2048]{1,0:T(8,128)(2,1)}, u32[]{:S(2)}) copy-start(bf16[1024,2048]{1,0:T(8,128)(2,1)} %get-tuple-element.8) | copy-start | bytes 12582916
  102.1 3.7 %copy-start.6 = (bf16[5,2048,256]{2,1,0:T(8,128)(2,1)S(1)}, bf16[5,2048,256]{2,1,0:T(8,128)(2,1)}, u32[]{:S(2)}) copy-start(bf16[5,2048,256]{2,1,0:T(8,128)(2,1)} %get-tuple-element.9) | copy-start | bytes 15728644
  103.1 10.2 %copy-start.1 = (bf16[1024,2048]{1,0:T(8,128)(2,1)}, bf16[1024,2048]{1,0:T(8,128)(2,1)S(1)}, u32[]{:S(2)}) copy-start(bf16[1024,2048]{1,0:T(8,128)(2,1)S(1)} %fusion.2) | copy-start | bytes 12582916
  108.4 6.3 %copy-start.5 = (f32[32]{0:T(128)S(1)}, f32[32]{0:T(128)}, u32[]{:S(2)}) copy-start(f32[32]{0:T(128)} %param.27) | copy-start | bytes 388
  108.4 53.2 %collective-permute-start = (bf16[15,256]{1,0:T(8,128)(2,1)S(1)}, bf16[15,256]{1,0:T(8,128)(2,1)S(1)}, u32[]{:S(2)}, u32[]{:S(2)}) collective-permute-start(bf16[15,256]{1,0:T(8,128)(2,1)S(1)} %get-tuple-element.27), channel_id=1, source_target_pairs={{0,8},{8,16},{16,24},{1,9},{9,17},{17,25},{2,10},{10,18},{18,26},{... | collective-permute-start | bytes 23048 | tf_op jit(solution)/shard_map/ppermute | solution.py:374
  111.9 49.7 %collective-permute-start.1 = (bf16[15,256]{1,0:T(8,128)(2,1)S(1)}, bf16[15,256]{1,0:T(8,128)(2,1)S(1)}, u32[]{:S(2)}, u32[]{:S(2)}) collective-permute-start(bf16[15,256]{1,0:T(8,128)(2,1)S(1)} %get-tuple-element.26), channel_id=1, source_target_pairs={{8,0},{16,8},{24,16},{9,1},{17,9},{25,17},{10,2},{18,10},{26,18},{... | collective-permute-start | bytes 23048 | tf_op jit(solution)/shard_map/ppermute | solution.py:375
  113.4 5.0 %copy-start.3 = (f32[4,16,256]{2,1,0:T(8,128)S(1)}, f32[4,16,256]{2,1,0:T(8,128)}, u32[]{:S(2)}) copy-start(f32[4,16,256]{2,1,0:T(8,128)} %get-tuple-element.10) | copy-start | bytes 196612
  182.1 23.7 %all-to-all-start = ((bf16[4,256,256]{1,2,0:T(8,128)(2,1)}), bf16[4,256,256]{1,2,0:T(8,128)(2,1)S(1)}, u32[]{:S(2)}, u32[]{:S(2)}) async-start(bf16[4,256,256]{1,2,0:T(8,128)(2,1)} %copy.47), calls=%async_computation | async-start | bytes 1048576 | tf_op jit(solution)/shard_map/all_to_all | solution.py:416
  193.0 5.1 %copy-start.8 = (f32[1024,1024]{0,1:T(8,128)S(1)}, f32[1024,1024]{0,1:T(8,128)}, u32[]{:S(2)}) copy-start(f32[1024,1024]{0,1:T(8,128)} %get-tuple-element.78) | copy-start | bytes 12582916
  200.3 3.0 %copy-start.7 = (f32[1024,256]{1,0:T(8,128)S(1)}, f32[1024,256]{1,0:T(8,128)}, u32[]{:S(2)}) copy-start(f32[1024,256]{1,0:T(8,128)} %fusion.21) | copy-start | bytes 3145732
  205.7 10.8 %all-to-all-start.1 = ((bf16[4,256,256]{1,2,0:T(8,128)(2,1)}), bf16[4,256,256]{1,2,0:T(8,128)(2,1)S(1)}, u32[]{:S(2)}, u32[]{:S(2)}) async-start(bf16[4,256,256]{1,2,0:T(8,128)(2,1)} %copy.54), calls=%async_computation.1 | async-start | bytes 1048576 | tf_op jit(solution)/shard_map/all_to_all | solution.py:416
  209.6 21.2 %reduce-scatter.2.cloned.1.call-start = ((), (), s32[]{:S(2)}) async-start(), calls=%async_computation.3 | async-start | bytes 1572864 | tf_op jit(solution)/shard_map/reduce_scatter | solution.py:420
Sparse Core Ops, SparseCore 0:
  148.8 31.3 all-gather.2
  221.1 9.6 reduce-scatter.1
where the time goes:
time: 239 us; the launch traced here: 238 us
  Pallas kernels  92.1 us (39%)
  matrix products  38.8 us (16%)
  between operations  33.7 us (14%)
  other arithmetic  18.8 us (8%)
  local copies, waits for them, and re-layouts  15.1 us (6%)
  blocking collectives  13.4 us (6%)
  waiting for transfers between devices  13.3 us (6%)
  starting transfers between devices  12.6 us (5%)
    pallas_call x1, Pallas kernels, exchange(): pl.pallas_call(functools.partial(exchange_kernel, outer, inner, tp, count...  92.1 us
    psum x1, blocking collectives, shards(): sums = lax.psum(sums, ('inner', 'tp')) / channels  13.4 us
    dot_general x5, matrix products, project(): return jnp.dot(normed, weights[i], preferred_element_type=jnp.float32)  11.3 us
    reduce_scatter x1, waiting for transfers between devices, shards(): lax.psum_scatter(result.astype(jnp.bfloat16), 'tp', scatter_dimension=0,...  9.81 us
    all_to_all x2, starting transfers between devices, back(): return lax.all_to_all(x, 'inner', split_axis=0, concat_axis=1, tiled=True)  7.6 us
    dot_general x2, matrix products, local_out(): jnp.einsum('hts,hse->hte', part.astype(jnp.bfloat16), values, preferred_e...  6.64 us
  transfers between devices with their start and end apart: 6, of which 2 were waited for; matrix products, arithmetic and copies ran while one was open for 25% of the time, Pallas kernels for 0%

commit v1 on v0

--- a/solution.py
+++ b/solution.py
@@ -1,5 +1,6 @@
 import functools
 import math
+import types
 
 import jax
 import jax.numpy as jnp
@@ -31,37 +32,36 @@
 MESH = pl.DeviceIdType.MESH
 
 
-def exchange_kernel(outer, inner, tp, count, *refs):
-    tokens, extra = refs[:2]
-    weights = refs[2 : 2 + count]
-    whole, extras, pieces, stage_w, stage_t, stage_e = refs[2 + count : 8 + count]
-    local, a2a_s, a2a_r, tok_s, tok_r, ext_s, ext_r, half_s, half_r, ring_s, ring_r = refs[8 + count :]
+def layer_kernel(outer, inner, tp, names, *refs):
+    r = types.SimpleNamespace(**dict(zip(names, refs)))
+    tokens, norm_gain = r.tokens, r.norm_gain
+    weights = [r.glu_value, r.glu_gate, r.key_weight, r.value_weight, r.query_weight]
+    count = len(weights)
     o, i, t = lax.axis_index("outer"), lax.axis_index("inner"), lax.axis_index("tp")
-    right, left = lax.rem(o + 1, outer), lax.rem(o + outer - 1, outer)
-    rows, half = tokens.shape
+    block, half = tokens.shape
     depth = weights[0].shape[0]
-    width = pieces.shape[2]
-
-    barrier = pltpu.get_barrier_semaphore()
-    greeted = [(o, lax.rem(i + k, inner), t) for k in range(1, inner)]
-    greeted += [(o, i, lax.rem(t + k, tp)) for k in range(1, tp)]
-    greeted += [(right, i, t), (left, i, t)]
-    for device in greeted:
-        pl.semaphore_signal(barrier, inc=1, device_id=device, device_id_type=MESH)
-    pl.semaphore_wait(barrier, len(greeted))
-
-    def columns(index):
-        return pl.ds(pl.multiple_of(index * width, width), width)
-
-    def piece(owner, index):
-        start = pl.multiple_of((owner * inner + index) * depth, depth)
-        return pieces.at[:, pl.ds(start, depth), :]
-
-    def block(index, core):
-        return whole.at[
-            pl.ds(pl.multiple_of(index * rows, rows), rows),
-            pl.ds(pl.multiple_of(core * half, half), half),
-        ]
+    hb = block // tp
+    quarter = inner * block
+    groups = outer // tp
+    model = half * tp
+    channels = MEMORY_HEADS * HEAD
+    scale = HEAD ** (-0.5)
+    f32, bf16 = jnp.float32, jnp.bfloat16
+
+    par, grp = lax.rem(o, tp), lax.div(o, tp)
+    mate = 1 - t
+    twin = o + 1 - 2 * par
+    primary = t == par
+    place = grp * tp + t
+    last = outer - 1
+    x, y = lax.rem(i, 2), lax.div(i, 2)
+    near = [i, y * 2 + 1 - x, (1 - y) * 2 + x, (1 - y) * 2 + 1 - x]
+    head = par * inner + i
+
+    nq, nsrc, xin, wst, wfull, ow = r.nq, r.nsrc, r.xin, r.wst, r.wfull, r.ow
+
+    def span(index, size):
+        return pl.ds(pl.multiple_of(index * size, size), size)
 
     def remote(src, dst, send, recv, device):
         return pltpu.make_async_remote_copy(
@@ -71,147 +71,715 @@
 
     sends = []
 
-    def start(copy):
+    def start(copy, when=None):
+        if when is None:
+            copy.start()
+        else:
+            pl.when(when)(copy.start)
+        sends.append((copy, when))
+
+    def guarded(when, action):
+        pl.when(when)(action)
+
+    local = pltpu.make_async_copy
+
+    own_rows = [local(weights[j], wst.at[j, o], r.own_s.at[j]) for j in range(count)]
+    tok_own = local(tokens.at[span(t, hb), :], xin.at[t], r.loc_s.at[0])
+    tok_own.start()
+
+    @pl.when(primary)
+    def _():
+        for copy in own_rows:
+            copy.start()
+
+    gate_in = local(r.gate_weight, r.gwp.at[pl.ds(0, r.gate_weight.shape[0]), :], r.loc_s.at[1])
+    out_in = [
+        local(source, ow.at[k], r.loc_s.at[2 + k]) for k, source in enumerate((r.out_conv, r.out_mem))
+    ]
+
+    barrier = pltpu.get_barrier_semaphore()
+    greeted = []
+    for dz in range(tp):
+        for k in range(inner):
+            for c in range(tp):
+                if (dz, k, c) != (0, 0, 0):
+                    greeted.append((o if dz == 0 else twin, near[k], t if c == 0 else mate))
+    for step in range(1, groups):
+        away = lax.rem(grp + step, groups) * tp
+        for dz in range(tp):
+            for c in range(tp):
+                greeted.append((away + dz, i, c))
+    for device in greeted:
+        pl.semaphore_signal(barrier, inc=1, device_id=device, device_id_type=MESH)
+    pl.semaphore_wait(barrier, len(greeted))
+
+    start(remote(tokens.at[span(mate, hb), :], xin.at[t], r.xin_s, r.xin_r, (o, i, mate)))
+
+    def spread(j, step):
+        target = lax.rem(grp + step, groups) * tp + t
+        return remote(
+            weights[j], wst.at[j, o], r.w1_s.at[j, step], r.w1_r.at[j, o], (target, i, t)
+        )
+
+    def spread_all(j):
+        for step in range(groups):
+            start(spread(j, step), None if step else jnp.logical_not(primary))
+
+    def arrived(j, plane):
+        remote(wst.at[j, plane], wst.at[j, plane], r.w1_s.at[j, 0], r.w1_r.at[j, plane], (o, i, mate)).wait_recv()
+
+    small = ((r.conv_taps, r.taps), (r.ln_gain, r.lng), (r.ln_bias, r.lnb), (r.mem_gain, r.mgn))
+    own_small = [
+        local(a.at[:, span(i, HEAD)], b, r.sml_s.at[k]) for k, (a, b) in enumerate(small)
+    ]
+    mate_small = [
+        remote(a.at[:, span(i, HEAD)], b, r.prm_s.at[k], r.prm_r.at[k], (o, i, mate))
+        for k, (a, b) in enumerate(small)
+    ]
+    spread_all(0)
+
+    @pl.when(primary)
+    def _():
+        for copy in own_small:
+            copy.start()
+        for copy in mate_small:
+            copy.start()
+
+    ext = r.ext
+    plane = jnp.where(primary, o, twin)
+    own_ext = local(r.extra, ext.at[i], r.loc_s.at[4])
+    guarded(primary, own_ext.start)
+    for k in range(inner):
+        copy = remote(r.extra, ext.at[i], r.ext_s.at[k], r.ext_r.at[i], (plane, near[k], par))
+        start(copy, None if k else jnp.logical_not(primary))
+
+    gate_in.start()
+    for copy in out_in:
         copy.start()
-        sends.append(copy)
-
-    staged = [
-        pltpu.make_async_copy(weights[j].at[:, columns(i)], stage_w.at[j], local.at[j])
-        for j in range(count)
-    ]
-    staged.append(pltpu.make_async_copy(tokens, stage_t, local.at[count]))
-    staged.append(pltpu.make_async_copy(extra, stage_e, local.at[count + 1]))
-    for copy in staged:
-        copy.start()
-
-    def a2a(k, j):
-        peer = lax.rem(i + k, inner)
-        start_row = pl.multiple_of((o * inner + i) * depth, depth)
+
+    tok_own.wait()
+    remote(xin.at[mate], xin.at[mate], r.xin_s, r.xin_r, (o, i, mate)).wait_recv()
+    norm_rows = 32
+
+    def norm_step(m, carry):
+        at = span(m, norm_rows)
+        parts = [xin[f, at, :].astype(f32) for f in range(tp)]
+        square = sum(jnp.sum(p * p, axis=-1, keepdims=True) for p in parts)
+        level = lax.rsqrt(square * (1.0 / model) + EPS)
+        for f in range(tp):
+            row = (parts[f] * level * norm_gain[:, pl.ds(f * half, half)]).astype(bf16)
+            nsrc[at, pl.ds(f * half, half)] = row
+
+            @pl.when(primary)
+            def _():
+                nq[pl.ds(pl.multiple_of(i * block + t * hb + m * norm_rows, norm_rows), norm_rows), pl.ds(f * half, half)] = row
+        return carry
+
+    lax.fori_loop(0, hb // norm_rows, norm_step, 0)
+
+    def rows_of(b, c):
+        return nq.at[pl.ds(pl.multiple_of(b * block + c * hb, hb), hb), :]
+
+    def tok_wait(b, c):
+        remote(rows_of(b, c), rows_of(b, c), r.tok_s.at[0], r.tok_r.at[b, c], (o, i, mate)).wait_recv()
+
+    start(remote(nsrc, rows_of(i, t), r.tok_s.at[0], r.tok_r.at[i, t], (o, i, mate)), jnp.logical_not(primary))
+    start(remote(nsrc, rows_of(i, t), r.tok_s.at[1], r.tok_r.at[i, t], (twin, i, par)))
+
+    def row_block(owner_plane, owner):
+        return pl.ds(pl.multiple_of((owner_plane * inner + owner) * depth, depth), depth)
+
+    def deal(j, plane_at, k):
         return remote(
-            weights[j].at[:, columns(peer)], pieces.at[j, pl.ds(start_row, depth), :],
-            a2a_s.at[k - 1, j], a2a_r.at[k - 1, j], (o, peer, t),
-        )
-
-    def ring(way, distance, k, src=None):
-        index = lax.rem(i + inner - k, inner)
-        back = outer - (distance - 1) if way == 0 else distance - 1
-        owner = lax.rem(o + back, outer)
-        target = right if way == 0 else left
+            wst.at[j, plane_at, :, span(near[k], HEAD)],
+            wfull.at[j, row_block(plane_at, i), :],
+            r.w2_s.at[j, plane_at, k - 1], r.w2_r.at[j, plane_at, k - 1], (o, near[k], t),
+        )
+
+    def keep(j, plane_at):
+        return local(
+            wst.at[j, plane_at, :, span(i, HEAD)], wfull.at[j, row_block(plane_at, i), :],
+            r.keep_s.at[j, plane_at],
+        )
+
+    def plane_of(step):
+        return lax.rem(grp + step, groups) * tp
+
+    def deal_planes(j):
+        planes = [o, twin]
+        for step in range(1, groups):
+            planes += [plane_of(step), plane_of(step) + 1]
+        return planes
+
+    def deal_all(j, which=None):
+        @pl.when(primary)
+        def _():
+            for index, plane_at in enumerate(deal_planes(j)):
+                if which is not None and index not in which:
+                    continue
+                if index == 0:
+                    own_rows[j].wait()
+                else:
+                    arrived(j, plane_at)
+                for k in range(1, inner):
+                    deal(j, plane_at, k).start()
+                keep(j, plane_at).start()
+
+    def share(j, plane_at):
+        rows = pl.ds(pl.multiple_of(plane_at * inner * depth, inner * depth), inner * depth)
         return remote(
-            piece(owner, index) if src is None else src, piece(owner, index),
-            ring_s.at[way, distance - 1, k], ring_r.at[way, distance - 1, k], (target, i, t),
-        )
-
-    far = outer // 2
-
-    def uses(way, distance, k):
-        if 2 * distance < outer:
-            return True
-        return (k < inner // 2) == (way == 0)
-
-    def tok(k):
-        peer = lax.rem(i + k, inner)
-        return remote(tokens, block(i, t), tok_s.at[k - 1], tok_r.at[k - 1], (o, peer, t))
-
-    def ext(k):
-        peer = lax.rem(i + k, inner)
-        return remote(extra, extras.at[i], ext_s.at[k - 1], ext_r.at[k - 1], (o, peer, t))
-
-    def hand(k, c, src=None):
-        index = lax.rem(i + inner - k, inner)
-        other = lax.rem(t + c, tp)
+            wfull.at[j, rows, :], wfull.at[j, rows, :],
+            r.fw_s.at[j, plane_at], r.fw_r.at[j, plane_at], (o, i, mate),
+        )
+
+    def collect(j):
+        @pl.when(primary)
+        def _():
+            for plane_at in deal_planes(j):
+                keep(j, plane_at).wait()
+                for k in range(1, inner):
+                    rows = wfull.at[j, row_block(plane_at, near[k]), :]
+                    remote(rows, rows, r.w2_s.at[j, plane_at, k - 1], r.w2_r.at[j, plane_at, k - 1], (o, i, mate)).wait_recv()
+                share(j, plane_at).start()
+
+        @pl.when(jnp.logical_not(primary))
+        def _():
+            for plane_at in deal_planes(j):
+                share(j, plane_at).wait_recv()
+
+    deal_all(0, (0,))
+
+    def pass_on(b_from, c, k, slot):
         return remote(
-            block(index, t) if src is None else src, block(index, t),
-            half_s.at[k, c - 1], half_r.at[k, c - 1], (o, i, other),
-        )
-
-    for k in range(1, inner):
+            rows_of(b_from, c), rows_of(b_from, c), r.pas_s.at[slot], r.tok_r.at[b_from, c], (o, near[k], t)
+        )
+
+    def own_half(c):
+        @pl.when(jnp.logical_not(jnp.logical_and(primary, t == c)))
+        def _():
+            tok_wait(i, c)
+
+    first, second = t, mate
+    for index, c in enumerate((first, second)):
+        own_half(c)
+        start(pass_on(i, c, 1, 2 * index))
+        start(pass_on(i, c, 2, 2 * index + 1))
+    for j in range(1, count):
+        spread_all(j)
+    deal_all(0, range(1, outer))
+    tok_wait(near[1], 0)
+    start(pass_on(near[1], 0, 2, 4))
+    tok_wait(near[2], 1)
+    start(pass_on(near[2], 1, 1, 5))
+    deal_all(1)
+    tok_wait(near[1], 1)
+    tok_wait(near[2], 0)
+    tok_wait(near[3], 0)
+    tok_wait(near[3], 1)
+
+    gwp, gt, rowsv, colsv = r.gwp, r.gt, r.rowsv, r.colsv
+    gate_in.wait()
+
+    def chunk(n):
+        return span(n, block)
+
+    def gate_step(n, carry):
+        got = lax.dot_general(
+            nq[chunk(n), :], gwp[...], (((1,), (1,)), ((), ())), preferred_element_type=f32
+        )
+        gt[:, chunk(n)] = got.T[: gt.shape[0]]
+        return carry
+
+    lax.fori_loop(0, inner, gate_step, 0)
+    guarded(primary, own_ext.wait)
+    for k in range(inner):
+        def hear(k=k):
+            remote(r.extra, ext.at[near[k]], r.ext_s.at[0], r.ext_r.at[near[k]], (o, i, mate)).wait_recv()
+        if k:
+            hear()
+        else:
+            guarded(jnp.logical_not(primary), hear)
+
+    mine = lax.broadcasted_iota(jnp.int32, (MEMORY_HEADS, quarter), 0) == head
+    mine_block = lax.broadcasted_iota(jnp.int32, (MEMORY_HEADS, block), 0) == head
+
+    def gate_row(g):
+        rows = gt[pl.ds(g * MEMORY_HEADS, MEMORY_HEADS), :]
+        return jnp.sum(jnp.where(mine, rows, 0.0), axis=0, keepdims=True) + r.gate_bias[g * MEMORY_HEADS + head]
+
+    def extra_row(d):
+        pieces = [
+            jnp.sum(jnp.where(mine_block, ext[b, pl.ds(d * MEMORY_HEADS, MEMORY_HEADS), :], 0.0), axis=0, keepdims=True)
+            for b in range(inner)
+        ]
+        return jnp.concatenate(pieces, axis=1)
+
+    def log_sigmoid(v):
+        return jnp.minimum(v, 0.0) - jnp.log1p(jnp.exp(-jnp.abs(v)))
+
+    within = lax.rem(lax.broadcasted_iota(jnp.int32, (1, quarter), 1), block)
+
+    def scan(v, forward, join, empty):
+        step = 1
+        while step < block:
+            if forward:
+                v = join(v, jnp.where(within >= step, pltpu.roll(v, step, 1), empty))
+            else:
+                v = join(v, jnp.where(within < block - step, pltpu.roll(v, quarter - step, 1), empty))
+            step *= 2
+        return v
+
+    table = []
+    for d in range(2):
+        gate_in_row = gate_row(2 * d)
+        forget = log_sigmoid(gate_row(2 * d + 1)) + extra_row(d)
+        decay = scan(forget, d == 0, jnp.add, 0.0)
+        shifted = gate_in_row - decay
+        running = scan(shifted, d == 0, jnp.maximum, -jnp.inf)
+        table += [shifted, running, decay]
+    table += [jnp.zeros((1, quarter), f32)] * 2
+    rowsv[...] = jnp.concatenate(table, axis=0)
+
+    def turn_step(n, carry):
+        piece = rowsv[:, chunk(n)]
+        wide = jnp.concatenate([piece, jnp.zeros((LANES - piece.shape[0], block), f32)], axis=0)
+        colsv[chunk(n), :] = wide.T
+        return carry
+
+    lax.fori_loop(0, inner, turn_step, 0)
+
+    gpad, conv, hsend, hrecv = r.gpad, r.conv, r.hsend, r.hrecv
+    pad = hsend.shape[1]
+    reach = KW // 2
+
+    def project(n, j):
+        return jnp.dot(nq[chunk(n), :], wfull[j], preferred_element_type=f32)
+
+    collect(0)
+    deal_all(2)
+    collect(1)
+
+    def glu_step(n, carry):
+        glu = (project(n, 0) * jax.nn.sigmoid(project(n, 1))).astype(bf16)
+        gpad[pl.ds(pl.multiple_of(n * block + pad, pad), block), :] = glu.astype(f32)
+
+        @pl.when(n == 0)
+        def _():
+            hsend[0] = glu[:pad]
+
+        @pl.when(n == inner - 1)
+        def _():
+            hsend[1] = glu[block - pad :]
+
+        return carry
+
+    lax.fori_loop(0, inner, glu_step, 0)
+    has_before, has_after = place > 0, place < last
+
+    def device_of(q):
+        return (lax.div(q, tp) * tp + par, i, lax.rem(q, tp))
+
+    start(remote(hsend.at[0], hrecv.at[1], r.hal_s.at[0], r.hal_r.at[1], device_of(jnp.maximum(place - 1, 0))), has_before)
+    start(remote(hsend.at[1], hrecv.at[0], r.hal_s.at[1], r.hal_r.at[0], device_of(jnp.minimum(place + 1, last))), has_after)
+    deal_all(3)
+
+    @pl.when(primary)
+    def _():
+        for copy in own_small:
+            copy.wait()
+
+    @pl.when(jnp.logical_not(primary))
+    def _():
+        for copy in mate_small:
+            copy.wait_recv()
+
+    for side, present, at in ((0, has_before, 0), (1, has_after, pad + quarter)):
+        @pl.when(present)
+        def _():
+            remote(hrecv.at[side], hrecv.at[side], r.hal_s.at[0], r.hal_r.at[side], (o, i, mate)).wait_recv()
+            gpad[pl.ds(at, pad), :] = hrecv[side].astype(f32)
+
+        @pl.when(jnp.logical_not(present))
+        def _():
+            gpad[pl.ds(at, pad), :] = jnp.zeros((pad, HEAD), f32)
+
+    taps, statc, stbuf = r.taps, r.statc, r.stbuf
+    conv_rows = 64
+    lane = lax.broadcasted_iota(jnp.int32, (conv_rows, LANES), 1)
+    shift = pad - reach
+
+    def conv_step(m, carry):
+        window = gpad[pl.ds(pl.multiple_of(m * conv_rows, conv_rows), conv_rows + 2 * pad), :]
+        total = jnp.zeros((conv_rows, HEAD), f32)
+        for residue in range(8):
+            moved = window[residue : residue + conv_rows + 2 * pad - 8] if residue else window
+            for j in range(KW):
+                at = j + shift
+                if at % 8 == residue:
+                    total = total + taps[pl.ds(j, 1), :] * moved[at - residue : at - residue + conv_rows]
+        conv[span(m, conv_rows), :] = total
+        s1 = jnp.sum(total, axis=-1, keepdims=True)
+        s2 = jnp.sum(total * total, axis=-1, keepdims=True)
+        statc[span(m, conv_rows), :] = jnp.where(lane == 0, s1, jnp.where(lane == 1, s2, 0.0))
+        return carry
+
+    lax.fori_loop(0, quarter // conv_rows, conv_step, 0)
+    sums = r.sums
+
+    def sums_step(n, carry):
+        sums[:, chunk(n)] = statc[chunk(n), :].T[: sums.shape[0]]
+        return carry
+
+    lax.fori_loop(0, inner, sums_step, 0)
+    peers = []
+    for dz in range(tp):
+        for k in range(inner):
+            if (dz, k) != (0, 0):
+                peers.append((o if dz == 0 else twin, near[k]))
+    for index, (plane_to, chip) in enumerate(peers):
+        start(remote(sums, stbuf.at[head], r.sta_s.at[index], r.sta_r.at[head], (plane_to, chip, t)))
+    deal_all(4)
+
+    kb, vb, cm, cv = r.kb, r.vb, r.cm, r.cv
+    smat, sinfo, matx, infox = r.smat, r.sinfo, r.matx, r.infox
+
+    def key_step(n, carry):
+        kb[chunk(n), :] = project(n, 2).astype(bf16)
+        return carry
+
+    def state_step(n, carry):
+        values = project(n, 3).astype(bf16)
+        vb[chunk(n), :] = values
+        keys = kb[chunk(n), :].astype(f32)
+        cols = colsv[chunk(n), :]
+        for d in range(2):
+            end = block - 1 if d == 0 else 0
+            top = cols[end : end + 1, 3 * d + 1 : 3 * d + 2]
+            weighted = keys * (jnp.exp(cols[:, 3 * d : 3 * d + 1] - top) * scale)
+            cm[d, n] = lax.dot_general(
+                weighted.astype(bf16), values, (((0,), (0,)), ((), ())), preferred_element_type=f32
+            )
+            cv[d, n] = jnp.broadcast_to(jnp.sum(weighted, axis=0, keepdims=True), (8, HEAD))
+        return carry
+
+    collect(2)
+    lax.fori_loop(0, inner, key_step, 0)
+    collect(3)
+    lax.fori_loop(0, inner, state_step, 0)
+
+    def corner(n, d, column):
+        end = block - 1 if d == 0 else 0
+        at = n * block + end
+        return colsv[pl.ds(at, 1), :][:, column : column + 1]
+
+    totals = [[corner(n, d, 3 * d + 2) for n in range(inner)] for d in range(2)]
+    levels = [[corner(n, d, 3 * d + 1) + totals[d][n] for n in range(inner)] for d in range(2)]
+    for d in range(2):
+        reaches = []
+        for n in range(inner):
+            later = range(n + 1, inner) if d == 0 else range(n)
+            value = levels[d][n]
+            for m in later:
+                value = value + totals[d][m]
+            reaches.append(value)
+        top = functools.reduce(jnp.maximum, reaches)
+        shares = [jnp.exp(v - top) for v in reaches]
+        matx[d] = sum(shares[n] * cm[d, n] for n in range(inner)).astype(bf16)
+        vec = sum(shares[n] * cv[d, n] for n in range(inner))
+        row = lax.broadcasted_iota(jnp.int32, (8, HEAD), 0)
+        decay = functools.reduce(jnp.add, totals[d])
+        infox[d] = jnp.where(row == 0, vec, jnp.where(row == 1, top, decay))
+
+    for d in range(2):
+        for slot in range(outer):
+            empty = place <= slot if d == 0 else place >= slot
+
+            @pl.when(empty)
+            def _():
+                row = lax.broadcasted_iota(jnp.int32, (8, HEAD), 0)
+                smat[d, slot] = jnp.zeros((HEAD, HEAD), bf16)
+                sinfo[d, slot] = jnp.where(row == 1, LOW_START, 0.0)
+
+    for step in range(1, outer):
+        for d in range(2):
+            target = place + step if d == 0 else place - step
+            present = target <= last if d == 0 else target >= 0
+            device = device_of(jnp.clip(target, 0, last))
+            start(remote(matx.at[d], smat.at[d, place], r.mat_s.at[d, step - 1], r.mat_r.at[d, place], device), present)
+            start(remote(infox.at[d], sinfo.at[d, place], r.inf_s.at[d, step - 1], r.inf_r.at[d, place], device), present)
+
+    for plane_from, chip in peers:
+        other = lax.rem(plane_from, tp) * inner + chip
+        remote(sums, stbuf.at[other], r.sta_s.at[0], r.sta_r.at[other], (o, i, mate)).wait_recv()
+    stbuf[head] = sums[...]
+
+    def stat_step(n, carry):
+        whole = stbuf[0, :, chunk(n)]
+        for k in range(1, MEMORY_HEADS):
+            whole = whole + stbuf[k, :, chunk(n)]
+        whole = whole * (1.0 / channels)
+        mean = whole[0:1]
+        rstd = lax.rsqrt(whole[1:2] - mean * mean + EPS)
+        wide = jnp.concatenate([mean, rstd, jnp.zeros((LANES - 2, block), f32)], axis=0)
+        statc[chunk(n), :] = wide.T
+        return carry
+
+    lax.fori_loop(0, inner, stat_step, 0)
+    actb, memb, cin = r.actb, r.memb, r.cin
+
+    def give(which, source, b):
+        return remote(
+            source.at[chunk(b), :], cin.at[which, i], r.ret_s.at[which, b], r.ret_r.at[which, i],
+            (plane, b, par),
+        )
+
+    def give_own(which, source):
+        return local(source.at[chunk(i), :], cin.at[which, i], r.rel_s.at[which])
+
+    def give_rows(which, source, b):
+        to_self = jnp.logical_and(primary, b == i)
+        guarded(to_self, give_own(which, source).start)
+        guarded(jnp.logical_not(to_self), give(which, source, b).start)
+
+    def act_step(n, carry):
+        for half_at in range(2):
+            rows = pl.ds(pl.multiple_of(n * block + half_at * (block // 2), block // 2), block // 2)
+            cols = statc[rows, :]
+            normal = (conv[rows, :] - cols[:, 0:1]) * cols[:, 1:2] * r.lng[...] + r.lnb[...]
+            actb[rows, :] = (normal * jax.nn.sigmoid(normal)).astype(bf16)
+        give_rows(0, actb, n)
+        return carry
+
+    lax.fori_loop(0, inner, act_step, 0)
+
+    for d in range(2):
+        for slot in range(outer):
+            present = slot < place if d == 0 else slot > place
+
+            @pl.when(present)
+            def _():
+                remote(matx.at[d], smat.at[d, slot], r.mat_s.at[d, 0], r.mat_r.at[d, slot], (o, i, mate)).wait_recv()
+                remote(infox.at[d], sinfo.at[d, slot], r.inf_s.at[d, 0], r.inf_r.at[d, slot], (o, i, mate)).wait_recv()
+
+    chi, clo, nvs, levs = r.chi, r.clo, r.nvs, r.levs
+    for d in range(2):
+        reaches = []
+        for slot in range(outer):
+            value = sinfo[d, slot][1:2, 0:1]
+            for m in (range(slot + 1, outer) if d == 0 else range(slot)):
+                value = value + sinfo[d, m][2:3, 0:1]
+            reaches.append(value)
+        level = functools.reduce(jnp.maximum, reaches)
+        shares = [jnp.exp(v - level) for v in reaches]
+        mat = sum(shares[s] * smat[d, s].astype(f32) for s in range(outer))
+        vec = sum(shares[s] * sinfo[d, s][0:1] for s in range(outer))
+        for n in (range(inner) if d == 0 else range(inner - 1, -1, -1)):
+            high = mat.astype(bf16)
+            chi[d, n] = high
+            clo[d, n] = (mat - high.astype(f32)).astype(bf16)
+            nvs[d, n] = jnp.broadcast_to(vec, (8, HEAD))
+            levs[d, n] = jnp.broadcast_to(level, (8, LANES))
+            carried = level + totals[d][n]
+            new_level = jnp.maximum(carried, levels[d][n])
+            kept, added = jnp.exp(carried - new_level), jnp.exp(levels[d][n] - new_level)
+            mat = kept * mat + added * cm[d, n]
+            vec = kept * vec + added * cv[d, n][0:1]
+            level = new_level
+
+    acc, pbuf = r.acc, r.pbuf
+    tile = 512
+    tiles = model // tile
+
+    def own_sender(which):
+        return local(actb.at[chunk(i), :], cin.at[which, i], r.rel_s.at[which])
+
+    def take(which):
+        for k in range(inner):
+            def hear(k=k):
+                remote(actb.at[chunk(0), :], cin.at[which, near[k]], r.ret_s.at[which, 0], r.ret_r.at[which, near[k]], (o, i, mate)).wait_recv()
+            if k:
+                hear()
+            else:
+                guarded(jnp.logical_not(primary), hear)
+                guarded(primary, own_sender(which).wait)
+
+    def part(which, n):
+        return sum(
+            jnp.dot(cin[which, k], ow[which, pl.ds(k * HEAD, HEAD), span(n, tile)], preferred_element_type=f32)
+            for k in range(inner)
+        )
+
+    def conv_out_step(n, carry):
+        acc[:, span(n, tile)] = part(0, n)
+        return carry
+
+    for copy in out_in:
+        copy.wait()
+    take(0)
+    lax.fori_loop(0, tiles, conv_out_step, 0)
+
+    collect(4)
+    earlier = lax.broadcasted_iota(jnp.int32, (block, block), 0) >= lax.broadcasted_iota(jnp.int32, (block, block), 1)
+    later = lax.broadcasted_iota(jnp.int32, (block, block), 0) <= lax.broadcasted_iota(jnp.int32, (block, block), 1)
+
+    def memory_step(n, carry):
+        queries = project(n, 4).astype(bf16)
+        wide = queries.astype(f32)
+        scores = lax.dot_general(
+            queries, kb[chunk(n), :], (((1,), (1,)), ((), ())), preferred_element_type=f32
+        ) * scale
+        values = vb[chunk(n), :]
+        cols = colsv[chunk(n), :]
+        rows = rowsv[:, chunk(n)]
+        out = jnp.zeros((block, HEAD), f32)
+        for d in range(2):
+            running, decay = cols[:, 3 * d + 1 : 3 * d + 2], cols[:, 3 * d + 2 : 3 * d + 3]
+            level = levs[d, n][0:1, 0:1]
+            top = jnp.maximum(running, level)
+            carry_weight = jnp.exp(level - top)
+            weight = jnp.where(
+                earlier if d == 0 else later, jnp.exp(jnp.minimum(rows[3 * d : 3 * d + 1] - top, 0.0)), 0.0
+            )
+            inner_part = scores * weight
+            num = jnp.dot(inner_part.astype(bf16), values, preferred_element_type=f32)
+            far = jnp.dot(queries, chi[d, n], preferred_element_type=f32)
+            far = far + jnp.dot(queries, clo[d, n], preferred_element_type=f32)
+            num = num + carry_weight * far
+            den = jnp.sum(inner_part + wide * (carry_weight * nvs[d, n][0:1]), axis=-1, keepdims=True)
+            out = out + num / jnp.maximum(jnp.abs(den), jnp.exp(-top - decay))
+        level = lax.rsqrt(jnp.mean(out * out, axis=-1, keepdims=True) + EPS)
+        memb[chunk(n), :] = (out * level * r.mgn[...]).astype(bf16)
+        give_rows(1, memb, n)
+        return carry
+
+    lax.fori_loop(0, inner, memory_step, 0)
+    take(1)
+
+    out_own, out_mate = r.out_own, r.out_mate
+
+    def piece(n):
+        return remote(
+            pbuf.at[span(mate, hb), span(n, tile)], out_mate.at[:, span(n, tile)],
+            r.fin_s.at[n], r.fin_r.at[n], (o, i, mate),
+        )
+
+    def stay(n):
+        return local(pbuf.at[span(t, hb), span(n, tile)], out_own.at[:, span(n, tile)], r.fil_s.at[n])
+
+    def mem_out_step(n, carry):
+        pbuf[:, span(n, tile)] = (acc[:, span(n, tile)] + part(1, n)).astype(bf16)
+        piece(n).start()
+        stay(n).start()
+        return carry
+
+    lax.fori_loop(0, tiles, mem_out_step, 0)
+
+    for copy, when in sends:
+        if when is None:
+            copy.wait_send()
+        else:
+            pl.when(when)(copy.wait_send)
+
+    @pl.when(primary)
+    def _():
+        for copy in mate_small:
+            copy.wait_send()
         for j in range(count):
-            start(a2a(k, j))
-        start(ext(k))
-    for j in range(count):
-        staged[j].wait()
-    for way in range(2):
-        start(ring(way, 1, 0, stage_w))
-    for k in range(1, inner):
-        start(tok(k))
-    for c in range(1, tp):
-        start(hand(0, c, tokens))
-    staged[count].wait()
-    staged[count + 1].wait()
-    start_own = [
-        pltpu.make_async_copy(stage_w, piece(o, i), local.at[0]),
-        pltpu.make_async_copy(stage_t, block(i, t), local.at[1]),
-        pltpu.make_async_copy(stage_e, extras.at[i], local.at[2]),
-    ]
-    for copy in start_own:
-        copy.start()
-
-    def relay(distance, k):
-        for way in range(2):
-            if uses(way, distance, k):
-                ring(way, distance, k).wait_recv()
-                if distance < far and uses(way, distance + 1, k):
-                    start(ring(way, distance + 1, k))
-
-    for k in range(1, inner):
-        for j in range(count):
-            a2a(k, j).wait_recv()
-        for way in range(2):
-            start(ring(way, 1, k))
-        relay(1, k - 1)
-    relay(1, inner - 1)
-    for k in range(1, inner):
-        tok(k).wait_recv()
-        for c in range(1, tp):
-            start(hand(k, c))
-    for distance in range(2, far + 1):
-        for k in range(inner):
-            relay(distance, k)
-    for k in range(1, inner):
-        ext(k).wait_recv()
-    for k in range(inner):
-        for c in range(1, tp):
-            hand(k, c).wait_recv()
-    for copy in start_own:
-        copy.wait()
-    for copy in sends:
-        copy.wait_send()
-
-
-def exchange(tokens, weights, extra, outer, inner, tp):
-    rows, half = tokens.shape
-    depth, columns = weights[0].shape
-    width = columns // inner
-    count = len(weights)
-    turned = extra.T
+            for plane_at in deal_planes(j):
+                for k in range(1, inner):
+                    deal(j, plane_at, k).wait_send()
+                share(j, plane_at).wait_send()
+
+    for which, source in ((0, actb), (1, memb)):
+        for b in range(inner):
+            guarded(jnp.logical_not(jnp.logical_and(primary, i == b)), give(which, source, b).wait_send)
+    for n in range(tiles):
+        stay(n).wait()
+        piece(n).wait()
+
+
+LANES = 128
+LOW_START = -1e30
+
+
+def whole_layer(outer, inner, tp, args):
+    tokens = args.tokens
+    block, half = tokens.shape
+    depth = args.glu_value.shape[0]
+    count = 5
+    quarter, model = inner * block, half * tp
+    hb = block // tp
+    pad = 16
+    f32, bf16 = jnp.float32, jnp.bfloat16
     dma = pltpu.SemaphoreType.DMA
-    far = outer // 2
+    tiles = model // 512
+    extra = args.log_decay_extra.T
+    operands = dict(
+        tokens=tokens, norm_gain=args.norm_gain[None],
+        glu_value=args.glu_value, glu_gate=args.glu_gate,
+        key_weight=args.key_weight, value_weight=args.value_weight, query_weight=args.query_weight,
+        conv_taps=args.conv_taps, ln_gain=args.ln_gain[None], ln_bias=args.ln_bias[None],
+        gate_weight=args.gate_weight.T, gate_bias=args.gate_bias,
+        extra=extra, mem_gain=args.mem_gain[None],
+        out_conv=args.out_conv, out_mem=args.out_mem,
+    )
+    scratch = dict(
+        nq=pltpu.VMEM((quarter, model), bf16),
+        nsrc=pltpu.VMEM((hb, model), bf16),
+        xin=pltpu.VMEM((tp, hb, half), bf16),
+        wst=pltpu.VMEM((count, outer, depth, half), bf16),
+        wfull=pltpu.VMEM((count, model, HEAD), bf16),
+        ow=pltpu.VMEM((2,) + args.out_conv.shape, bf16),
+        taps=pltpu.VMEM((KW, HEAD), f32), lng=pltpu.VMEM((1, HEAD), f32),
+        lnb=pltpu.VMEM((1, HEAD), f32), mgn=pltpu.VMEM((1, HEAD), f32),
+        ext=pltpu.VMEM((inner,) + extra.shape, f32),
+        gwp=pltpu.VMEM((LANES, model), bf16),
+        gt=pltpu.VMEM((4 * MEMORY_HEADS, quarter), f32),
+        rowsv=pltpu.VMEM((8, quarter), f32), colsv=pltpu.VMEM((quarter, LANES), f32),
+        gpad=pltpu.VMEM((quarter + 2 * pad, HEAD), f32), conv=pltpu.VMEM((quarter, HEAD), f32),
+        hsend=pltpu.VMEM((2, pad, HEAD), bf16), hrecv=pltpu.VMEM((2, pad, HEAD), bf16),
+        statc=pltpu.VMEM((quarter, LANES), f32), sums=pltpu.VMEM((8, quarter), f32),
+        stbuf=pltpu.VMEM((MEMORY_HEADS, 8, quarter), f32),
+        kb=pltpu.VMEM((quarter, HEAD), bf16), vb=pltpu.VMEM((quarter, HEAD), bf16),
+        cm=pltpu.VMEM((2, inner, HEAD, HEAD), f32), cv=pltpu.VMEM((2, inner, 8, HEAD), f32),
+        matx=pltpu.VMEM((2, HEAD, HEAD), bf16), infox=pltpu.VMEM((2, 8, HEAD), f32),
+        smat=pltpu.VMEM((2, outer, HEAD, HEAD), bf16), sinfo=pltpu.VMEM((2, outer, 8, HEAD), f32),
+        chi=pltpu.VMEM((2, inner, HEAD, HEAD), bf16), clo=pltpu.VMEM((2, inner, HEAD, HEAD), bf16),
+        nvs=pltpu.VMEM((2, inner, 8, HEAD), f32), levs=pltpu.VMEM((2, inner, 8, LANES), f32),
+        actb=pltpu.VMEM((quarter, HEAD), bf16), memb=pltpu.VMEM((quarter, HEAD), bf16),
+        cin=pltpu.VMEM((2, inner, block, HEAD), bf16),
+        acc=pltpu.VMEM((block, model), f32), pbuf=pltpu.VMEM((block, model), bf16),
+        own_s=dma((count,)), loc_s=dma((5,)), xin_s=dma, xin_r=dma,
+        w1_s=dma((count, outer // tp)), w1_r=dma((count, outer)),
+        sml_s=dma((4,)), prm_s=dma((4,)), prm_r=dma((4,)),
+        ext_s=dma((inner,)), ext_r=dma((inner,)),
+        tok_s=dma((2,)), tok_r=dma((inner, tp)), pas_s=dma((6,)),
+        w2_s=dma((count, outer, inner - 1)), w2_r=dma((count, outer, inner - 1)),
+        keep_s=dma((count, outer)), fw_s=dma((count, outer)), fw_r=dma((count, outer)),
+        hal_s=dma((2,)), hal_r=dma((2,)),
+        sta_s=dma((MEMORY_HEADS,)), sta_r=dma((MEMORY_HEADS,)),
+        mat_s=dma((2, outer)), mat_r=dma((2, outer)), inf_s=dma((2, outer)), inf_r=dma((2, outer)),
+        ret_s=dma((2, inner)), ret_r=dma((2, inner)), rel_s=dma((2,)),
+        fin_s=dma((tiles,)), fin_r=dma((tiles,)), fil_s=dma((tiles,)),
+    )
     any_space = pl.BlockSpec(memory_space=pl.ANY)
-    whole, extras, pieces = pl.pallas_call(
-        functools.partial(exchange_kernel, outer, inner, tp, count),
-        out_shape=(
-            jax.ShapeDtypeStruct((inner * rows, tp * half), tokens.dtype),
-            jax.ShapeDtypeStruct((inner,) + turned.shape, turned.dtype),
-            jax.ShapeDtypeStruct((count, outer * inner * depth, width), weights[0].dtype),
+    spaces = {n: any_space for n in operands}
+    spaces.update(
+        gate_bias=pl.BlockSpec(memory_space=pltpu.SMEM), norm_gain=pl.BlockSpec(memory_space=pltpu.VMEM)
+    )
+    names = list(operands) + ["out_own", "out_mate"] + list(scratch)
+    shape = jax.ShapeDtypeStruct((hb, model), bf16)
+    own, mate = pl.pallas_call(
+        functools.partial(layer_kernel, outer, inner, tp, names),
+        out_shape=(shape, shape),
+        in_specs=[spaces[n] for n in operands],
+        out_specs=(any_space, any_space),
+        scratch_shapes=list(scratch.values()),
+        compiler_params=pltpu.CompilerParams(
+            collective_id=0, has_side_effects=True, vmem_limit_bytes=60 * 2**20
         ),
-        in_specs=[any_space] * (2 + count),
-        out_specs=(any_space,) * 3,
-        scratch_shapes=[
-            pltpu.VMEM((count, depth, width), weights[0].dtype),
-            pltpu.VMEM((rows, half), tokens.dtype),
-            pltpu.VMEM(turned.shape, turned.dtype),
-            dma((count + 2,)),
-            dma((inner - 1, count)), dma((inner - 1, count)),
-            dma((inner - 1,)), dma((inner - 1,)),
-            dma((inner - 1,)), dma((inner - 1,)),
-            dma((inner, tp - 1)), dma((inner, tp - 1)),
-            dma((2, far, inner)), dma((2, far, inner)),
-        ],
-        compiler_params=pltpu.CompilerParams(collective_id=0, has_side_effects=True),
-    )(tokens, turned, *weights)
-    extras = jnp.transpose(extras, (1, 0, 2)).reshape(turned.shape[0], inner * rows)
-    return whole, pieces, extras
+    )(*operands.values())
+    return (own.astype(f32) + mate.astype(f32)).astype(bf16)
 
 
 def gather_inputs(tokens, weights, extra, inner):
@@ -309,16 +877,22 @@
         out_conv,
         out_mem,
     ):
+        fits = tp == 2 and inner == 4 and outer % tp == 0 and inner * tp == MEMORY_HEADS
+        if fits and tokens.shape[1] == inner * HEAD and conv_taps.shape[1] == inner * HEAD:
+            return whole_layer(outer, inner, tp, types.SimpleNamespace(
+                tokens=tokens, norm_gain=norm_gain, glu_value=glu_value, glu_gate=glu_gate,
+                conv_taps=conv_taps, ln_gain=ln_gain, ln_bias=ln_bias, query_weight=query_weight,
+                key_weight=key_weight, value_weight=value_weight, gate_weight=gate_weight,
+                gate_bias=gate_bias, log_decay_extra=log_decay_extra, mem_gain=mem_gain,
+                out_conv=out_conv, out_mem=out_mem,
+            ))
         taps, gain, bias, mgain = own(conv_taps, 1), own(ln_gain, 0), own(ln_bias, 0), own(mem_gain, 0)
         channels = conv_taps.shape[1] * tp
         width = gain.shape[0]
         heads = mgain.shape[0] // HEAD
         first = (lax.axis_index("tp") * inner + lax.axis_index("inner")) * heads
         stacked = (query_weight, key_weight, value_weight, glu_value, glu_gate)
-        if inner > 1 and tp > 1 and outer > 2:
-            whole, weights, extras = exchange(tokens, stacked, log_decay_extra, outer, inner, tp)
-        else:
-            whole, weights, extras = gather_inputs(tokens, stacked, log_decay_extra, inner)
+        whole, weights, extras = gather_inputs(tokens, stacked, log_decay_extra, inner)
         rows = whole.shape[0]
         wide = whole.astype(jnp.float32)
         normed = (

time: 239 us -> 128 us (0.54)
  the two profiles are of different devices: /device:TPU:0 before, /device:TPU:15 now
where the time goes in v1:
time: 128 us
  Pallas kernels  126 us (98%)
  other arithmetic  2.12 us (2%)
    pallas_call x1, Pallas kernels, whole_layer(): pl.pallas_call(functools.partial(layer_kernel, outer, inner, tp, names),...  126 us

profile of v1, /device:TPU:15, one launch (start us, length us, event | category | flops | bytes accessed | tf_op | source)
XLA Modules:
  0.0 128.0 jit_solution(10843720320844082325)
XLA Ops:
  0.0 125.9 %shard_map.154 = (bf16[128,2048]{1,0:T(8,128)(2,1)}, bf16[128,2048]{1,0:T(8,128)(2,1)}) custom-call(bf16[256,1024]{1,0:T(8,128)(2,1)} %refs_0_.1, f32[1,2048]{1,0:T(1,128)} %bitcast.8, bf16[128,1024]{1,0:T(8,128)(2,1)} %refs_2_.1, bf16[128,1024]{1,0:T(8,128)(2,1)} %refs_3_.1, bf16[128,1024]{1,0:T(8,128)(2,1)} %refs_4_.1, bf16[128,1024]{1,0:T(8,128)(2,1)} %refs_5_.1, ...), custom_call_target="tpu_custom_call" | custom-call | tf_op jit(solution)/shard_map/pallas_call | solution.py:772
  125.9 2.1 %add_convert_fusion = bf16[128,2048]{1,0:T(8,128)(2,1)} fusion(bf16[128,2048]{1,0:T(8,128)(2,1)} %get-tuple-element.8, bf16[128,2048]{1,0:T(8,128)(2,1)} %get-tuple-element.7), kind=kLoop, calls=%fused_computation | loop fusion | flops 1048576 | bytes 1572864 | tf_op jit(solution)/shard_map/convert_element_type | solution.py:782

commit v2 on v1

--- a/solution.py
+++ b/solution.py
@@ -35,7 +35,7 @@
 def layer_kernel(outer, inner, tp, names, *refs):
     r = types.SimpleNamespace(**dict(zip(names, refs)))
     tokens, norm_gain = r.tokens, r.norm_gain
-    weights = [r.glu_value, r.glu_gate, r.key_weight, r.value_weight, r.query_weight]
+    weights = [r.key_weight, r.value_weight, r.glu_value, r.glu_gate, r.query_weight]
     count = len(weights)
     o, i, t = lax.axis_index("outer"), lax.axis_index("inner"), lax.axis_index("tp")
     block, half = tokens.shape
@@ -87,10 +87,8 @@
     tok_own = local(tokens.at[span(t, hb), :], xin.at[t], r.loc_s.at[0])
     tok_own.start()
 
-    @pl.when(primary)
-    def _():
-        for copy in own_rows:
-            copy.start()
+    for copy in own_rows:
+        copy.start()
 
     gate_in = local(r.gate_weight, r.gwp.at[pl.ds(0, r.gate_weight.shape[0]), :], r.loc_s.at[1])
     out_in = [
@@ -118,12 +116,44 @@
     def spread(j, step):
         target = lax.rem(grp + step, groups) * tp + t
         return remote(
-            weights[j], wst.at[j, o], r.w1_s.at[j, step], r.w1_r.at[j, o], (target, i, t)
-        )
-
-    def spread_all(j):
+            wst.at[j, o], wst.at[j, o], r.w1_s.at[j, step], r.w1_r.at[j, o], (target, i, t)
+        )
+
+    moved = (1, 3)
+
+    def plane_of(step):
+        return lax.rem(grp + step, groups) * tp
+
+    def hand_over(j):
+        at = moved.index(j)
+        return remote(wst.at[j, o], r.wmv.at[at], r.mov_s.at[at], r.mov_r.at[at], (o, i, mate))
+
+    def spread_all(j, phase):
         for step in range(groups):
-            start(spread(j, step), None if step else jnp.logical_not(primary))
+            target = lax.rem(grp + step, groups) * tp + t
+            apart = (target - o) * (twin - o) < 0
+            if phase == 0:
+                when = jnp.logical_and(apart, jnp.logical_not(primary))
+            elif phase == 1:
+                when = jnp.logical_not(apart)
+                if step == 0:
+                    when = jnp.logical_and(when, jnp.logical_not(primary))
+            else:
+                when = jnp.logical_and(apart, primary)
+            if step and phase == 1 and j in moved:
+                start(spread(j, step), jnp.logical_and(when, primary))
+                other = plane_of(step) + mate
+                at_end = jnp.logical_and(primary, (other - o) * (twin - o) > 0)
+
+                @pl.when(at_end)
+                def _():
+                    hand_over(j).wait_recv()
+
+                start(remote(
+                    r.wmv.at[moved.index(j)], wst.at[j, o], r.mvd_s.at[moved.index(j)], r.w1_r.at[j, o], (other, i, mate)
+                ), at_end)
+            elif step or phase == 1:
+                start(spread(j, step), when)
 
     def arrived(j, plane):
         remote(wst.at[j, plane], wst.at[j, plane], r.w1_s.at[j, 0], r.w1_r.at[j, plane], (o, i, mate)).wait_recv()
@@ -136,7 +166,12 @@
         remote(a.at[:, span(i, HEAD)], b, r.prm_s.at[k], r.prm_r.at[k], (o, i, mate))
         for k, (a, b) in enumerate(small)
     ]
-    spread_all(0)
+    for j in range(count):
+        own_rows[j].wait()
+        spread_all(j, 0)
+        if j in moved:
+            at_end = (plane_of(1) + t - o) * (twin - o) > 0
+            start(hand_over(j), jnp.logical_and(jnp.logical_not(primary), at_end))
 
     @pl.when(primary)
     def _():
@@ -160,6 +195,8 @@
     tok_own.wait()
     remote(xin.at[mate], xin.at[mate], r.xin_s, r.xin_r, (o, i, mate)).wait_recv()
     norm_rows = 32
+    pieces = 2
+    piece_rows = hb // pieces
 
     def norm_step(m, carry):
         at = span(m, norm_rows)
@@ -175,16 +212,21 @@
                 nq[pl.ds(pl.multiple_of(i * block + t * hb + m * norm_rows, norm_rows), norm_rows), pl.ds(f * half, half)] = row
         return carry
 
-    lax.fori_loop(0, hb // norm_rows, norm_step, 0)
-
-    def rows_of(b, c):
-        return nq.at[pl.ds(pl.multiple_of(b * block + c * hb, hb), hb), :]
-
-    def tok_wait(b, c):
-        remote(rows_of(b, c), rows_of(b, c), r.tok_s.at[0], r.tok_r.at[b, c], (o, i, mate)).wait_recv()
-
-    start(remote(nsrc, rows_of(i, t), r.tok_s.at[0], r.tok_r.at[i, t], (o, i, mate)), jnp.logical_not(primary))
-    start(remote(nsrc, rows_of(i, t), r.tok_s.at[1], r.tok_r.at[i, t], (twin, i, par)))
+    def rows_of(b, c, s):
+        return nq.at[pl.ds(pl.multiple_of(b * block + c * hb + s * piece_rows, piece_rows), piece_rows), :]
+
+    def tok_wait(b, c, s):
+        rows = rows_of(b, c, s)
+        remote(rows, rows, r.tok_s.at[0, 0], r.tok_r.at[b, c, s], (o, i, mate)).wait_recv()
+
+    steps = piece_rows // norm_rows
+    for s in range(pieces):
+        lax.fori_loop(s * steps, (s + 1) * steps, norm_step, 0)
+        source = nsrc.at[pl.ds(s * piece_rows, piece_rows), :]
+        start(remote(source, rows_of(i, t, s), r.tok_s.at[1, s], r.tok_r.at[i, t, s], (twin, i, par)))
+        start(remote(source, rows_of(i, t, s), r.tok_s.at[0, s], r.tok_r.at[i, t, s], (o, i, mate)), jnp.logical_not(primary))
+    for j in range(count):
+        spread_all(j, 1)
 
     def row_block(owner_plane, owner):
         return pl.ds(pl.multiple_of((owner_plane * inner + owner) * depth, depth), depth)
@@ -202,14 +244,11 @@
             r.keep_s.at[j, plane_at],
         )
 
-    def plane_of(step):
-        return lax.rem(grp + step, groups) * tp
-
     def deal_planes(j):
-        planes = [o, twin]
-        for step in range(1, groups):
-            planes += [plane_of(step), plane_of(step) + 1]
-        return planes
+        bases = [plane_of(step) for step in range(1, groups)]
+        nearer = [base + jnp.where(base < o, 1, 0) for base in bases]
+        farther = [base + jnp.where(base < o, 0, 1) for base in bases]
+        return [o] + nearer + [twin] + farther
 
     def deal_all(j, which=None):
         @pl.when(primary)
@@ -217,9 +256,7 @@
             for index, plane_at in enumerate(deal_planes(j)):
                 if which is not None and index not in which:
                     continue
-                if index == 0:
-                    own_rows[j].wait()
-                else:
+                if index:
                     arrived(j, plane_at)
                 for k in range(1, inner):
                     deal(j, plane_at, k).start()
@@ -247,35 +284,42 @@
             for plane_at in deal_planes(j):
                 share(j, plane_at).wait_recv()
 
-    deal_all(0, (0,))
-
-    def pass_on(b_from, c, k, slot):
-        return remote(
-            rows_of(b_from, c), rows_of(b_from, c), r.pas_s.at[slot], r.tok_r.at[b_from, c], (o, near[k], t)
-        )
-
-    def own_half(c):
-        @pl.when(jnp.logical_not(jnp.logical_and(primary, t == c)))
-        def _():
-            tok_wait(i, c)
-
-    first, second = t, mate
-    for index, c in enumerate((first, second)):
-        own_half(c)
-        start(pass_on(i, c, 1, 2 * index))
-        start(pass_on(i, c, 2, 2 * index + 1))
-    for j in range(1, count):
-        spread_all(j)
-    deal_all(0, range(1, outer))
-    tok_wait(near[1], 0)
-    start(pass_on(near[1], 0, 2, 4))
-    tok_wait(near[2], 1)
-    start(pass_on(near[2], 1, 1, 5))
+    def pass_on(b_from, c, s, k, slot):
+        rows = rows_of(b_from, c, s)
+        return remote(rows, rows, r.pas_s.at[slot, s], r.tok_r.at[b_from, c, s], (o, near[k], t))
+
+    @pl.when(primary)
+    def _():
+        for s in range(pieces):
+            for c, slot in ((t, 0), (mate, 2)):
+                if slot:
+                    tok_wait(i, c, s)
+                pass_on(i, c, s, 1, slot).start()
+                pass_on(i, c, s, 2, slot + 1).start()
+
+    @pl.when(jnp.logical_not(primary))
+    def _():
+        for s in range(pieces):
+            for c, slot in ((t, 0), (mate, 2)):
+                tok_wait(i, c, s)
+                pass_on(i, c, s, 1, slot).start()
+                pass_on(i, c, s, 2, slot + 1).start()
+
+    for s in range(pieces):
+        tok_wait(near[1], 0, s)
+        start(pass_on(near[1], 0, s, 2, 4))
+        tok_wait(near[2], 1, s)
+        start(pass_on(near[2], 1, s, 1, 5))
+    for j in range(count):
+        spread_all(j, 2)
+    for s in range(pieces):
+        tok_wait(near[1], 1, s)
+        tok_wait(near[2], 0, s)
+        tok_wait(near[3], 0, s)
+        tok_wait(near[3], 1, s)
+
+    deal_all(0)
     deal_all(1)
-    tok_wait(near[1], 1)
-    tok_wait(near[2], 0)
-    tok_wait(near[3], 0)
-    tok_wait(near[3], 1)
 
     gwp, gt, rowsv, colsv = r.gwp, r.gt, r.rowsv, r.colsv
     gate_in.wait()
@@ -348,107 +392,19 @@
 
     lax.fori_loop(0, inner, turn_step, 0)
 
-    gpad, conv, hsend, hrecv = r.gpad, r.conv, r.hsend, r.hrecv
-    pad = hsend.shape[1]
-    reach = KW // 2
-
     def project(n, j):
         return jnp.dot(nq[chunk(n), :], wfull[j], preferred_element_type=f32)
 
-    collect(0)
-    deal_all(2)
-    collect(1)
-
-    def glu_step(n, carry):
-        glu = (project(n, 0) * jax.nn.sigmoid(project(n, 1))).astype(bf16)
-        gpad[pl.ds(pl.multiple_of(n * block + pad, pad), block), :] = glu.astype(f32)
-
-        @pl.when(n == 0)
-        def _():
-            hsend[0] = glu[:pad]
-
-        @pl.when(n == inner - 1)
-        def _():
-            hsend[1] = glu[block - pad :]
-
-        return carry
-
-    lax.fori_loop(0, inner, glu_step, 0)
-    has_before, has_after = place > 0, place < last
-
-    def device_of(q):
-        return (lax.div(q, tp) * tp + par, i, lax.rem(q, tp))
-
-    start(remote(hsend.at[0], hrecv.at[1], r.hal_s.at[0], r.hal_r.at[1], device_of(jnp.maximum(place - 1, 0))), has_before)
-    start(remote(hsend.at[1], hrecv.at[0], r.hal_s.at[1], r.hal_r.at[0], device_of(jnp.minimum(place + 1, last))), has_after)
-    deal_all(3)
-
-    @pl.when(primary)
-    def _():
-        for copy in own_small:
-            copy.wait()
-
-    @pl.when(jnp.logical_not(primary))
-    def _():
-        for copy in mate_small:
-            copy.wait_recv()
-
-    for side, present, at in ((0, has_before, 0), (1, has_after, pad + quarter)):
-        @pl.when(present)
-        def _():
-            remote(hrecv.at[side], hrecv.at[side], r.hal_s.at[0], r.hal_r.at[side], (o, i, mate)).wait_recv()
-            gpad[pl.ds(at, pad), :] = hrecv[side].astype(f32)
-
-        @pl.when(jnp.logical_not(present))
-        def _():
-            gpad[pl.ds(at, pad), :] = jnp.zeros((pad, HEAD), f32)
-
-    taps, statc, stbuf = r.taps, r.statc, r.stbuf
-    conv_rows = 64
-    lane = lax.broadcasted_iota(jnp.int32, (conv_rows, LANES), 1)
-    shift = pad - reach
-
-    def conv_step(m, carry):
-        window = gpad[pl.ds(pl.multiple_of(m * conv_rows, conv_rows), conv_rows + 2 * pad), :]
-        total = jnp.zeros((conv_rows, HEAD), f32)
-        for residue in range(8):
-            moved = window[residue : residue + conv_rows + 2 * pad - 8] if residue else window
-            for j in range(KW):
-                at = j + shift
-                if at % 8 == residue:
-                    total = total + taps[pl.ds(j, 1), :] * moved[at - residue : at - residue + conv_rows]
-        conv[span(m, conv_rows), :] = total
-        s1 = jnp.sum(total, axis=-1, keepdims=True)
-        s2 = jnp.sum(total * total, axis=-1, keepdims=True)
-        statc[span(m, conv_rows), :] = jnp.where(lane == 0, s1, jnp.where(lane == 1, s2, 0.0))
-        return carry
-
-    lax.fori_loop(0, quarter // conv_rows, conv_step, 0)
-    sums = r.sums
-
-    def sums_step(n, carry):
-        sums[:, chunk(n)] = statc[chunk(n), :].T[: sums.shape[0]]
-        return carry
-
-    lax.fori_loop(0, inner, sums_step, 0)
-    peers = []
-    for dz in range(tp):
-        for k in range(inner):
-            if (dz, k) != (0, 0):
-                peers.append((o if dz == 0 else twin, near[k]))
-    for index, (plane_to, chip) in enumerate(peers):
-        start(remote(sums, stbuf.at[head], r.sta_s.at[index], r.sta_r.at[head], (plane_to, chip, t)))
-    deal_all(4)
-
     kb, vb, cm, cv = r.kb, r.vb, r.cm, r.cv
     smat, sinfo, matx, infox = r.smat, r.sinfo, r.matx, r.infox
+    gmat, ginfo, gin, gininfo = r.gmat, r.ginfo, r.gin, r.gininfo
 
     def key_step(n, carry):
-        kb[chunk(n), :] = project(n, 2).astype(bf16)
+        kb[chunk(n), :] = project(n, 0).astype(bf16)
         return carry
 
     def state_step(n, carry):
-        values = project(n, 3).astype(bf16)
+        values = project(n, 1).astype(bf16)
         vb[chunk(n), :] = values
         keys = kb[chunk(n), :].astype(f32)
         cols = colsv[chunk(n), :]
@@ -462,15 +418,19 @@
             cv[d, n] = jnp.broadcast_to(jnp.sum(weighted, axis=0, keepdims=True), (8, HEAD))
         return carry
 
-    collect(2)
+    collect(0)
     lax.fori_loop(0, inner, key_step, 0)
-    collect(3)
+    deal_all(2)
+    collect(1)
     lax.fori_loop(0, inner, state_step, 0)
 
     def corner(n, d, column):
         end = block - 1 if d == 0 else 0
         at = n * block + end
         return colsv[pl.ds(at, 1), :][:, column : column + 1]
+
+    def device_of(q):
+        return (lax.div(q, tp) * tp + par, i, lax.rem(q, tp))
 
     totals = [[corner(n, d, 3 * d + 2) for n in range(inner)] for d in range(2)]
     levels = [[corner(n, d, 3 * d + 1) + totals[d][n] for n in range(inner)] for d in range(2)]
@@ -490,89 +450,136 @@
         decay = functools.reduce(jnp.add, totals[d])
         infox[d] = jnp.where(row == 0, vec, jnp.where(row == 1, top, decay))
 
-    for d in range(2):
-        for slot in range(outer):
-            empty = place <= slot if d == 0 else place >= slot
-
-            @pl.when(empty)
-            def _():
-                row = lax.broadcasted_iota(jnp.int32, (8, HEAD), 0)
-                smat[d, slot] = jnp.zeros((HEAD, HEAD), bf16)
-                sinfo[d, slot] = jnp.where(row == 1, LOW_START, 0.0)
-
-    for step in range(1, outer):
-        for d in range(2):
-            target = place + step if d == 0 else place - step
-            present = target <= last if d == 0 else target >= 0
-            device = device_of(jnp.clip(target, 0, last))
-            start(remote(matx.at[d], smat.at[d, place], r.mat_s.at[d, step - 1], r.mat_r.at[d, place], device), present)
-            start(remote(infox.at[d], sinfo.at[d, place], r.inf_s.at[d, step - 1], r.inf_r.at[d, place], device), present)
-
-    for plane_from, chip in peers:
-        other = lax.rem(plane_from, tp) * inner + chip
-        remote(sums, stbuf.at[other], r.sta_s.at[0], r.sta_r.at[other], (o, i, mate)).wait_recv()
-    stbuf[head] = sums[...]
-
-    def stat_step(n, carry):
-        whole = stbuf[0, :, chunk(n)]
-        for k in range(1, MEMORY_HEADS):
-            whole = whole + stbuf[k, :, chunk(n)]
-        whole = whole * (1.0 / channels)
-        mean = whole[0:1]
-        rstd = lax.rsqrt(whole[1:2] - mean * mean + EPS)
-        wide = jnp.concatenate([mean, rstd, jnp.zeros((LANES - 2, block), f32)], axis=0)
-        statc[chunk(n), :] = wide.T
-        return carry
-
-    lax.fori_loop(0, inner, stat_step, 0)
-    actb, memb, cin = r.actb, r.memb, r.cin
-
-    def give(which, source, b):
-        return remote(
-            source.at[chunk(b), :], cin.at[which, i], r.ret_s.at[which, b], r.ret_r.at[which, i],
-            (plane, b, par),
-        )
-
-    def give_own(which, source):
-        return local(source.at[chunk(i), :], cin.at[which, i], r.rel_s.at[which])
-
-    def give_rows(which, source, b):
-        to_self = jnp.logical_and(primary, b == i)
-        guarded(to_self, give_own(which, source).start)
-        guarded(jnp.logical_not(to_self), give(which, source, b).start)
-
-    def act_step(n, carry):
-        for half_at in range(2):
-            rows = pl.ds(pl.multiple_of(n * block + half_at * (block // 2), block // 2), block // 2)
-            cols = statc[rows, :]
-            normal = (conv[rows, :] - cols[:, 0:1]) * cols[:, 1:2] * r.lng[...] + r.lnb[...]
-            actb[rows, :] = (normal * jax.nn.sigmoid(normal)).astype(bf16)
-        give_rows(0, actb, n)
-        return carry
-
-    lax.fori_loop(0, inner, act_step, 0)
-
-    for d in range(2):
-        for slot in range(outer):
-            present = slot < place if d == 0 else slot > place
-
-            @pl.when(present)
-            def _():
-                remote(matx.at[d], smat.at[d, slot], r.mat_s.at[d, 0], r.mat_r.at[d, slot], (o, i, mate)).wait_recv()
-                remote(infox.at[d], sinfo.at[d, slot], r.inf_s.at[d, 0], r.inf_r.at[d, slot], (o, i, mate)).wait_recv()
+    start(remote(matx, smat, r.mat_s.at[0], r.mat_r.at[0], (o, i, mate)))
+    start(remote(infox, sinfo, r.inf_s.at[0], r.inf_r.at[0], (o, i, mate)))
+    gpad, conv, hsend, hrecv = r.gpad, r.conv, r.hsend, r.hrecv
+    pad = hsend.shape[1]
+    reach = KW // 2
+    sides = HEAD // LANES
+
+    def value_step(n, carry):
+        r.gval[chunk(n), :] = project(n, 2)
+        return carry
+
+    deal_all(3, range(2))
+    mat_rows = gin.at[span(t, HEAD // tp), :]
+    mate_rows = gin.at[span(mate, HEAD // tp), :]
+    remote(matx, smat, r.mat_s.at[0], r.mat_r.at[0], (o, i, mate)).wait_recv()
+    remote(infox, sinfo, r.inf_s.at[0], r.inf_r.at[0], (o, i, mate)).wait_recv()
+    ours, theirs = infox[grp], sinfo[grp]
+    is_far = t == grp
+    our_reach = ours[1:2, 0:1] + jnp.where(is_far, theirs[2:3, 0:1], 0.0)
+    their_reach = theirs[1:2, 0:1] + jnp.where(is_far, 0.0, ours[2:3, 0:1])
+    group_level = jnp.maximum(our_reach, their_reach)
+    our_share, their_share = jnp.exp(our_reach - group_level), jnp.exp(their_reach - group_level)
+    gmat[...] = (our_share * matx[grp].astype(f32) + their_share * smat[grp].astype(f32)).astype(bf16)
+    state_row = lax.broadcasted_iota(jnp.int32, (8, HEAD), 0)
+    ginfo[...] = jnp.where(state_row == 0, our_share * ours[0:1] + their_share * theirs[0:1], group_level)
+    across = ((1 - grp) * tp + par, i, t)
+    start(remote(gmat.at[span(t, HEAD // tp), :], mat_rows, r.mat_s.at[1], r.mat_r.at[1], across))
+    start(remote(ginfo, gininfo, r.inf_s.at[1], r.inf_r.at[1], across))
+    collect(2)
+    lax.fori_loop(0, inner, value_step, 0)
+    deal_all(3, range(2, outer))
+    deal_all(4, range(2))
+    collect(3)
+
+    def glu_step(n, carry):
+        glu = (r.gval[chunk(n), :] * jax.nn.sigmoid(project(n, 3))).astype(bf16)
+        for side in range(sides):
+            gpad[side, pl.ds(pl.multiple_of(n * block + pad, pad), block), :] = glu[:, side * LANES : (side + 1) * LANES].astype(f32)
+
+        @pl.when(n == 0)
+        def _():
+            hsend[0] = glu[:pad]
+
+        @pl.when(n == inner - 1)
+        def _():
+            hsend[1] = glu[block - pad :]
+
+        return carry
+
+    lax.fori_loop(0, inner, glu_step, 0)
+    has_before, has_after = place > 0, place < last
+    start(remote(hsend.at[0], hrecv.at[1], r.hal_s.at[0], r.hal_r.at[1], device_of(jnp.maximum(place - 1, 0))), has_before)
+    start(remote(hsend.at[1], hrecv.at[0], r.hal_s.at[1], r.hal_r.at[0], device_of(jnp.minimum(place + 1, last))), has_after)
+
+    deal_all(4, (2,))
+
+    @pl.when(primary)
+    def _():
+        for copy in own_small:
+            copy.wait()
+
+    @pl.when(jnp.logical_not(primary))
+    def _():
+        for copy in mate_small:
+            copy.wait_recv()
+
+    for edge, present, at in ((0, has_before, 0), (1, has_after, pad + quarter)):
+        @pl.when(present)
+        def _():
+            remote(hrecv.at[edge], hrecv.at[edge], r.hal_s.at[0], r.hal_r.at[edge], (o, i, mate)).wait_recv()
+            for side in range(sides):
+                gpad[side, pl.ds(at, pad), :] = hrecv[edge, :, side * LANES : (side + 1) * LANES].astype(f32)
+
+        @pl.when(jnp.logical_not(present))
+        def _():
+            for side in range(sides):
+                gpad[side, pl.ds(at, pad), :] = jnp.zeros((pad, LANES), f32)
+
+    taps, statc, stbuf = r.taps, r.statc, r.stbuf
+    conv_rows = 64
+    lane = lax.broadcasted_iota(jnp.int32, (conv_rows, LANES), 1)
+    shift = pad - reach
+
+    def conv_step(m, carry):
+        s1 = s2 = 0.0
+        for side in range(sides):
+            total = jnp.zeros((conv_rows, LANES), f32)
+            for j in range(KW):
+                rows = gpad[side, pl.ds(m * conv_rows + (j + shift), conv_rows), :]
+                total = total + taps[pl.ds(j, 1), pl.ds(side * LANES, LANES)] * rows
+            conv[side, span(m, conv_rows), :] = total
+            s1 = s1 + total
+            s2 = s2 + total * total
+        s1 = jnp.sum(s1, axis=-1, keepdims=True)
+        s2 = jnp.sum(s2, axis=-1, keepdims=True)
+        statc[span(m, conv_rows), :] = jnp.where(lane == 0, s1, jnp.where(lane == 1, s2, 0.0))
+        return carry
+
+    lax.fori_loop(0, quarter // conv_rows, conv_step, 0)
+    deal_all(4, range(3, outer))
+    sums = r.sums
+
+    def sums_step(n, carry):
+        sums[:, chunk(n)] = statc[chunk(n), :].T[: sums.shape[0]]
+        return carry
+
+    lax.fori_loop(0, inner, sums_step, 0)
+    peers = []
+    for dz in range(tp):
+        for k in range(inner):
+            if (dz, k) != (0, 0):
+                peers.append((o if dz == 0 else twin, near[k]))
+    for index, (plane_to, chip) in enumerate(peers):
+        start(remote(sums, stbuf.at[head], r.sta_s.at[index], r.sta_r.at[head], (plane_to, chip, t)))
+    remote(mat_rows, mat_rows, r.mat_s.at[1], r.mat_r.at[1], (o, i, mate)).wait_recv()
+    start(remote(mat_rows, mat_rows, r.mat_s.at[2], r.mat_r.at[2], (o, i, mate)))
+    remote(ginfo, gininfo, r.inf_s.at[1], r.inf_r.at[1], (o, i, mate)).wait_recv()
+    remote(mate_rows, mate_rows, r.mat_s.at[2], r.mat_r.at[2], (o, i, mate)).wait_recv()
 
     chi, clo, nvs, levs = r.chi, r.clo, r.nvs, r.levs
     for d in range(2):
-        reaches = []
-        for slot in range(outer):
-            value = sinfo[d, slot][1:2, 0:1]
-            for m in (range(slot + 1, outer) if d == 0 else range(slot)):
-                value = value + sinfo[d, m][2:3, 0:1]
-            reaches.append(value)
-        level = functools.reduce(jnp.maximum, reaches)
-        shares = [jnp.exp(v - level) for v in reaches]
-        mat = sum(shares[s] * smat[d, s].astype(f32) for s in range(outer))
-        vec = sum(shares[s] * sinfo[d, s][0:1] for s in range(outer))
+        by_mate, by_group = t == 1 - d, grp == 1 - d
+        near_reach = jnp.where(by_mate, sinfo[d][1:2, 0:1], LOW_START)
+        far_reach = gininfo[1:2, 0:1] + jnp.where(by_mate, sinfo[d][2:3, 0:1], 0.0)
+        far_reach = jnp.where(by_group, far_reach, LOW_START)
+        level = jnp.maximum(near_reach, far_reach)
+        near_share = jnp.where(by_mate, jnp.exp(near_reach - level), 0.0)
+        far_share = jnp.where(by_group, jnp.exp(far_reach - level), 0.0)
+        mat = near_share * smat[d].astype(f32) + far_share * gin[...].astype(f32)
+        vec = near_share * sinfo[d][0:1] + far_share * gininfo[0:1]
         for n in (range(inner) if d == 0 else range(inner - 1, -1, -1)):
             high = mat.astype(bf16)
             chi[d, n] = high
@@ -586,6 +593,106 @@
             vec = kept * vec + added * cv[d, n][0:1]
             level = new_level
 
+    earlier = lax.broadcasted_iota(jnp.int32, (block, block), 0) >= lax.broadcasted_iota(jnp.int32, (block, block), 1)
+    later = lax.broadcasted_iota(jnp.int32, (block, block), 0) <= lax.broadcasted_iota(jnp.int32, (block, block), 1)
+    lane_at = lax.broadcasted_iota(jnp.int32, (block, LANES), 1)
+
+    def weight_step(n, carry):
+        cols = colsv[chunk(n), :]
+        rows = rowsv[:, chunk(n)]
+        kept = jnp.zeros((block, LANES), f32)
+        for d in range(2):
+            running, decay = cols[:, 3 * d + 1 : 3 * d + 2], cols[:, 3 * d + 2 : 3 * d + 3]
+            level = levs[d, n][0:1, 0:1]
+            top = jnp.maximum(running, level)
+            r.wgt[d, n] = jnp.where(
+                earlier if d == 0 else later,
+                jnp.exp(jnp.minimum(rows[3 * d : 3 * d + 1] - top, 0.0)) * scale, 0.0,
+            )
+            kept = jnp.where(lane_at == 2 * d, jnp.exp(level - top), kept)
+            kept = jnp.where(lane_at == 2 * d + 1, jnp.exp(-top - decay), kept)
+        r.colw[chunk(n), :] = kept
+        return carry
+
+    lax.fori_loop(0, inner, weight_step, 0)
+    collect(4)
+    for plane_from, chip in peers:
+        other = lax.rem(plane_from, tp) * inner + chip
+        remote(sums, stbuf.at[other], r.sta_s.at[0], r.sta_r.at[other], (o, i, mate)).wait_recv()
+    stbuf[head] = sums[...]
+
+    def stat_step(n, carry):
+        whole = stbuf[0, :, chunk(n)]
+        for k in range(1, MEMORY_HEADS):
+            whole = whole + stbuf[k, :, chunk(n)]
+        whole = whole * (1.0 / channels)
+        mean = whole[0:1]
+        rstd = lax.rsqrt(whole[1:2] - mean * mean + EPS)
+        wide = jnp.concatenate([mean, rstd, jnp.zeros((LANES - 2, block), f32)], axis=0)
+        statc[chunk(n), :] = wide.T
+        return carry
+
+    lax.fori_loop(0, inner, stat_step, 0)
+    actb, memb, cin = r.actb, r.memb, r.cin
+
+    def give(which, source, b):
+        return remote(
+            source.at[chunk(b), :], cin.at[which, i], r.ret_s.at[which, b], r.ret_r.at[which, i],
+            (plane, b, par),
+        )
+
+    def give_own(which, source):
+        return local(source.at[chunk(i), :], cin.at[which, i], r.rel_s.at[which])
+
+    def give_rows(which, source, b):
+        to_self = jnp.logical_and(primary, b == i)
+        guarded(to_self, give_own(which, source).start)
+        guarded(jnp.logical_not(to_self), give(which, source, b).start)
+
+    def turn(step):
+        k = inner - 1 - step
+        flip_x, flip_y = lax.rem(k, 2), lax.div(k, 2)
+        return (y + flip_y - 2 * y * flip_y) * 2 + x + flip_x - 2 * x * flip_x
+
+    def act_step(step, carry):
+        n = turn(step)
+        for half_at in range(2):
+            rows = pl.ds(pl.multiple_of(n * block + half_at * (block // 2), block // 2), block // 2)
+            cols = statc[rows, :]
+            for side in range(sides):
+                lanes = pl.ds(side * LANES, LANES)
+                normal = (conv[side, rows, :] - cols[:, 0:1]) * cols[:, 1:2] * r.lng[:, lanes] + r.lnb[:, lanes]
+                actb[rows, lanes] = (normal * jax.nn.sigmoid(normal)).astype(bf16)
+        give_rows(0, actb, n)
+        return carry
+
+    lax.fori_loop(0, inner, act_step, 0)
+
+    def memory_step(step, carry):
+        n = turn(step)
+        queries = project(n, 4).astype(bf16)
+        wide = queries.astype(f32)
+        scores = lax.dot_general(
+            queries, kb[chunk(n), :], (((1,), (1,)), ((), ())), preferred_element_type=f32
+        )
+        values = vb[chunk(n), :]
+        cols = r.colw[chunk(n), :]
+        out = jnp.zeros((block, HEAD), f32)
+        for d in range(2):
+            carry_weight, floor = cols[:, 2 * d : 2 * d + 1], cols[:, 2 * d + 1 : 2 * d + 2]
+            inner_part = scores * r.wgt[d, n]
+            num = jnp.dot(inner_part.astype(bf16), values, preferred_element_type=f32)
+            far = jnp.dot(queries, chi[d, n], preferred_element_type=f32)
+            far = far + jnp.dot(queries, clo[d, n], preferred_element_type=f32)
+            den = jnp.sum(inner_part + carry_weight * (wide * nvs[d, n][0:1]), axis=-1, keepdims=True)
+            share_of = 1.0 / jnp.maximum(jnp.abs(den), floor)
+            out = out + (num * share_of + far * (carry_weight * share_of))
+        level = lax.rsqrt(jnp.mean(out * out, axis=-1, keepdims=True) + EPS)
+        memb[chunk(n), :] = (out * level * r.mgn[...]).astype(bf16)
+        give_rows(1, memb, n)
+        return carry
+
+    lax.fori_loop(0, inner, memory_step, 0)
     acc, pbuf = r.acc, r.pbuf
     tile = 512
     tiles = model // tile
@@ -618,41 +725,6 @@
     take(0)
     lax.fori_loop(0, tiles, conv_out_step, 0)
 
-    collect(4)
-    earlier = lax.broadcasted_iota(jnp.int32, (block, block), 0) >= lax.broadcasted_iota(jnp.int32, (block, block), 1)
-    later = lax.broadcasted_iota(jnp.int32, (block, block), 0) <= lax.broadcasted_iota(jnp.int32, (block, block), 1)
-
-    def memory_step(n, carry):
-        queries = project(n, 4).astype(bf16)
-        wide = queries.astype(f32)
-        scores = lax.dot_general(
-            queries, kb[chunk(n), :], (((1,), (1,)), ((), ())), preferred_element_type=f32
-        ) * scale
-        values = vb[chunk(n), :]
-        cols = colsv[chunk(n), :]
-        rows = rowsv[:, chunk(n)]
-        out = jnp.zeros((block, HEAD), f32)
-        for d in range(2):
-            running, decay = cols[:, 3 * d + 1 : 3 * d + 2], cols[:, 3 * d + 2 : 3 * d + 3]
-            level = levs[d, n][0:1, 0:1]
-            top = jnp.maximum(running, level)
-            carry_weight = jnp.exp(level - top)
-            weight = jnp.where(
-                earlier if d == 0 else later, jnp.exp(jnp.minimum(rows[3 * d : 3 * d + 1] - top, 0.0)), 0.0
-            )
-            inner_part = scores * weight
-            num = jnp.dot(inner_part.astype(bf16), values, preferred_element_type=f32)
-            far = jnp.dot(queries, chi[d, n], preferred_element_type=f32)
-            far = far + jnp.dot(queries, clo[d, n], preferred_element_type=f32)
-            num = num + carry_weight * far
-            den = jnp.sum(inner_part + wide * (carry_weight * nvs[d, n][0:1]), axis=-1, keepdims=True)
-            out = out + num / jnp.maximum(jnp.abs(den), jnp.exp(-top - decay))
-        level = lax.rsqrt(jnp.mean(out * out, axis=-1, keepdims=True) + EPS)
-        memb[chunk(n), :] = (out * level * r.mgn[...]).astype(bf16)
-        give_rows(1, memb, n)
-        return carry
-
-    lax.fori_loop(0, inner, memory_step, 0)
     take(1)
 
     out_own, out_mate = r.out_own, r.out_mate
@@ -679,6 +751,11 @@
             copy.wait_send()
         else:
             pl.when(when)(copy.wait_send)
+
+    for s in range(pieces):
+        for c, slot in ((t, 0), (mate, 2)):
+            pass_on(i, c, s, 1, slot).wait_send()
+            pass_on(i, c, s, 2, slot + 1).wait_send()
 
     @pl.when(primary)
     def _():
@@ -729,6 +806,7 @@
         xin=pltpu.VMEM((tp, hb, half), bf16),
         wst=pltpu.VMEM((count, outer, depth, half), bf16),
         wfull=pltpu.VMEM((count, model, HEAD), bf16),
+        wmv=pltpu.VMEM((2, depth, half), bf16),
         ow=pltpu.VMEM((2,) + args.out_conv.shape, bf16),
         taps=pltpu.VMEM((KW, HEAD), f32), lng=pltpu.VMEM((1, HEAD), f32),
         lnb=pltpu.VMEM((1, HEAD), f32), mgn=pltpu.VMEM((1, HEAD), f32),
@@ -736,29 +814,33 @@
         gwp=pltpu.VMEM((LANES, model), bf16),
         gt=pltpu.VMEM((4 * MEMORY_HEADS, quarter), f32),
         rowsv=pltpu.VMEM((8, quarter), f32), colsv=pltpu.VMEM((quarter, LANES), f32),
-        gpad=pltpu.VMEM((quarter + 2 * pad, HEAD), f32), conv=pltpu.VMEM((quarter, HEAD), f32),
+        gpad=pltpu.VMEM((HEAD // LANES, quarter + 2 * pad, LANES), f32),
+        conv=pltpu.VMEM((HEAD // LANES, quarter, LANES), f32), gval=pltpu.VMEM((quarter, HEAD), f32),
         hsend=pltpu.VMEM((2, pad, HEAD), bf16), hrecv=pltpu.VMEM((2, pad, HEAD), bf16),
         statc=pltpu.VMEM((quarter, LANES), f32), sums=pltpu.VMEM((8, quarter), f32),
         stbuf=pltpu.VMEM((MEMORY_HEADS, 8, quarter), f32),
         kb=pltpu.VMEM((quarter, HEAD), bf16), vb=pltpu.VMEM((quarter, HEAD), bf16),
         cm=pltpu.VMEM((2, inner, HEAD, HEAD), f32), cv=pltpu.VMEM((2, inner, 8, HEAD), f32),
         matx=pltpu.VMEM((2, HEAD, HEAD), bf16), infox=pltpu.VMEM((2, 8, HEAD), f32),
-        smat=pltpu.VMEM((2, outer, HEAD, HEAD), bf16), sinfo=pltpu.VMEM((2, outer, 8, HEAD), f32),
+        smat=pltpu.VMEM((2, HEAD, HEAD), bf16), sinfo=pltpu.VMEM((2, 8, HEAD), f32),
+        gmat=pltpu.VMEM((HEAD, HEAD), bf16), ginfo=pltpu.VMEM((8, HEAD), f32),
+        gin=pltpu.VMEM((HEAD, HEAD), bf16), gininfo=pltpu.VMEM((8, HEAD), f32),
         chi=pltpu.VMEM((2, inner, HEAD, HEAD), bf16), clo=pltpu.VMEM((2, inner, HEAD, HEAD), bf16),
+        wgt=pltpu.VMEM((2, inner, block, block), f32), colw=pltpu.VMEM((quarter, LANES), f32),
         nvs=pltpu.VMEM((2, inner, 8, HEAD), f32), levs=pltpu.VMEM((2, inner, 8, LANES), f32),
         actb=pltpu.VMEM((quarter, HEAD), bf16), memb=pltpu.VMEM((quarter, HEAD), bf16),
         cin=pltpu.VMEM((2, inner, block, HEAD), bf16),
         acc=pltpu.VMEM((block, model), f32), pbuf=pltpu.VMEM((block, model), bf16),
-        own_s=dma((count,)), loc_s=dma((5,)), xin_s=dma, xin_r=dma,
+        own_s=dma((count,)), mov_s=dma((2,)), mov_r=dma((2,)), mvd_s=dma((2,)), loc_s=dma((5,)), xin_s=dma, xin_r=dma,
         w1_s=dma((count, outer // tp)), w1_r=dma((count, outer)),
         sml_s=dma((4,)), prm_s=dma((4,)), prm_r=dma((4,)),
         ext_s=dma((inner,)), ext_r=dma((inner,)),
-        tok_s=dma((2,)), tok_r=dma((inner, tp)), pas_s=dma((6,)),
+        tok_s=dma((2, 2)), tok_r=dma((inner, tp, 2)), pas_s=dma((6, 2)),
         w2_s=dma((count, outer, inner - 1)), w2_r=dma((count, outer, inner - 1)),
         keep_s=dma((count, outer)), fw_s=dma((count, outer)), fw_r=dma((count, outer)),
         hal_s=dma((2,)), hal_r=dma((2,)),
         sta_s=dma((MEMORY_HEADS,)), sta_r=dma((MEMORY_HEADS,)),
-        mat_s=dma((2, outer)), mat_r=dma((2, outer)), inf_s=dma((2, outer)), inf_r=dma((2, outer)),
+        mat_s=dma((3,)), mat_r=dma((3,)), inf_s=dma((2,)), inf_r=dma((2,)),
         ret_s=dma((2, inner)), ret_r=dma((2, inner)), rel_s=dma((2,)),
         fin_s=dma((tiles,)), fin_r=dma((tiles,)), fil_s=dma((tiles,)),
     )
@@ -768,12 +850,12 @@
         gate_bias=pl.BlockSpec(memory_space=pltpu.SMEM), norm_gain=pl.BlockSpec(memory_space=pltpu.VMEM)
     )
     names = list(operands) + ["out_own", "out_mate"] + list(scratch)
-    shape = jax.ShapeDtypeStruct((hb, model), bf16)
+    shape = pltpu.VMEM((hb, model), bf16)
     own, mate = pl.pallas_call(
         functools.partial(layer_kernel, outer, inner, tp, names),
         out_shape=(shape, shape),
         in_specs=[spaces[n] for n in operands],
-        out_specs=(any_space, any_space),
+        out_specs=(pl.BlockSpec(memory_space=pltpu.VMEM),) * 2,
         scratch_shapes=list(scratch.values()),
         compiler_params=pltpu.CompilerParams(
             collective_id=0, has_side_effects=True, vmem_limit_bytes=60 * 2**20
@@ -877,7 +959,7 @@
         out_conv,
         out_mem,
     ):
-        fits = tp == 2 and inner == 4 and outer % tp == 0 and inner * tp == MEMORY_HEADS
+        fits = tp == 2 and inner == 4 and outer == 2 * tp and inner * tp == MEMORY_HEADS
         if fits and tokens.shape[1] == inner * HEAD and conv_taps.shape[1] == inner * HEAD:
             return whole_layer(outer, inner, tp, types.SimpleNamespace(
                 tokens=tokens, norm_gain=norm_gain, glu_value=glu_value, glu_gate=glu_gate,

time: 128 us -> 113 us (0.88)
  the two profiles are of different devices: /device:TPU:15 before, /device:TPU:0 now
where the time goes in v2:
time: 113 us; the launch traced here: 112 us
  Pallas kernels  112 us (99%)
    pallas_call x1, Pallas kernels, whole_layer(): pl.pallas_call(functools.partial(layer_kernel, outer, inner, tp, names),...  112 us

profile of v2, /device:TPU:0, one launch (start us, length us, event | category | flops | bytes accessed | tf_op | source)
XLA Modules:
  0.0 112.5 jit_solution(13202958774305830726)
XLA Ops:
  0.0 111.5 %shard_map.154 = (bf16[128,2048]{1,0:T(8,128)(2,1)S(1)}, bf16[128,2048]{1,0:T(8,128)(2,1)S(1)}) custom-call(bf16[256,1024]{1,0:T(8,128)(2,1)} %refs_0_.1, f32[1,2048]{1,0:T(1,128)} %bitcast.8, bf16[128,1024]{1,0:T(8,128)(2,1)} %refs_2_.1, bf16[128,1024]{1,0:T(8,128)(2,1)} %refs_3_.1, bf16[128,1024]{1,0:T(8,128)(2,1)} %refs_4_.1, bf16[128,1024]{1,0:T(8,128)(2,1)} %refs_5_.1, ...), custom_call_target="tpu_custom_call" | custom-call | tf_op jit(solution)/shard_map/pallas_call | solution.py:854
  111.5 0.9 add_convert_fusion

commit v3 on v2

--- a/solution.py
+++ b/solution.py
@@ -35,7 +35,7 @@
 def layer_kernel(outer, inner, tp, names, *refs):
     r = types.SimpleNamespace(**dict(zip(names, refs)))
     tokens, norm_gain = r.tokens, r.norm_gain
-    weights = [r.key_weight, r.value_weight, r.glu_value, r.glu_gate, r.query_weight]
+    weights = [r.glu_value, r.glu_gate, r.key_weight, r.value_weight, r.query_weight]
     count = len(weights)
     o, i, t = lax.axis_index("outer"), lax.axis_index("inner"), lax.axis_index("tp")
     block, half = tokens.shape
@@ -400,11 +400,11 @@
     gmat, ginfo, gin, gininfo = r.gmat, r.ginfo, r.gin, r.gininfo
 
     def key_step(n, carry):
-        kb[chunk(n), :] = project(n, 0).astype(bf16)
+        kb[chunk(n), :] = project(n, 2).astype(bf16)
         return carry
 
     def state_step(n, carry):
-        values = project(n, 1).astype(bf16)
+        values = project(n, 3).astype(bf16)
         vb[chunk(n), :] = values
         keys = kb[chunk(n), :].astype(f32)
         cols = colsv[chunk(n), :]
@@ -418,19 +418,135 @@
             cv[d, n] = jnp.broadcast_to(jnp.sum(weighted, axis=0, keepdims=True), (8, HEAD))
         return carry
 
+    earlier = lax.broadcasted_iota(jnp.int32, (block, block), 0) >= lax.broadcasted_iota(jnp.int32, (block, block), 1)
+    later = lax.broadcasted_iota(jnp.int32, (block, block), 0) <= lax.broadcasted_iota(jnp.int32, (block, block), 1)
+
+    def weight_step(n, carry):
+        cols = colsv[chunk(n), :]
+        rows = rowsv[:, chunk(n)]
+        for d in range(2):
+            gap = jnp.minimum(rows[3 * d : 3 * d + 1] - cols[:, 3 * d + 1 : 3 * d + 2], 0.0)
+            r.wgt[d, n] = jnp.where(earlier if d == 0 else later, jnp.exp(gap) * scale, 0.0)
+        return carry
+
+    lax.fori_loop(0, inner, weight_step, 0)
     collect(0)
-    lax.fori_loop(0, inner, key_step, 0)
+    gpad, conv, hsend, hrecv = r.gpad, r.conv, r.hsend, r.hrecv
+    pad = hsend.shape[1]
+    reach = KW // 2
+    sides = HEAD // LANES
+
+    def value_step(n, carry):
+        r.gval[chunk(n), :] = project(n, 0)
+        return carry
+
+    lax.fori_loop(0, inner, value_step, 0)
     deal_all(2)
     collect(1)
-    lax.fori_loop(0, inner, state_step, 0)
+
+    def glu_step(n, carry):
+        glu = (r.gval[chunk(n), :] * jax.nn.sigmoid(project(n, 1))).astype(bf16)
+        for side in range(sides):
+            gpad[side, pl.ds(pl.multiple_of(n * block + pad, pad), block), :] = glu[:, side * LANES : (side + 1) * LANES].astype(f32)
+
+        @pl.when(n == 0)
+        def _():
+            hsend[0] = glu[:pad]
+
+        @pl.when(n == inner - 1)
+        def _():
+            hsend[1] = glu[block - pad :]
+
+        return carry
+
+    lax.fori_loop(0, inner, glu_step, 0)
+    def device_of(q):
+        return (lax.div(q, tp) * tp + par, i, lax.rem(q, tp))
+
+    has_before, has_after = place > 0, place < last
+    start(remote(hsend.at[0], hrecv.at[1], r.hal_s.at[0], r.hal_r.at[1], device_of(jnp.maximum(place - 1, 0))), has_before)
+    start(remote(hsend.at[1], hrecv.at[0], r.hal_s.at[1], r.hal_r.at[0], device_of(jnp.minimum(place + 1, last))), has_after)
+
+    @pl.when(primary)
+    def _():
+        for copy in own_small:
+            copy.wait()
+
+    @pl.when(jnp.logical_not(primary))
+    def _():
+        for copy in mate_small:
+            copy.wait_recv()
+
+    deal_all(3, range(2))
+    taps, statc, stbuf = r.taps, r.statc, r.stbuf
+    conv_rows = 64
+    lane = lax.broadcasted_iota(jnp.int32, (conv_rows, LANES), 1)
+    shift = pad - reach
+
+    def conv_step(m, carry):
+        s1 = s2 = 0.0
+        for side in range(sides):
+            total = jnp.zeros((conv_rows, LANES), f32)
+            for residue in range(8):
+                moved = gpad[side, pl.ds(m * conv_rows + residue, conv_rows + 2 * pad - 8), :]
+                for j in range(KW):
+                    at = j + shift - residue
+                    if at % 8 == 0:
+                        tap = taps[pl.ds(j, 1), pl.ds(side * LANES, LANES)]
+                        total = total + tap * moved[at : at + conv_rows]
+            conv[side, span(m, conv_rows), :] = total
+            s1 = s1 + total
+            s2 = s2 + total * total
+        s1 = jnp.sum(s1, axis=-1, keepdims=True)
+        s2 = jnp.sum(s2, axis=-1, keepdims=True)
+        statc[span(m, conv_rows), :] = jnp.where(lane == 0, s1, jnp.where(lane == 1, s2, 0.0))
+        return carry
+
+    conv_steps = quarter // conv_rows
+    lax.fori_loop(1, conv_steps // 2, conv_step, 0)
+    collect(2)
+    lax.fori_loop(conv_steps // 2, conv_steps - 1, conv_step, 0)
+    deal_all(3, range(2, outer))
+    for edge, present, at in ((0, has_before, 0), (1, has_after, pad + quarter)):
+        @pl.when(present)
+        def _():
+            remote(hrecv.at[edge], hrecv.at[edge], r.hal_s.at[0], r.hal_r.at[edge], (o, i, mate)).wait_recv()
+            for side in range(sides):
+                gpad[side, pl.ds(at, pad), :] = hrecv[edge, :, side * LANES : (side + 1) * LANES].astype(f32)
+
+        @pl.when(jnp.logical_not(present))
+        def _():
+            for side in range(sides):
+                gpad[side, pl.ds(at, pad), :] = jnp.zeros((pad, LANES), f32)
+
+    lax.fori_loop(0, 2, lambda m, carry: conv_step(m * (conv_steps - 1), carry), 0)
+    sums = r.sums
+    two = pl.ds(0, 2)
+
+    def sums_step(n, carry):
+        sums[:, chunk(n)] = statc[chunk(n), :].T[: sums.shape[0]]
+        return carry
+
+    lax.fori_loop(0, inner, sums_step, 0)
+    peers = []
+    for dz in range(tp):
+        for k in range(inner):
+            if (dz, k) != (0, 0):
+                peers.append((o if dz == 0 else twin, near[k]))
+    for index, (plane_to, chip) in enumerate(peers):
+        start(remote(sums.at[two, :], stbuf.at[head, two, :], r.sta_s.at[index], r.sta_r.at[head], (plane_to, chip, t)))
+    lax.fori_loop(0, inner, key_step, 0)
+    deal_all(4, range(2))
+    collect(3)
+    deal_all(4, (2,))
+    lax.fori_loop(0, inner // 2, state_step, 0)
+    deal_all(4, range(3, outer))
+    lax.fori_loop(inner // 2, inner, state_step, 0)
 
     def corner(n, d, column):
         end = block - 1 if d == 0 else 0
         at = n * block + end
         return colsv[pl.ds(at, 1), :][:, column : column + 1]
-
-    def device_of(q):
-        return (lax.div(q, tp) * tp + par, i, lax.rem(q, tp))
 
     totals = [[corner(n, d, 3 * d + 2) for n in range(inner)] for d in range(2)]
     levels = [[corner(n, d, 3 * d + 1) + totals[d][n] for n in range(inner)] for d in range(2)]
@@ -452,16 +568,56 @@
 
     start(remote(matx, smat, r.mat_s.at[0], r.mat_r.at[0], (o, i, mate)))
     start(remote(infox, sinfo, r.inf_s.at[0], r.inf_r.at[0], (o, i, mate)))
-    gpad, conv, hsend, hrecv = r.gpad, r.conv, r.hsend, r.hrecv
-    pad = hsend.shape[1]
-    reach = KW // 2
-    sides = HEAD // LANES
-
-    def value_step(n, carry):
-        r.gval[chunk(n), :] = project(n, 2)
-        return carry
-
-    deal_all(3, range(2))
+    for plane_from, chip in peers:
+        other = lax.rem(plane_from, tp) * inner + chip
+        remote(sums.at[two, :], stbuf.at[other, two, :], r.sta_s.at[0], r.sta_r.at[other], (o, i, mate)).wait_recv()
+    stbuf[head] = sums[...]
+
+    def stat_step(n, carry):
+        whole = stbuf[0, :, chunk(n)]
+        for k in range(1, MEMORY_HEADS):
+            whole = whole + stbuf[k, :, chunk(n)]
+        whole = whole * (1.0 / channels)
+        mean = whole[0:1]
+        rstd = lax.rsqrt(whole[1:2] - mean * mean + EPS)
+        wide = jnp.concatenate([mean, rstd, jnp.zeros((LANES - 2, block), f32)], axis=0)
+        statc[chunk(n), :] = wide.T
+        return carry
+
+    lax.fori_loop(0, inner, stat_step, 0)
+    actb, memb, cin = r.actb, r.memb, r.cin
+
+    def give(which, source, b):
+        return remote(
+            source.at[chunk(b), :], cin.at[which, i], r.ret_s.at[which, b], r.ret_r.at[which, i],
+            (plane, b, par),
+        )
+
+    def give_own(which, source):
+        return local(source.at[chunk(i), :], cin.at[which, i], r.rel_s.at[which])
+
+    def give_rows(which, source, b):
+        to_self = jnp.logical_and(primary, b == i)
+        guarded(to_self, give_own(which, source).start)
+        guarded(jnp.logical_not(to_self), give(which, source, b).start)
+
+    def turn(step):
+        k = inner - 1 - step
+        flip_x, flip_y = lax.rem(k, 2), lax.div(k, 2)
+        return (y + flip_y - 2 * y * flip_y) * 2 + x + flip_x - 2 * x * flip_x
+
+    def act_step(n, carry):
+        for half_at in range(2):
+            rows = pl.ds(pl.multiple_of(n * block + half_at * (block // 2), block // 2), block // 2)
+            cols = statc[rows, :]
+            for side in range(sides):
+                lanes = pl.ds(side * LANES, LANES)
+                normal = (conv[side, rows, :] - cols[:, 0:1]) * cols[:, 1:2] * r.lng[:, lanes] + r.lnb[:, lanes]
+                actb[rows, lanes] = (normal * jax.nn.sigmoid(normal)).astype(bf16)
+        return carry
+
+    lax.fori_loop(0, inner, act_step, 0)
+
     mat_rows = gin.at[span(t, HEAD // tp), :]
     mate_rows = gin.at[span(mate, HEAD // tp), :]
     remote(matx, smat, r.mat_s.at[0], r.mat_r.at[0], (o, i, mate)).wait_recv()
@@ -478,98 +634,21 @@
     across = ((1 - grp) * tp + par, i, t)
     start(remote(gmat.at[span(t, HEAD // tp), :], mat_rows, r.mat_s.at[1], r.mat_r.at[1], across))
     start(remote(ginfo, gininfo, r.inf_s.at[1], r.inf_r.at[1], across))
-    collect(2)
-    lax.fori_loop(0, inner, value_step, 0)
-    deal_all(3, range(2, outer))
-    deal_all(4, range(2))
-    collect(3)
-
-    def glu_step(n, carry):
-        glu = (r.gval[chunk(n), :] * jax.nn.sigmoid(project(n, 3))).astype(bf16)
-        for side in range(sides):
-            gpad[side, pl.ds(pl.multiple_of(n * block + pad, pad), block), :] = glu[:, side * LANES : (side + 1) * LANES].astype(f32)
-
-        @pl.when(n == 0)
-        def _():
-            hsend[0] = glu[:pad]
-
-        @pl.when(n == inner - 1)
-        def _():
-            hsend[1] = glu[block - pad :]
-
-        return carry
-
-    lax.fori_loop(0, inner, glu_step, 0)
-    has_before, has_after = place > 0, place < last
-    start(remote(hsend.at[0], hrecv.at[1], r.hal_s.at[0], r.hal_r.at[1], device_of(jnp.maximum(place - 1, 0))), has_before)
-    start(remote(hsend.at[1], hrecv.at[0], r.hal_s.at[1], r.hal_r.at[0], device_of(jnp.minimum(place + 1, last))), has_after)
-
-    deal_all(4, (2,))
-
-    @pl.when(primary)
-    def _():
-        for copy in own_small:
-            copy.wait()
-
-    @pl.when(jnp.logical_not(primary))
-    def _():
-        for copy in mate_small:
-            copy.wait_recv()
-
-    for edge, present, at in ((0, has_before, 0), (1, has_after, pad + quarter)):
-        @pl.when(present)
-        def _():
-            remote(hrecv.at[edge], hrecv.at[edge], r.hal_s.at[0], r.hal_r.at[edge], (o, i, mate)).wait_recv()
-            for side in range(sides):
-                gpad[side, pl.ds(at, pad), :] = hrecv[edge, :, side * LANES : (side + 1) * LANES].astype(f32)
-
-        @pl.when(jnp.logical_not(present))
-        def _():
-            for side in range(sides):
-                gpad[side, pl.ds(at, pad), :] = jnp.zeros((pad, LANES), f32)
-
-    taps, statc, stbuf = r.taps, r.statc, r.stbuf
-    conv_rows = 64
-    lane = lax.broadcasted_iota(jnp.int32, (conv_rows, LANES), 1)
-    shift = pad - reach
-
-    def conv_step(m, carry):
-        s1 = s2 = 0.0
-        for side in range(sides):
-            total = jnp.zeros((conv_rows, LANES), f32)
-            for j in range(KW):
-                rows = gpad[side, pl.ds(m * conv_rows + (j + shift), conv_rows), :]
-                total = total + taps[pl.ds(j, 1), pl.ds(side * LANES, LANES)] * rows
-            conv[side, span(m, conv_rows), :] = total
-            s1 = s1 + total
-            s2 = s2 + total * total
-        s1 = jnp.sum(s1, axis=-1, keepdims=True)
-        s2 = jnp.sum(s2, axis=-1, keepdims=True)
-        statc[span(m, conv_rows), :] = jnp.where(lane == 0, s1, jnp.where(lane == 1, s2, 0.0))
-        return carry
-
-    lax.fori_loop(0, quarter // conv_rows, conv_step, 0)
-    deal_all(4, range(3, outer))
-    sums = r.sums
-
-    def sums_step(n, carry):
-        sums[:, chunk(n)] = statc[chunk(n), :].T[: sums.shape[0]]
-        return carry
-
-    lax.fori_loop(0, inner, sums_step, 0)
-    peers = []
-    for dz in range(tp):
-        for k in range(inner):
-            if (dz, k) != (0, 0):
-                peers.append((o if dz == 0 else twin, near[k]))
-    for index, (plane_to, chip) in enumerate(peers):
-        start(remote(sums, stbuf.at[head], r.sta_s.at[index], r.sta_r.at[head], (plane_to, chip, t)))
+    for k in range(inner - 1, -1, -1):
+        give_rows(0, actb, near[k])
+    collect(4)
+
+    def query_step(n, carry):
+        r.qb[chunk(n), :] = project(n, 4).astype(bf16)
+        return carry
+
+    lax.fori_loop(0, inner, query_step, 0)
     remote(mat_rows, mat_rows, r.mat_s.at[1], r.mat_r.at[1], (o, i, mate)).wait_recv()
     start(remote(mat_rows, mat_rows, r.mat_s.at[2], r.mat_r.at[2], (o, i, mate)))
     remote(ginfo, gininfo, r.inf_s.at[1], r.inf_r.at[1], (o, i, mate)).wait_recv()
     remote(mate_rows, mate_rows, r.mat_s.at[2], r.mat_r.at[2], (o, i, mate)).wait_recv()
 
-    chi, clo, nvs, levs = r.chi, r.clo, r.nvs, r.levs
+    nvs, levs = r.nvs, r.levs
     for d in range(2):
         by_mate, by_group = t == 1 - d, grp == 1 - d
         near_reach = jnp.where(by_mate, sinfo[d][1:2, 0:1], LOW_START)
@@ -582,8 +661,8 @@
         vec = near_share * sinfo[d][0:1] + far_share * gininfo[0:1]
         for n in (range(inner) if d == 0 else range(inner - 1, -1, -1)):
             high = mat.astype(bf16)
-            chi[d, n] = high
-            clo[d, n] = (mat - high.astype(f32)).astype(bf16)
+            r.cst[d, n, pl.ds(0, HEAD), :] = high
+            r.cst[d, n, pl.ds(HEAD, HEAD), :] = (mat - high.astype(f32)).astype(bf16)
             nvs[d, n] = jnp.broadcast_to(vec, (8, HEAD))
             levs[d, n] = jnp.broadcast_to(level, (8, LANES))
             carried = level + totals[d][n]
@@ -593,100 +672,41 @@
             vec = kept * vec + added * cv[d, n][0:1]
             level = new_level
 
-    earlier = lax.broadcasted_iota(jnp.int32, (block, block), 0) >= lax.broadcasted_iota(jnp.int32, (block, block), 1)
-    later = lax.broadcasted_iota(jnp.int32, (block, block), 0) <= lax.broadcasted_iota(jnp.int32, (block, block), 1)
-    lane_at = lax.broadcasted_iota(jnp.int32, (block, LANES), 1)
-
-    def weight_step(n, carry):
-        cols = colsv[chunk(n), :]
+    def column_step(n, carry):
         rows = rowsv[:, chunk(n)]
-        kept = jnp.zeros((block, LANES), f32)
+        kept = []
         for d in range(2):
-            running, decay = cols[:, 3 * d + 1 : 3 * d + 2], cols[:, 3 * d + 2 : 3 * d + 3]
+            running, decay = rows[3 * d + 1 : 3 * d + 2], rows[3 * d + 2 : 3 * d + 3]
             level = levs[d, n][0:1, 0:1]
             top = jnp.maximum(running, level)
-            r.wgt[d, n] = jnp.where(
-                earlier if d == 0 else later,
-                jnp.exp(jnp.minimum(rows[3 * d : 3 * d + 1] - top, 0.0)) * scale, 0.0,
-            )
-            kept = jnp.where(lane_at == 2 * d, jnp.exp(level - top), kept)
-            kept = jnp.where(lane_at == 2 * d + 1, jnp.exp(-top - decay), kept)
-        r.colw[chunk(n), :] = kept
-        return carry
-
-    lax.fori_loop(0, inner, weight_step, 0)
-    collect(4)
-    for plane_from, chip in peers:
-        other = lax.rem(plane_from, tp) * inner + chip
-        remote(sums, stbuf.at[other], r.sta_s.at[0], r.sta_r.at[other], (o, i, mate)).wait_recv()
-    stbuf[head] = sums[...]
-
-    def stat_step(n, carry):
-        whole = stbuf[0, :, chunk(n)]
-        for k in range(1, MEMORY_HEADS):
-            whole = whole + stbuf[k, :, chunk(n)]
-        whole = whole * (1.0 / channels)
-        mean = whole[0:1]
-        rstd = lax.rsqrt(whole[1:2] - mean * mean + EPS)
-        wide = jnp.concatenate([mean, rstd, jnp.zeros((LANES - 2, block), f32)], axis=0)
-        statc[chunk(n), :] = wide.T
-        return carry
-
-    lax.fori_loop(0, inner, stat_step, 0)
-    actb, memb, cin = r.actb, r.memb, r.cin
-
-    def give(which, source, b):
-        return remote(
-            source.at[chunk(b), :], cin.at[which, i], r.ret_s.at[which, b], r.ret_r.at[which, i],
-            (plane, b, par),
-        )
-
-    def give_own(which, source):
-        return local(source.at[chunk(i), :], cin.at[which, i], r.rel_s.at[which])
-
-    def give_rows(which, source, b):
-        to_self = jnp.logical_and(primary, b == i)
-        guarded(to_self, give_own(which, source).start)
-        guarded(jnp.logical_not(to_self), give(which, source, b).start)
-
-    def turn(step):
-        k = inner - 1 - step
-        flip_x, flip_y = lax.rem(k, 2), lax.div(k, 2)
-        return (y + flip_y - 2 * y * flip_y) * 2 + x + flip_x - 2 * x * flip_x
-
-    def act_step(step, carry):
-        n = turn(step)
-        for half_at in range(2):
-            rows = pl.ds(pl.multiple_of(n * block + half_at * (block // 2), block // 2), block // 2)
-            cols = statc[rows, :]
-            for side in range(sides):
-                lanes = pl.ds(side * LANES, LANES)
-                normal = (conv[side, rows, :] - cols[:, 0:1]) * cols[:, 1:2] * r.lng[:, lanes] + r.lnb[:, lanes]
-                actb[rows, lanes] = (normal * jax.nn.sigmoid(normal)).astype(bf16)
-        give_rows(0, actb, n)
-        return carry
-
-    lax.fori_loop(0, inner, act_step, 0)
-
+            kept += [jnp.exp(running - top), jnp.exp(level - top), jnp.exp(-top - decay)]
+        kept.append(jnp.zeros((LANES - len(kept), block), f32))
+        r.colw[chunk(n), :] = jnp.concatenate(kept, axis=0).T
+        return carry
+
+    lax.fori_loop(0, inner, column_step, 0)
     def memory_step(step, carry):
         n = turn(step)
-        queries = project(n, 4).astype(bf16)
+        queries = r.qb[chunk(n), :]
+        score = lax.dot_general(
+            queries, kb[chunk(n), :], (((1,), (1,)), ((), ())), preferred_element_type=f32
+        )
         wide = queries.astype(f32)
-        scores = lax.dot_general(
-            queries, kb[chunk(n), :], (((1,), (1,)), ((), ())), preferred_element_type=f32
-        )
+        twice = jnp.concatenate([queries, queries], axis=1)
         values = vb[chunk(n), :]
         cols = r.colw[chunk(n), :]
-        out = jnp.zeros((block, HEAD), f32)
+        out = 0.0
         for d in range(2):
-            carry_weight, floor = cols[:, 2 * d : 2 * d + 1], cols[:, 2 * d + 1 : 2 * d + 2]
-            inner_part = scores * r.wgt[d, n]
+            local_weight, carry_weight = cols[:, 3 * d : 3 * d + 1], cols[:, 3 * d + 1 : 3 * d + 2]
+            floor = cols[:, 3 * d + 2 : 3 * d + 3]
+            inner_part = score * r.wgt[d, n]
             num = jnp.dot(inner_part.astype(bf16), values, preferred_element_type=f32)
-            far = jnp.dot(queries, chi[d, n], preferred_element_type=f32)
-            far = far + jnp.dot(queries, clo[d, n], preferred_element_type=f32)
-            den = jnp.sum(inner_part + carry_weight * (wide * nvs[d, n][0:1]), axis=-1, keepdims=True)
+            far = jnp.dot(twice, r.cst[d, n], preferred_element_type=f32)
+            inner_sum = jnp.sum(inner_part, axis=-1, keepdims=True)
+            far_sum = jnp.sum(wide * nvs[d, n][0:1], axis=-1, keepdims=True)
+            den = local_weight * inner_sum + carry_weight * far_sum
             share_of = 1.0 / jnp.maximum(jnp.abs(den), floor)
-            out = out + (num * share_of + far * (carry_weight * share_of))
+            out = out + (num * (local_weight * share_of) + far * (carry_weight * share_of))
         level = lax.rsqrt(jnp.mean(out * out, axis=-1, keepdims=True) + EPS)
         memb[chunk(n), :] = (out * level * r.mgn[...]).astype(bf16)
         give_rows(1, memb, n)
@@ -825,7 +845,7 @@
         smat=pltpu.VMEM((2, HEAD, HEAD), bf16), sinfo=pltpu.VMEM((2, 8, HEAD), f32),
         gmat=pltpu.VMEM((HEAD, HEAD), bf16), ginfo=pltpu.VMEM((8, HEAD), f32),
         gin=pltpu.VMEM((HEAD, HEAD), bf16), gininfo=pltpu.VMEM((8, HEAD), f32),
-        chi=pltpu.VMEM((2, inner, HEAD, HEAD), bf16), clo=pltpu.VMEM((2, inner, HEAD, HEAD), bf16),
+        cst=pltpu.VMEM((2, inner, 2 * HEAD, HEAD), bf16), qb=pltpu.VMEM((quarter, HEAD), bf16),
         wgt=pltpu.VMEM((2, inner, block, block), f32), colw=pltpu.VMEM((quarter, LANES), f32),
         nvs=pltpu.VMEM((2, inner, 8, HEAD), f32), levs=pltpu.VMEM((2, inner, 8, LANES), f32),
         actb=pltpu.VMEM((quarter, HEAD), bf16), memb=pltpu.VMEM((quarter, HEAD), bf16),

time: 113 us -> 101 us (0.89)
  Pallas kernels: 112 us -> 99.7 us
    pallas_call x1, Pallas kernels: 112 us -> 99.7 us  [whole_layer(): pl.pallas_call(functools.partial(layer_kernel, outer, inner, tp, names),...]
where the time goes in v3:
time: 101 us
  Pallas kernels  99.7 us (99%)
    pallas_call x1, Pallas kernels, whole_layer(): pl.pallas_call(functools.partial(layer_kernel, outer, inner, tp, names),...  99.7 us

profile of v3, /device:TPU:0, one launch (start us, length us, event | category | flops | bytes accessed | tf_op | source)
XLA Modules:
  0.0 100.6 jit_solution(13399374983533666499)
XLA Ops:
  0.0 99.7 %shard_map.154 = (bf16[128,2048]{1,0:T(8,128)(2,1)S(1)}, bf16[128,2048]{1,0:T(8,128)(2,1)S(1)}) custom-call(bf16[256,1024]{1,0:T(8,128)(2,1)} %refs_0_.1, f32[1,2048]{1,0:T(1,128)} %bitcast.8, bf16[128,1024]{1,0:T(8,128)(2,1)} %refs_2_.1, bf16[128,1024]{1,0:T(8,128)(2,1)} %refs_3_.1, bf16[128,1024]{1,0:T(8,128)(2,1)} %refs_4_.1, bf16[128,1024]{1,0:T(8,128)(2,1)} %refs_5_.1, ...), custom_call_target="tpu_custom_call" | custom-call | tf_op jit(solution)/shard_map/pallas_call | solution.py:874
  99.7 0.9 add_convert_fusion

commit v4 on v3

--- a/solution.py
+++ b/solution.py
@@ -86,6 +86,10 @@
     own_rows = [local(weights[j], wst.at[j, o], r.own_s.at[j]) for j in range(count)]
     tok_own = local(tokens.at[span(t, hb), :], xin.at[t], r.loc_s.at[0])
     tok_own.start()
+    gain_in = local(norm_gain, r.gain, r.loc_s.at[5])
+    bias_in = local(r.gate_bias, r.bias, r.loc_s.at[6])
+    gain_in.start()
+    bias_in.start()
 
     for copy in own_rows:
         copy.start()
@@ -158,6 +162,70 @@
     def arrived(j, plane):
         remote(wst.at[j, plane], wst.at[j, plane], r.w1_s.at[j, 0], r.w1_r.at[j, plane], (o, i, mate)).wait_recv()
 
+    def row_block(owner_plane, owner):
+        return pl.ds(pl.multiple_of((owner_plane * inner + owner) * depth, depth), depth)
+
+    by_second = (4,)
+
+    def keep(j, plane_at):
+        return local(
+            wst.at[j, plane_at, :, span(i, HEAD)], wfull.at[j, row_block(plane_at, i), :], r.keep_s.at[j]
+        )
+
+    def deal(j, plane_at, k):
+        return remote(
+            wst.at[j, plane_at, :, span(near[k], HEAD)],
+            wfull.at[j, row_block(plane_at, i), :],
+            r.w2_s.at[j], r.w2_r.at[j, plane_at], (o, near[k], mate if j in by_second else t),
+        )
+
+    def deal_planes(j):
+        base = plane_of(1)
+        nearer, farther = base + jnp.where(base < o, 1, 0), base + jnp.where(base < o, 0, 1)
+        at_end = (nearer - o) * (twin - o) > 0
+        return [o, jnp.where(at_end, twin, nearer), farther, jnp.where(at_end, nearer, twin)]
+
+    def deal_all(j, which=None):
+        @pl.when(primary)
+        def _():
+            for index, plane_at in enumerate(deal_planes(j)):
+                if which is not None and index not in which:
+                    continue
+                if index:
+                    arrived(j, plane_at)
+                for k in range(0 if j in by_second else 1, inner):
+                    deal(j, plane_at, k).start()
+                if j not in by_second:
+                    keep(j, plane_at).start()
+
+    def share(j, plane_at):
+        rows = pl.ds(pl.multiple_of(plane_at * inner * depth, inner * depth), inner * depth)
+        return remote(
+            wfull.at[j, rows, :], wfull.at[j, rows, :],
+            r.fw_s.at[j], r.fw_r.at[j], (o, i, mate),
+        )
+
+    def received(ref, semaphore):
+        remote(ref, ref, semaphore, semaphore, (o, i, mate)).wait_recv()
+
+    def collect(j):
+        second = j in by_second
+        collects = jnp.logical_not(primary) if second else primary
+
+        @pl.when(collects)
+        def _():
+            if not second:
+                local(wst.at[j, 0], wst.at[j, 0], r.keep_s.at[j]).wait()
+            for plane_at in deal_planes(j):
+                start_row = pl.multiple_of(plane_at * inner * depth, depth)
+                rows = (inner if second else inner - 1) * depth
+                received(wfull.at[j, pl.ds(start_row, rows), :], r.w2_r.at[j, plane_at])
+                share(j, plane_at).start()
+
+        @pl.when(jnp.logical_not(collects))
+        def _():
+            received(wfull.at[j], r.fw_r.at[j])
+
     small = ((r.conv_taps, r.taps), (r.ln_gain, r.lng), (r.ln_bias, r.lnb), (r.mem_gain, r.mgn))
     own_small = [
         local(a.at[:, span(i, HEAD)], b, r.sml_s.at[k]) for k, (a, b) in enumerate(small)
@@ -188,11 +256,15 @@
         copy = remote(r.extra, ext.at[i], r.ext_s.at[k], r.ext_r.at[i], (plane, near[k], par))
         start(copy, None if k else jnp.logical_not(primary))
 
+    early = 2
+    for j in range(early):
+        deal_all(j, (0,))
     gate_in.start()
     for copy in out_in:
         copy.start()
 
     tok_own.wait()
+    gain_in.wait()
     remote(xin.at[mate], xin.at[mate], r.xin_s, r.xin_r, (o, i, mate)).wait_recv()
     norm_rows = 32
     pieces = 2
@@ -204,7 +276,7 @@
         square = sum(jnp.sum(p * p, axis=-1, keepdims=True) for p in parts)
         level = lax.rsqrt(square * (1.0 / model) + EPS)
         for f in range(tp):
-            row = (parts[f] * level * norm_gain[:, pl.ds(f * half, half)]).astype(bf16)
+            row = (parts[f] * level * r.gain[:, pl.ds(f * half, half)]).astype(bf16)
             nsrc[at, pl.ds(f * half, half)] = row
 
             @pl.when(primary)
@@ -228,101 +300,55 @@
     for j in range(count):
         spread_all(j, 1)
 
-    def row_block(owner_plane, owner):
-        return pl.ds(pl.multiple_of((owner_plane * inner + owner) * depth, depth), depth)
-
-    def deal(j, plane_at, k):
-        return remote(
-            wst.at[j, plane_at, :, span(near[k], HEAD)],
-            wfull.at[j, row_block(plane_at, i), :],
-            r.w2_s.at[j, plane_at, k - 1], r.w2_r.at[j, plane_at, k - 1], (o, near[k], t),
-        )
-
-    def keep(j, plane_at):
-        return local(
-            wst.at[j, plane_at, :, span(i, HEAD)], wfull.at[j, row_block(plane_at, i), :],
-            r.keep_s.at[j, plane_at],
-        )
-
-    def deal_planes(j):
-        bases = [plane_of(step) for step in range(1, groups)]
-        nearer = [base + jnp.where(base < o, 1, 0) for base in bases]
-        farther = [base + jnp.where(base < o, 0, 1) for base in bases]
-        return [o] + nearer + [twin] + farther
-
-    def deal_all(j, which=None):
-        @pl.when(primary)
-        def _():
-            for index, plane_at in enumerate(deal_planes(j)):
-                if which is not None and index not in which:
-                    continue
-                if index:
-                    arrived(j, plane_at)
-                for k in range(1, inner):
-                    deal(j, plane_at, k).start()
-                keep(j, plane_at).start()
-
-    def share(j, plane_at):
-        rows = pl.ds(pl.multiple_of(plane_at * inner * depth, inner * depth), inner * depth)
-        return remote(
-            wfull.at[j, rows, :], wfull.at[j, rows, :],
-            r.fw_s.at[j, plane_at], r.fw_r.at[j, plane_at], (o, i, mate),
-        )
-
-    def collect(j):
-        @pl.when(primary)
-        def _():
-            for plane_at in deal_planes(j):
-                keep(j, plane_at).wait()
-                for k in range(1, inner):
-                    rows = wfull.at[j, row_block(plane_at, near[k]), :]
-                    remote(rows, rows, r.w2_s.at[j, plane_at, k - 1], r.w2_r.at[j, plane_at, k - 1], (o, i, mate)).wait_recv()
-                share(j, plane_at).start()
-
-        @pl.when(jnp.logical_not(primary))
-        def _():
-            for plane_at in deal_planes(j):
-                share(j, plane_at).wait_recv()
-
     def pass_on(b_from, c, s, k, slot):
         rows = rows_of(b_from, c, s)
-        return remote(rows, rows, r.pas_s.at[slot, s], r.tok_r.at[b_from, c, s], (o, near[k], t))
+        target = near[k] if isinstance(k, int) else jnp.where(k == 1, near[1], near[2])
+        return remote(rows, rows, r.pas_s, r.tok_r.at[b_from, c, s], (o, target, t))
 
     @pl.when(primary)
     def _():
         for s in range(pieces):
-            for c, slot in ((t, 0), (mate, 2)):
-                if slot:
-                    tok_wait(i, c, s)
-                pass_on(i, c, s, 1, slot).start()
-                pass_on(i, c, s, 2, slot + 1).start()
+            pass_on(i, t, s, 1 + t, 0).start()
+        for s in range(pieces):
+            tok_wait(i, mate, s)
+            pass_on(i, mate, s, 1 + mate, 1).start()
+        for s in range(pieces):
+            pass_on(i, t, s, 1 + mate, 2).start()
+            pass_on(i, mate, s, 1 + t, 3).start()
 
     @pl.when(jnp.logical_not(primary))
     def _():
         for s in range(pieces):
-            for c, slot in ((t, 0), (mate, 2)):
+            for c, slot in ((0, 0), (1, 1)):
                 tok_wait(i, c, s)
-                pass_on(i, c, s, 1, slot).start()
-                pass_on(i, c, s, 2, slot + 1).start()
+                pass_on(i, c, s, 1 + c, slot).start()
+        for s in range(pieces):
+            for c, slot in ((0, 2), (1, 3)):
+                pass_on(i, c, s, 2 - c, slot).start()
 
     for s in range(pieces):
         tok_wait(near[1], 0, s)
-        start(pass_on(near[1], 0, s, 2, 4))
+        pass_on(near[1], 0, s, 2, 4).start()
         tok_wait(near[2], 1, s)
-        start(pass_on(near[2], 1, s, 1, 5))
+        pass_on(near[2], 1, s, 1, 5).start()
     for j in range(count):
         spread_all(j, 2)
+    received(nq.at[pl.ds(0, (inner - 1) * block), :], r.pas_s)
+
+    @pl.when(jnp.logical_not(primary))
+    def _():
+        pl.semaphore_signal(r.clear, inc=1, device_id=(o, i, mate), device_id_type=MESH)
+
     for s in range(pieces):
         tok_wait(near[1], 1, s)
         tok_wait(near[2], 0, s)
         tok_wait(near[3], 0, s)
         tok_wait(near[3], 1, s)
 
-    deal_all(0)
-    deal_all(1)
-
     gwp, gt, rowsv, colsv = r.gwp, r.gt, r.rowsv, r.colsv
     gate_in.wait()
+    bias_in.wait()
+    bias_row = jnp.concatenate([r.bias[...], jnp.zeros((1, LANES - r.bias.shape[1]), f32)], axis=1)
 
     def chunk(n):
         return span(n, block)
@@ -331,7 +357,7 @@
         got = lax.dot_general(
             nq[chunk(n), :], gwp[...], (((1,), (1,)), ((), ())), preferred_element_type=f32
         )
-        gt[:, chunk(n)] = got.T[: gt.shape[0]]
+        gt[:, chunk(n)] = (got + bias_row).T[: gt.shape[0]]
         return carry
 
     lax.fori_loop(0, inner, gate_step, 0)
@@ -349,7 +375,7 @@
 
     def gate_row(g):
         rows = gt[pl.ds(g * MEMORY_HEADS, MEMORY_HEADS), :]
-        return jnp.sum(jnp.where(mine, rows, 0.0), axis=0, keepdims=True) + r.gate_bias[g * MEMORY_HEADS + head]
+        return jnp.sum(jnp.where(mine, rows, 0.0), axis=0, keepdims=True)
 
     def extra_row(d):
         pieces = [
@@ -400,22 +426,26 @@
     gmat, ginfo, gin, gininfo = r.gmat, r.ginfo, r.gin, r.gininfo
 
     def key_step(n, carry):
-        kb[chunk(n), :] = project(n, 2).astype(bf16)
-        return carry
-
-    def state_step(n, carry):
-        values = project(n, 3).astype(bf16)
-        vb[chunk(n), :] = values
-        keys = kb[chunk(n), :].astype(f32)
+        keys = project(n, 2)
+        kb[chunk(n), :] = keys.astype(bf16)
+        wide = keys.astype(bf16).astype(f32)
         cols = colsv[chunk(n), :]
         for d in range(2):
             end = block - 1 if d == 0 else 0
             top = cols[end : end + 1, 3 * d + 1 : 3 * d + 2]
-            weighted = keys * (jnp.exp(cols[:, 3 * d : 3 * d + 1] - top) * scale)
-            cm[d, n] = lax.dot_general(
-                weighted.astype(bf16), values, (((0,), (0,)), ((), ())), preferred_element_type=f32
-            )
+            weighted = wide * (jnp.exp(cols[:, 3 * d : 3 * d + 1] - top) * scale)
+            r.kwt[d, :, chunk(n)] = weighted.T.astype(bf16)
             cv[d, n] = jnp.broadcast_to(jnp.sum(weighted, axis=0, keepdims=True), (8, HEAD))
+        return carry
+
+    def state_step(m, carry):
+        ns = [m * 2 + p for p in range(2)]
+        values = [project(n, 3).astype(bf16) for n in ns]
+        for n, value in zip(ns, values):
+            vb[chunk(n), :] = value
+        for n, value in zip(ns, values):
+            for d in range(2):
+                cm[d, n] = jnp.dot(r.kwt[d, :, chunk(n)], value, preferred_element_type=f32)
         return carry
 
     earlier = lax.broadcasted_iota(jnp.int32, (block, block), 0) >= lax.broadcasted_iota(jnp.int32, (block, block), 1)
@@ -430,6 +460,14 @@
         return carry
 
     lax.fori_loop(0, inner, weight_step, 0)
+    @pl.when(primary)
+    def _():
+        pl.semaphore_wait(r.clear, 1)
+
+    deal_all(0, range(1, outer))
+    deal_all(1, range(1, outer))
+    deal_all(2, range(2))
+
     collect(0)
     gpad, conv, hsend, hrecv = r.gpad, r.conv, r.hsend, r.hrecv
     pad = hsend.shape[1]
@@ -441,7 +479,8 @@
         return carry
 
     lax.fori_loop(0, inner, value_step, 0)
-    deal_all(2)
+    deal_all(2, range(2, outer))
+    deal_all(3, range(2))
     collect(1)
 
     def glu_step(n, carry):
@@ -477,7 +516,7 @@
         for copy in mate_small:
             copy.wait_recv()
 
-    deal_all(3, range(2))
+    deal_all(3, range(2, outer))
     taps, statc, stbuf = r.taps, r.statc, r.stbuf
     conv_rows = 64
     lane = lax.broadcasted_iota(jnp.int32, (conv_rows, LANES), 1)
@@ -504,9 +543,9 @@
 
     conv_steps = quarter // conv_rows
     lax.fori_loop(1, conv_steps // 2, conv_step, 0)
+    deal_all(4, range(2))
     collect(2)
     lax.fori_loop(conv_steps // 2, conv_steps - 1, conv_step, 0)
-    deal_all(3, range(2, outer))
     for edge, present, at in ((0, has_before, 0), (1, has_after, pad + quarter)):
         @pl.when(present)
         def _():
@@ -534,14 +573,11 @@
             if (dz, k) != (0, 0):
                 peers.append((o if dz == 0 else twin, near[k]))
     for index, (plane_to, chip) in enumerate(peers):
-        start(remote(sums.at[two, :], stbuf.at[head, two, :], r.sta_s.at[index], r.sta_r.at[head], (plane_to, chip, t)))
+        remote(sums.at[two, :], stbuf.at[head, two, :], r.sta_s, r.sta_r, (plane_to, chip, t)).start()
+    deal_all(4, range(2, outer))
     lax.fori_loop(0, inner, key_step, 0)
-    deal_all(4, range(2))
     collect(3)
-    deal_all(4, (2,))
     lax.fori_loop(0, inner // 2, state_step, 0)
-    deal_all(4, range(3, outer))
-    lax.fori_loop(inner // 2, inner, state_step, 0)
 
     def corner(n, d, column):
         end = block - 1 if d == 0 else 0
@@ -568,9 +604,7 @@
 
     start(remote(matx, smat, r.mat_s.at[0], r.mat_r.at[0], (o, i, mate)))
     start(remote(infox, sinfo, r.inf_s.at[0], r.inf_r.at[0], (o, i, mate)))
-    for plane_from, chip in peers:
-        other = lax.rem(plane_from, tp) * inner + chip
-        remote(sums.at[two, :], stbuf.at[other, two, :], r.sta_s.at[0], r.sta_r.at[other], (o, i, mate)).wait_recv()
+    received(stbuf.at[pl.ds(0, MEMORY_HEADS - 1), two, :], r.sta_r)
     stbuf[head] = sums[...]
 
     def stat_step(n, carry):
@@ -636,29 +670,13 @@
     start(remote(ginfo, gininfo, r.inf_s.at[1], r.inf_r.at[1], across))
     for k in range(inner - 1, -1, -1):
         give_rows(0, actb, near[k])
-    collect(4)
-
-    def query_step(n, carry):
-        r.qb[chunk(n), :] = project(n, 4).astype(bf16)
-        return carry
-
-    lax.fori_loop(0, inner, query_step, 0)
-    remote(mat_rows, mat_rows, r.mat_s.at[1], r.mat_r.at[1], (o, i, mate)).wait_recv()
-    start(remote(mat_rows, mat_rows, r.mat_s.at[2], r.mat_r.at[2], (o, i, mate)))
-    remote(ginfo, gininfo, r.inf_s.at[1], r.inf_r.at[1], (o, i, mate)).wait_recv()
-    remote(mate_rows, mate_rows, r.mat_s.at[2], r.mat_r.at[2], (o, i, mate)).wait_recv()
-
     nvs, levs = r.nvs, r.levs
     for d in range(2):
-        by_mate, by_group = t == 1 - d, grp == 1 - d
-        near_reach = jnp.where(by_mate, sinfo[d][1:2, 0:1], LOW_START)
-        far_reach = gininfo[1:2, 0:1] + jnp.where(by_mate, sinfo[d][2:3, 0:1], 0.0)
-        far_reach = jnp.where(by_group, far_reach, LOW_START)
-        level = jnp.maximum(near_reach, far_reach)
-        near_share = jnp.where(by_mate, jnp.exp(near_reach - level), 0.0)
-        far_share = jnp.where(by_group, jnp.exp(far_reach - level), 0.0)
-        mat = near_share * smat[d].astype(f32) + far_share * gin[...].astype(f32)
-        vec = near_share * sinfo[d][0:1] + far_share * gininfo[0:1]
+        by_mate = t == 1 - d
+        level = jnp.where(by_mate, sinfo[d][1:2, 0:1], LOW_START)
+        present = jnp.where(by_mate, 1.0, 0.0)
+        mat = present * smat[d].astype(f32)
+        vec = present * sinfo[d][0:1]
         for n in (range(inner) if d == 0 else range(inner - 1, -1, -1)):
             high = mat.astype(bf16)
             r.cst[d, n, pl.ds(0, HEAD), :] = high
@@ -672,63 +690,102 @@
             vec = kept * vec + added * cv[d, n][0:1]
             level = new_level
 
-    def column_step(n, carry):
-        rows = rowsv[:, chunk(n)]
-        kept = []
-        for d in range(2):
-            running, decay = rows[3 * d + 1 : 3 * d + 2], rows[3 * d + 2 : 3 * d + 3]
-            level = levs[d, n][0:1, 0:1]
-            top = jnp.maximum(running, level)
-            kept += [jnp.exp(running - top), jnp.exp(level - top), jnp.exp(-top - decay)]
-        kept.append(jnp.zeros((LANES - len(kept), block), f32))
-        r.colw[chunk(n), :] = jnp.concatenate(kept, axis=0).T
-        return carry
-
-    lax.fori_loop(0, inner, column_step, 0)
-    def memory_step(step, carry):
-        n = turn(step)
-        queries = r.qb[chunk(n), :]
-        score = lax.dot_general(
-            queries, kb[chunk(n), :], (((1,), (1,)), ((), ())), preferred_element_type=f32
-        )
-        wide = queries.astype(f32)
-        twice = jnp.concatenate([queries, queries], axis=1)
-        values = vb[chunk(n), :]
-        cols = r.colw[chunk(n), :]
-        out = 0.0
-        for d in range(2):
-            local_weight, carry_weight = cols[:, 3 * d : 3 * d + 1], cols[:, 3 * d + 1 : 3 * d + 2]
-            floor = cols[:, 3 * d + 2 : 3 * d + 3]
-            inner_part = score * r.wgt[d, n]
-            num = jnp.dot(inner_part.astype(bf16), values, preferred_element_type=f32)
-            far = jnp.dot(twice, r.cst[d, n], preferred_element_type=f32)
-            inner_sum = jnp.sum(inner_part, axis=-1, keepdims=True)
-            far_sum = jnp.sum(wide * nvs[d, n][0:1], axis=-1, keepdims=True)
-            den = local_weight * inner_sum + carry_weight * far_sum
-            share_of = 1.0 / jnp.maximum(jnp.abs(den), floor)
-            out = out + (num * (local_weight * share_of) + far * (carry_weight * share_of))
-        level = lax.rsqrt(jnp.mean(out * out, axis=-1, keepdims=True) + EPS)
-        memb[chunk(n), :] = (out * level * r.mgn[...]).astype(bf16)
-        give_rows(1, memb, n)
-        return carry
-
-    lax.fori_loop(0, inner, memory_step, 0)
+    first_group = grp == 0
+
+    def along(values):
+        return jnp.concatenate([jnp.broadcast_to(v, (1, block)) for v in values], axis=1)
+
+    kept, tops = [], []
+    for d in range(2):
+        running, decay = rowsv[pl.ds(3 * d + 1, 1), :], rowsv[pl.ds(3 * d + 2, 1), :]
+        level = along([levs[d, n][0:1, 0:1] for n in range(inner)])
+        top = jnp.maximum(running, level)
+        tops.append((top, decay))
+        kept.append([jnp.exp(running - top), jnp.exp(level - top), jnp.exp(-top - decay)])
+    alone = [jnp.where(first_group, a, b) for a, b in zip(*kept)]
+    joined = [jnp.where(first_group, b, a) for a, b in zip(*kept)]
+    joined_top, joined_decay = (jnp.where(first_group, b, a) for a, b in zip(*tops))
+    r.colw[:, pl.ds(0, 8)] = jnp.concatenate(alone + joined + [jnp.zeros((2, quarter), f32)], axis=0).T
+    collect(4)
+
+    pair = 2
+
+    def query_step(m, carry):
+        ns = [m * pair + p for p in range(pair)]
+        queries = [project(n, 4).astype(bf16) for n in ns]
+        scores = [
+            lax.dot_general(q, kb[chunk(n), :], (((1,), (1,)), ((), ())), preferred_element_type=f32)
+            for n, q in zip(ns, queries)
+        ]
+        for n, q in zip(ns, queries):
+            r.qb[chunk(n), :] = q
+        for role, d in ((0, grp), (1, 1 - grp)):
+            for n, q, score in zip(ns, queries, scores):
+                cols = r.colw[chunk(n), :]
+                local_weight, carry_weight = cols[:, 3 * role : 3 * role + 1], cols[:, 3 * role + 1 : 3 * role + 2]
+                part = score * r.wgt[d, n]
+                num = jnp.dot(part.astype(bf16), vb[chunk(n), :], preferred_element_type=f32)
+                far = jnp.dot(jnp.concatenate([q, q], axis=1), r.cst[d, n], preferred_element_type=f32)
+                num = local_weight * num + carry_weight * far
+                far_sum = jnp.sum(q.astype(f32) * nvs[d, n][0:1], axis=-1, keepdims=True)
+                den = local_weight * jnp.sum(part, axis=-1, keepdims=True) + carry_weight * far_sum
+                if role == 0:
+                    r.alone[chunk(n), :] = num * (1.0 / jnp.maximum(jnp.abs(den), cols[:, 2:3]))
+                else:
+                    r.numj[chunk(n), :] = num
+                    r.denj[chunk(n), :] = jnp.broadcast_to(den, (block, LANES))
+        return carry
+
+    lax.fori_loop(0, inner // pair // 2, query_step, 0)
+    remote(mat_rows, mat_rows, r.mat_s.at[1], r.mat_r.at[1], (o, i, mate)).wait_recv()
+    start(remote(mat_rows, mat_rows, r.mat_s.at[2], r.mat_r.at[2], (o, i, mate)))
+    lax.fori_loop(inner // pair // 2, inner // pair, query_step, 0)
+    remote(ginfo, gininfo, r.inf_s.at[1], r.inf_r.at[1], (o, i, mate)).wait_recv()
+    remote(mate_rows, mate_rows, r.mat_s.at[2], r.mat_r.at[2], (o, i, mate)).wait_recv()
+
+    arriving = gininfo[1:2, 0:1] + jnp.where(t == grp, sinfo[1 - grp][2:3, 0:1], 0.0)
+    group_levels = []
+    for n in range(inner):
+        lost_f = functools.reduce(jnp.add, totals[0][:n], jnp.zeros((1, 1), f32))
+        lost_b = functools.reduce(jnp.add, totals[1][n + 1 :], jnp.zeros((1, 1), f32))
+        group_levels.append(arriving + jnp.where(first_group, lost_b, lost_f))
+    level = along(group_levels)
+    top = jnp.maximum(joined_top, level)
+    kept = [jnp.exp(joined_top - top), jnp.exp(level - top), jnp.exp(-top - joined_decay)]
+    r.colw[:, pl.ds(0, 8)] = jnp.concatenate(kept + [jnp.zeros((5, quarter), f32)], axis=0).T
+
+    def memory_rows(ns):
+        queries = [r.qb[chunk(n), :] for n in ns]
+        fars = [jnp.dot(q, gin[...], preferred_element_type=f32) for q in queries]
+        far_sums = [jnp.sum(q.astype(f32) * gininfo[0:1], axis=-1, keepdims=True) for q in queries]
+        for n, far, far_sum in zip(ns, fars, far_sums):
+            cols = r.colw[chunk(n), :]
+            den = cols[:, 0:1] * r.denj[chunk(n), pl.ds(0, 1)] + cols[:, 1:2] * far_sum
+            share_of = 1.0 / jnp.maximum(jnp.abs(den), cols[:, 2:3])
+            out = r.alone[chunk(n), :] + (
+                r.numj[chunk(n), :] * (cols[:, 0:1] * share_of) + far * (cols[:, 1:2] * share_of)
+            )
+            level = lax.rsqrt(jnp.mean(out * out, axis=-1, keepdims=True) + EPS)
+            memb[chunk(n), :] = (out * level * r.mgn[...]).astype(bf16)
+        for n in ns:
+            give_rows(1, memb, n)
+
+    for ns in ([near[3]], [near[2]], [near[1], near[0]]):
+        memory_rows(ns)
     acc, pbuf = r.acc, r.pbuf
     tile = 512
     tiles = model // tile
 
-    def own_sender(which):
-        return local(actb.at[chunk(i), :], cin.at[which, i], r.rel_s.at[which])
-
-    def take(which):
-        for k in range(inner):
-            def hear(k=k):
-                remote(actb.at[chunk(0), :], cin.at[which, near[k]], r.ret_s.at[which, 0], r.ret_r.at[which, near[k]], (o, i, mate)).wait_recv()
-            if k:
-                hear()
-            else:
-                guarded(jnp.logical_not(primary), hear)
-                guarded(primary, own_sender(which).wait)
+    def take(which, k):
+        def hear():
+            rows = cin.at[which, near[k]]
+            remote(rows, rows, r.ret_s.at[which, 0], r.ret_r.at[which, near[k]], (o, i, mate)).wait_recv()
+
+        if k:
+            hear()
+        else:
+            guarded(jnp.logical_not(primary), hear)
+            guarded(primary, give_own(which, actb).wait)
 
     def part(which, n):
         return sum(
@@ -742,24 +799,38 @@
 
     for copy in out_in:
         copy.wait()
-    take(0)
+    for k in range(inner):
+        take(0, k)
     lax.fori_loop(0, tiles, conv_out_step, 0)
 
-    take(1)
-
+    def add_step(k):
+        def step(n, carry):
+            rows = pl.ds(pl.multiple_of(near[k] * HEAD, HEAD), HEAD)
+            acc[:, span(n, tile)] += jnp.dot(
+                cin[1, near[k]], ow[1, rows, span(n, tile)], preferred_element_type=f32
+            )
+            return carry
+        return step
+
+    for k in range(inner - 1, 0, -1):
+        take(1, k)
+        lax.fori_loop(0, tiles, add_step(k), 0)
+    take(1, 0)
     out_own, out_mate = r.out_own, r.out_mate
 
     def piece(n):
         return remote(
             pbuf.at[span(mate, hb), span(n, tile)], out_mate.at[:, span(n, tile)],
-            r.fin_s.at[n], r.fin_r.at[n], (o, i, mate),
+            r.fin_s, r.fin_r, (o, i, mate),
         )
 
     def stay(n):
-        return local(pbuf.at[span(t, hb), span(n, tile)], out_own.at[:, span(n, tile)], r.fil_s.at[n])
+        return local(pbuf.at[span(t, hb), span(n, tile)], out_own.at[:, span(n, tile)], r.fil_s)
 
     def mem_out_step(n, carry):
-        pbuf[:, span(n, tile)] = (acc[:, span(n, tile)] + part(1, n)).astype(bf16)
+        rows = pl.ds(pl.multiple_of(i * HEAD, HEAD), HEAD)
+        rest = jnp.dot(cin[1, i], ow[1, rows, span(n, tile)], preferred_element_type=f32)
+        pbuf[:, span(n, tile)] = (acc[:, span(n, tile)] + rest).astype(bf16)
         piece(n).start()
         stay(n).start()
         return carry
@@ -772,27 +843,29 @@
         else:
             pl.when(when)(copy.wait_send)
 
-    for s in range(pieces):
-        for c, slot in ((t, 0), (mate, 2)):
-            pass_on(i, c, s, 1, slot).wait_send()
-            pass_on(i, c, s, 2, slot + 1).wait_send()
+
+    received(stbuf.at[pl.ds(0, MEMORY_HEADS - 1), two, :], r.sta_s)
 
     @pl.when(primary)
     def _():
         for copy in mate_small:
             copy.wait_send()
         for j in range(count):
-            for plane_at in deal_planes(j):
-                for k in range(1, inner):
-                    deal(j, plane_at, k).wait_send()
-                share(j, plane_at).wait_send()
+            received(wst.at[j] if j in by_second else wst.at[j, pl.ds(0, inner - 1)], r.w2_s.at[j])
+            if j not in by_second:
+                received(wfull.at[j], r.fw_s.at[j])
+
+    @pl.when(jnp.logical_not(primary))
+    def _():
+        for j in by_second:
+            received(wfull.at[j], r.fw_s.at[j])
 
     for which, source in ((0, actb), (1, memb)):
         for b in range(inner):
             guarded(jnp.logical_not(jnp.logical_and(primary, i == b)), give(which, source, b).wait_send)
-    for n in range(tiles):
-        stay(n).wait()
-        piece(n).wait()
+    local(out_own, out_own, r.fil_s).wait()
+    received(out_mate, r.fin_s)
+    received(out_mate, r.fin_r)
 
 
 LANES = 128
@@ -816,7 +889,7 @@
         glu_value=args.glu_value, glu_gate=args.glu_gate,
         key_weight=args.key_weight, value_weight=args.value_weight, query_weight=args.query_weight,
         conv_taps=args.conv_taps, ln_gain=args.ln_gain[None], ln_bias=args.ln_bias[None],
-        gate_weight=args.gate_weight.T, gate_bias=args.gate_bias,
+        gate_weight=args.gate_weight.T, gate_bias=args.gate_bias[None],
         extra=extra, mem_gain=args.mem_gain[None],
         out_conv=args.out_conv, out_mem=args.out_mem,
     )
@@ -832,6 +905,7 @@
         lnb=pltpu.VMEM((1, HEAD), f32), mgn=pltpu.VMEM((1, HEAD), f32),
         ext=pltpu.VMEM((inner,) + extra.shape, f32),
         gwp=pltpu.VMEM((LANES, model), bf16),
+        gain=pltpu.VMEM((1, model), f32), bias=pltpu.VMEM((1, 4 * MEMORY_HEADS), f32),
         gt=pltpu.VMEM((4 * MEMORY_HEADS, quarter), f32),
         rowsv=pltpu.VMEM((8, quarter), f32), colsv=pltpu.VMEM((quarter, LANES), f32),
         gpad=pltpu.VMEM((HEAD // LANES, quarter + 2 * pad, LANES), f32),
@@ -845,37 +919,35 @@
         smat=pltpu.VMEM((2, HEAD, HEAD), bf16), sinfo=pltpu.VMEM((2, 8, HEAD), f32),
         gmat=pltpu.VMEM((HEAD, HEAD), bf16), ginfo=pltpu.VMEM((8, HEAD), f32),
         gin=pltpu.VMEM((HEAD, HEAD), bf16), gininfo=pltpu.VMEM((8, HEAD), f32),
-        cst=pltpu.VMEM((2, inner, 2 * HEAD, HEAD), bf16), qb=pltpu.VMEM((quarter, HEAD), bf16),
+        cst=pltpu.VMEM((2, inner, 2 * HEAD, HEAD), bf16), qb=pltpu.VMEM((quarter, HEAD), bf16), kwt=pltpu.VMEM((2, HEAD, quarter), bf16),
+        alone=pltpu.VMEM((quarter, HEAD), f32), numj=pltpu.VMEM((quarter, HEAD), f32), denj=pltpu.VMEM((quarter, LANES), f32),
         wgt=pltpu.VMEM((2, inner, block, block), f32), colw=pltpu.VMEM((quarter, LANES), f32),
         nvs=pltpu.VMEM((2, inner, 8, HEAD), f32), levs=pltpu.VMEM((2, inner, 8, LANES), f32),
         actb=pltpu.VMEM((quarter, HEAD), bf16), memb=pltpu.VMEM((quarter, HEAD), bf16),
         cin=pltpu.VMEM((2, inner, block, HEAD), bf16),
         acc=pltpu.VMEM((block, model), f32), pbuf=pltpu.VMEM((block, model), bf16),
-        own_s=dma((count,)), mov_s=dma((2,)), mov_r=dma((2,)), mvd_s=dma((2,)), loc_s=dma((5,)), xin_s=dma, xin_r=dma,
+        own_s=dma((count,)), mov_s=dma((2,)), mov_r=dma((2,)), mvd_s=dma((2,)), loc_s=dma((7,)), xin_s=dma, xin_r=dma,
         w1_s=dma((count, outer // tp)), w1_r=dma((count, outer)),
         sml_s=dma((4,)), prm_s=dma((4,)), prm_r=dma((4,)),
         ext_s=dma((inner,)), ext_r=dma((inner,)),
-        tok_s=dma((2, 2)), tok_r=dma((inner, tp, 2)), pas_s=dma((6, 2)),
-        w2_s=dma((count, outer, inner - 1)), w2_r=dma((count, outer, inner - 1)),
-        keep_s=dma((count, outer)), fw_s=dma((count, outer)), fw_r=dma((count, outer)),
+        tok_s=dma((2, 2)), tok_r=dma((inner, tp, 2)), pas_s=dma, clear=pltpu.SemaphoreType.REGULAR,
+        w2_s=dma((count,)), w2_r=dma((count, outer)),
+        keep_s=dma((count,)), fw_s=dma((count,)), fw_r=dma((count,)),
         hal_s=dma((2,)), hal_r=dma((2,)),
-        sta_s=dma((MEMORY_HEADS,)), sta_r=dma((MEMORY_HEADS,)),
+        sta_s=dma, sta_r=dma,
         mat_s=dma((3,)), mat_r=dma((3,)), inf_s=dma((2,)), inf_r=dma((2,)),
         ret_s=dma((2, inner)), ret_r=dma((2, inner)), rel_s=dma((2,)),
-        fin_s=dma((tiles,)), fin_r=dma((tiles,)), fil_s=dma((tiles,)),
+        fin_s=dma, fin_r=dma, fil_s=dma,
     )
     any_space = pl.BlockSpec(memory_space=pl.ANY)
     spaces = {n: any_space for n in operands}
-    spaces.update(
-        gate_bias=pl.BlockSpec(memory_space=pltpu.SMEM), norm_gain=pl.BlockSpec(memory_space=pltpu.VMEM)
-    )
     names = list(operands) + ["out_own", "out_mate"] + list(scratch)
     shape = pltpu.VMEM((hb, model), bf16)
     own, mate = pl.pallas_call(
         functools.partial(layer_kernel, outer, inner, tp, names),
         out_shape=(shape, shape),
         in_specs=[spaces[n] for n in operands],
-        out_specs=(pl.BlockSpec(memory_space=pltpu.VMEM),) * 2,
+        out_specs=(any_space, any_space),
         scratch_shapes=list(scratch.values()),
         compiler_params=pltpu.CompilerParams(
             collective_id=0, has_side_effects=True, vmem_limit_bytes=60 * 2**20

time: 101 us -> 95.7 us (0.948)
  Pallas kernels: 99.7 us -> 94.7 us
    pallas_call x1, Pallas kernels: 99.7 us -> 94.7 us  [whole_layer(): pl.pallas_call(functools.partial(layer_kernel, outer, inner, tp, names),...]
where the time goes in v4:
time: 95.7 us; the launch traced here: 95.6 us
  Pallas kernels  94.7 us (99%)
    pallas_call x1, Pallas kernels, whole_layer(): pl.pallas_call(functools.partial(layer_kernel, outer, inner, tp, names),...  94.7 us

profile of v4, /device:TPU:0, one launch (start us, length us, event | category | flops | bytes accessed | tf_op | source)
XLA Modules:
  0.0 95.6 jit_solution(9419820717381624821)
XLA Ops:
  0.0 94.7 %shard_map.154 = (bf16[128,2048]{1,0:T(8,128)(2,1)S(1)}, bf16[128,2048]{1,0:T(8,128)(2,1)S(1)}) custom-call(bf16[256,1024]{1,0:T(8,128)(2,1)} %refs_0_.1, f32[1,2048]{1,0:T(1,128)} %bitcast.9, bf16[128,1024]{1,0:T(8,128)(2,1)} %refs_2_.1, bf16[128,1024]{1,0:T(8,128)(2,1)} %refs_3_.1, bf16[128,1024]{1,0:T(8,128)(2,1)} %refs_4_.1, bf16[128,1024]{1,0:T(8,128)(2,1)} %refs_5_.1, ...), custom_call_target="tpu_custom_call" | custom-call | tf_op jit(solution)/shard_map/pallas_call | solution.py:946
  94.7 0.9 add_convert_fusion

commit v5 on v4

--- a/solution.py
+++ b/solution.py
@@ -208,23 +208,29 @@
     def received(ref, semaphore):
         remote(ref, ref, semaphore, semaphore, (o, i, mate)).wait_recv()
 
-    def collect(j):
+    def gather(j, which=None):
         second = j in by_second
-        collects = jnp.logical_not(primary) if second else primary
-
-        @pl.when(collects)
+
+        @pl.when(jnp.logical_not(primary) if second else primary)
         def _():
-            if not second:
+            if not second and (which is None or 0 in which):
                 local(wst.at[j, 0], wst.at[j, 0], r.keep_s.at[j]).wait()
-            for plane_at in deal_planes(j):
+            for index, plane_at in enumerate(deal_planes(j)):
+                if which is not None and index not in which:
+                    continue
                 start_row = pl.multiple_of(plane_at * inner * depth, depth)
                 rows = (inner if second else inner - 1) * depth
                 received(wfull.at[j, pl.ds(start_row, rows), :], r.w2_r.at[j, plane_at])
                 share(j, plane_at).start()
 
-        @pl.when(jnp.logical_not(collects))
+    def handed(j):
+        @pl.when(primary if j in by_second else jnp.logical_not(primary))
         def _():
             received(wfull.at[j], r.fw_r.at[j])
+
+    def collect(j, which=None):
+        gather(j, which)
+        handed(j)
 
     small = ((r.conv_taps, r.taps), (r.ln_gain, r.lng), (r.ln_bias, r.lnb), (r.mem_gain, r.mgn))
     own_small = [
@@ -575,8 +581,9 @@
     for index, (plane_to, chip) in enumerate(peers):
         remote(sums.at[two, :], stbuf.at[head, two, :], r.sta_s, r.sta_r, (plane_to, chip, t)).start()
     deal_all(4, range(2, outer))
+    gather(3, range(2))
     lax.fori_loop(0, inner, key_step, 0)
-    collect(3)
+    collect(3, range(2, outer))
     lax.fori_loop(0, inner // 2, state_step, 0)
 
     def corner(n, d, column):
@@ -604,6 +611,7 @@
 
     start(remote(matx, smat, r.mat_s.at[0], r.mat_r.at[0], (o, i, mate)))
     start(remote(infox, sinfo, r.inf_s.at[0], r.inf_r.at[0], (o, i, mate)))
+    gather(4, range(2))
     received(stbuf.at[pl.ds(0, MEMORY_HEADS - 1), two, :], r.sta_r)
     stbuf[head] = sums[...]
 
@@ -635,10 +643,7 @@
         guarded(to_self, give_own(which, source).start)
         guarded(jnp.logical_not(to_self), give(which, source, b).start)
 
-    def turn(step):
-        k = inner - 1 - step
-        flip_x, flip_y = lax.rem(k, 2), lax.div(k, 2)
-        return (y + flip_y - 2 * y * flip_y) * 2 + x + flip_x - 2 * x * flip_x
+    order = [jnp.where(primary, near[a], near[b]) for a, b in zip((1, 2, 3, 0), (2, 1, 3, 0))]
 
     def act_step(n, carry):
         for half_at in range(2):
@@ -668,8 +673,9 @@
     across = ((1 - grp) * tp + par, i, t)
     start(remote(gmat.at[span(t, HEAD // tp), :], mat_rows, r.mat_s.at[1], r.mat_r.at[1], across))
     start(remote(ginfo, gininfo, r.inf_s.at[1], r.inf_r.at[1], across))
-    for k in range(inner - 1, -1, -1):
-        give_rows(0, actb, near[k])
+    for b in order:
+        give_rows(0, actb, b)
+    gather(4, range(2, outer))
     nvs, levs = r.nvs, r.levs
     for d in range(2):
         by_mate = t == 1 - d
@@ -706,12 +712,10 @@
     joined = [jnp.where(first_group, b, a) for a, b in zip(*kept)]
     joined_top, joined_decay = (jnp.where(first_group, b, a) for a, b in zip(*tops))
     r.colw[:, pl.ds(0, 8)] = jnp.concatenate(alone + joined + [jnp.zeros((2, quarter), f32)], axis=0).T
-    collect(4)
-
-    pair = 2
-
-    def query_step(m, carry):
-        ns = [m * pair + p for p in range(pair)]
+    handed(4)
+
+
+    def query_rows(ns):
         queries = [project(n, 4).astype(bf16) for n in ns]
         scores = [
             lax.dot_general(q, kb[chunk(n), :], (((1,), (1,)), ((), ())), preferred_element_type=f32)
@@ -734,12 +738,12 @@
                 else:
                     r.numj[chunk(n), :] = num
                     r.denj[chunk(n), :] = jnp.broadcast_to(den, (block, LANES))
-        return carry
-
-    lax.fori_loop(0, inner // pair // 2, query_step, 0)
+
+    query_rows([0, 1])
+    query_rows([2])
     remote(mat_rows, mat_rows, r.mat_s.at[1], r.mat_r.at[1], (o, i, mate)).wait_recv()
     start(remote(mat_rows, mat_rows, r.mat_s.at[2], r.mat_r.at[2], (o, i, mate)))
-    lax.fori_loop(inner // pair // 2, inner // pair, query_step, 0)
+    query_rows([3])
     remote(ginfo, gininfo, r.inf_s.at[1], r.inf_r.at[1], (o, i, mate)).wait_recv()
     remote(mate_rows, mate_rows, r.mat_s.at[2], r.mat_r.at[2], (o, i, mate)).wait_recv()
 
@@ -770,7 +774,7 @@
         for n in ns:
             give_rows(1, memb, n)
 
-    for ns in ([near[3]], [near[2]], [near[1], near[0]]):
+    for ns in ([order[0]], [order[1]], [order[2], order[3]]):
         memory_rows(ns)
     acc, pbuf = r.acc, r.pbuf
     tile = 512
@@ -803,18 +807,23 @@
         take(0, k)
     lax.fori_loop(0, tiles, conv_out_step, 0)
 
-    def add_step(k):
-        def step(n, carry):
-            rows = pl.ds(pl.multiple_of(near[k] * HEAD, HEAD), HEAD)
-            acc[:, span(n, tile)] += jnp.dot(
-                cin[1, near[k]], ow[1, rows, span(n, tile)], preferred_element_type=f32
+    def rows_part(ks, n):
+        return sum(
+            jnp.dot(
+                cin[1, near[k]], ow[1, pl.ds(pl.multiple_of(near[k] * HEAD, HEAD), HEAD), span(n, tile)],
+                preferred_element_type=f32,
             )
-            return carry
-        return step
-
-    for k in range(inner - 1, 0, -1):
-        take(1, k)
-        lax.fori_loop(0, tiles, add_step(k), 0)
+            for k in ks
+        )
+
+    def add_step(n, carry):
+        acc[:, span(n, tile)] += rows_part((1, 2), n)
+        return carry
+
+    take(1, 1)
+    take(1, 2)
+    lax.fori_loop(0, tiles, add_step, 0)
+    take(1, 3)
     take(1, 0)
     out_own, out_mate = r.out_own, r.out_mate
 
@@ -828,9 +837,7 @@
         return local(pbuf.at[span(t, hb), span(n, tile)], out_own.at[:, span(n, tile)], r.fil_s)
 
     def mem_out_step(n, carry):
-        rows = pl.ds(pl.multiple_of(i * HEAD, HEAD), HEAD)
-        rest = jnp.dot(cin[1, i], ow[1, rows, span(n, tile)], preferred_element_type=f32)
-        pbuf[:, span(n, tile)] = (acc[:, span(n, tile)] + rest).astype(bf16)
+        pbuf[:, span(n, tile)] = (acc[:, span(n, tile)] + rows_part((3, 0), n)).astype(bf16)
         piece(n).start()
         stay(n).start()
         return carry

time: 95.7 us -> 93.9 us (0.981)
  Pallas kernels: 94.7 us -> 92.8 us
    pallas_call x1, Pallas kernels: 94.7 us -> 92.8 us  [whole_layer(): pl.pallas_call(functools.partial(layer_kernel, outer, inner, tp, names),...]
where the time goes in v5:
time: 93.9 us; the launch traced here: 93.8 us
  Pallas kernels  92.8 us (99%)
    pallas_call x1, Pallas kernels, whole_layer(): pl.pallas_call(functools.partial(layer_kernel, outer, inner, tp, names),...  92.8 us

profile of v5, /device:TPU:0, one launch (start us, length us, event | category | flops | bytes accessed | tf_op | source)
XLA Modules:
  0.0 93.8 jit_solution(1603986418883590269)
XLA Ops:
  0.0 92.8 %shard_map.154 = (bf16[128,2048]{1,0:T(8,128)(2,1)S(1)}, bf16[128,2048]{1,0:T(8,128)(2,1)S(1)}) custom-call(bf16[256,1024]{1,0:T(8,128)(2,1)} %refs_0_.1, f32[1,2048]{1,0:T(1,128)} %bitcast.9, bf16[128,1024]{1,0:T(8,128)(2,1)} %refs_2_.1, bf16[128,1024]{1,0:T(8,128)(2,1)} %refs_3_.1, bf16[128,1024]{1,0:T(8,128)(2,1)} %refs_4_.1, bf16[128,1024]{1,0:T(8,128)(2,1)} %refs_5_.1, ...), custom_call_target="tpu_custom_call" | custom-call | tf_op jit(solution)/shard_map/pallas_call | solution.py:953
  92.9 0.9 add_convert_fusion

commit v6 on v5

--- a/solution.py
+++ b/solution.py
@@ -424,6 +424,14 @@
 
     lax.fori_loop(0, inner, turn_step, 0)
 
+    @pl.when(primary)
+    def _():
+        pl.semaphore_wait(r.clear, 1)
+
+    deal_all(0, range(1, outer))
+    deal_all(1, range(1, outer))
+    deal_all(2, range(2))
+
     def project(n, j):
         return jnp.dot(nq[chunk(n), :], wfull[j], preferred_element_type=f32)
 
@@ -466,14 +474,6 @@
         return carry
 
     lax.fori_loop(0, inner, weight_step, 0)
-    @pl.when(primary)
-    def _():
-        pl.semaphore_wait(r.clear, 1)
-
-    deal_all(0, range(1, outer))
-    deal_all(1, range(1, outer))
-    deal_all(2, range(2))
-
     collect(0)
     gpad, conv, hsend, hrecv = r.gpad, r.conv, r.hsend, r.hrecv
     pad = hsend.shape[1]
@@ -777,8 +777,8 @@
     for ns in ([order[0]], [order[1]], [order[2], order[3]]):
         memory_rows(ns)
     acc, pbuf = r.acc, r.pbuf
-    tile = 512
-    tiles = model // tile
+    tile = half
+    tiles = tp
 
     def take(which, k):
         def hear():
@@ -889,7 +889,7 @@
     pad = 16
     f32, bf16 = jnp.float32, jnp.bfloat16
     dma = pltpu.SemaphoreType.DMA
-    tiles = model // 512
+    tiles = tp
     extra = args.log_decay_extra.T
     operands = dict(
         tokens=tokens, norm_gain=args.norm_gain[None],

time: 93.9 us -> 93.6 us (level)
  no operation moved by 1% of the time
where the time goes in v6:
time: 93.6 us; the launch traced here: 93.4 us
  Pallas kernels  92.5 us (99%)
    pallas_call x1, Pallas kernels, whole_layer(): pl.pallas_call(functools.partial(layer_kernel, outer, inner, tp, names),...  92.5 us

profile of v6, /device:TPU:0, one launch (start us, length us, event | category | flops | bytes accessed | tf_op | source)
XLA Modules:
  0.0 93.4 jit_solution(1993425841886321041)
XLA Ops:
  0.0 92.5 %shard_map.154 = (bf16[128,2048]{1,0:T(8,128)(2,1)S(1)}, bf16[128,2048]{1,0:T(8,128)(2,1)S(1)}) custom-call(bf16[256,1024]{1,0:T(8,128)(2,1)} %refs_0_.1, f32[1,2048]{1,0:T(1,128)} %bitcast.9, bf16[128,1024]{1,0:T(8,128)(2,1)} %refs_2_.1, bf16[128,1024]{1,0:T(8,128)(2,1)} %refs_3_.1, bf16[128,1024]{1,0:T(8,128)(2,1)} %refs_4_.1, bf16[128,1024]{1,0:T(8,128)(2,1)} %refs_5_.1, ...), custom_call_target="tpu_custom_call" | custom-call | tf_op jit(solution)/shard_map/pallas_call | solution.py:953
  92.5 0.9 add_convert_fusion
